TPU v7x, 32 devices: a whole 2x2x4 slice. The times are simulated.
32 devices in a mesh: ep: 16 (over z, y, x), tp: 2 (over core).
Axes of the slice: x: 2, y: 2, z: 4, core: 2. Of those that a mesh axis runs over, the one named last changes fastest.
Arguments:
- tokens: bfloat16 [3072, 2048], P('ep', 'tp'), may hold values from -6 to 6
- chosen: int32 [16, 384], P('ep'), may hold values from 0 to 3071, as said below
- gate_score: float32 [16, 384], P('ep'), may hold values from 0.1 to 1
- gate_weight: bfloat16 [16, 2048, 2048], P('ep', None, 'tp'), may hold values from -0.125 to 0.125
- up_weight: bfloat16 [16, 2048, 2048], P('ep', None, 'tp'), may hold values from -0.125 to 0.125
- down_weight: bfloat16 [16, 2048, 2048], P('ep', 'tp'), may hold values from -0.125 to 0.125
Outputs:
- mixed: bfloat16 [3072, 2048], P('ep', 'tp')
Inputs may be any that keep to these rules, and one draw needn't show every extreme that they name: For every expert and every s, columns s * 24 to (s + 1) * 24 - 1 of chosen name 24 different tokens, all among tokens s * 192 to (s + 1) * 192 - 1.
All inputs are finite; a program needn't handle non-finite values.
Results may differ from a plain program's by a relative error of at most 0.012.
Values may be sent and summed in bfloat16 or wider, within the bound.
No kernel may reach another device: no remote copies, remote signals or barrier semaphores. Data moves between devices by JAX's collectives and lax.ppermute only.
A program may use at most 128 MiB of HBM per device.

v0:
```python
import jax
import jax.numpy as jnp
from jax import lax
from jax.sharding import PartitionSpec as P


def on_device(tokens, chosen, gate_score, gate_weight, up_weight, down_weight):
    ep_count = lax.axis_size("ep")
    tok_rows = tokens.shape[0]
    per_source = chosen.shape[1] // ep_count
    offset = lax.axis_index("ep") * tok_rows
    w_gate = gate_weight[0]
    w_up = up_weight[0]
    w_down = down_weight[0]
    owned_ids = lax.all_to_all(
        chosen.reshape(ep_count, per_source), "ep", split_axis=0, concat_axis=0, tiled=True
    )
    local_rows = owned_ids.reshape(-1) - offset
    outgoing = jnp.take(tokens, local_rows, axis=0).reshape(ep_count, per_source, -1)
    arrived = lax.all_to_all(outgoing, "ep", split_axis=0, concat_axis=0, tiled=True).reshape(
        ep_count * per_source, -1
    )
    shard_piece = lax.all_gather(arrived, "tp", axis=1, tiled=True)
    gate_pre = jnp.dot(shard_piece, w_gate, preferred_element_type=jnp.float32)
    up_pre = jnp.dot(shard_piece, w_up, preferred_element_type=jnp.float32)
    hidden = (jax.nn.silu(gate_pre) * up_pre).astype(jnp.bfloat16)
    summed = lax.psum_scatter(
        jnp.einsum("fd,cf->dc", w_down, hidden, preferred_element_type=jnp.float32).astype(
            jnp.bfloat16
        ),
        "tp",
        scatter_dimension=0,
        tiled=True,
    ).astype(jnp.float32)
    weighted = (summed * gate_score[0][None, :]).astype(jnp.bfloat16)
    returned = lax.all_to_all(weighted, "ep", split_axis=1, concat_axis=1, tiled=True)
    positions = lax.broadcasted_iota(jnp.int32, (tok_rows, 1), 0)
    selector = (positions == local_rows[None, :]).astype(jnp.bfloat16)
    mixed_out = jnp.einsum("tc,dc->td", selector, returned, preferred_element_type=jnp.float32)
    return mixed_out.astype(jnp.bfloat16)


def solution(mesh):
    in_specs = (
        P("ep", "tp"),
        P("ep", None),
        P("ep", None),
        P("ep", None, "tp"),
        P("ep", None, "tp"),
        P("ep", "tp", None),
    )
    out_specs = P("ep", "tp")
    return jax.shard_map(
        on_device, mesh=mesh, in_specs=in_specs, out_specs=out_specs, check_vma=False
    )
```

profile of v0, /device:TPU:0, one launch (start us, length us, event | category | flops | bytes accessed | tf_op | source)
XLA Modules:
  0.0 118.5 jit_solution(7388291144038302701)
XLA Ops:
  6.5 0.0 copy-start
  6.5 0.7 reduce
  7.3 0.7 all_to_all.17
  8.0 8.3 %all-to-all-start = ((s32[16,1,24]{2,1,0:T(1,128)}), s32[16,1,24]{2,1,0:T(1,128)S(1)}, u32[]{:S(2)}, u32[]{:S(2)}) async-start(s32[16,1,24]{2,1,0:T(1,128)} %all_to_all.17), calls=%async_computation | async-start | bytes 16384 | tf_op jit(solution)/shard_map/all_to_all | solution.py:15
  16.3 0.0 all-gather.2.cloned.1.call-start
  16.4 7.2 %all-to-all-done = s32[16,1,24]{2,1,0:T(1,128)S(1)} async-done(((s32[16,1,24]{2,1,0:T(1,128)}), s32[16,1,24]{2,1,0:T(1,128)S(1)}, u32[]{:S(2)}, u32[]{:S(2)}) %all-to-all-start) | async-done | bytes 1568 | tf_op jit(solution)/shard_map/all_to_all | solution.py:15
  23.6 0.5 broadcast.65
  24.1 0.7 fusion.20
  24.8 0.1 sub.33
  24.9 0.0 copy-done
  24.9 2.1 %gather_fusion = bf16[384,1024]{1,0:T(8,128)(2,1)S(1)} fusion(bf16[192,1024]{1,0:T(8,128)(2,1)S(1)} %copy-done, s32[1024]{0:T(1024)S(1)} %pad_clamp_fusion), kind=kCustom, calls=%fused_computation | custom fusion | bytes 1574400 | tf_op jit(solution)/shard_map/jit(_take)/gather | solution.py:19
  27.0 0.1 broadcast_select_fusion
  27.1 23.4 %all_to_all.26 = bf16[16,24,1024]{2,1,0:T(8,128)(2,1)} all-to-all(bf16[16,24,1024]{2,1,0:T(8,128)(2,1)S(1)} %broadcast_select_fusion), channel_id=1, replica_groups=mesh['ep'=16,'tp'=2] {'ep'}, dimensions={0} | all-to-all | bytes 1572864 | tf_op jit(solution)/shard_map/all_to_all | solution.py:20
  50.6 0.0 all-gather.2.cloned.1.call-update
  50.6 0.0 reduce-scatter.2.cloned.1.call-start
  50.6 7.6 %all-gather.2.cloned.1.call-done = bf16[384,2048]{1,0:T(8,128)(2,1)} async-done(((bf16[384,1024]{1,0:T(8,128)(2,1)}), bf16[384,2048]{1,0:T(8,128)(2,1)}) %all-gather.2.cloned.1.call-update) | async-done | bytes 1572880 | tf_op jit(solution)/shard_map/all_gather | solution.py:23
  58.3 0.0 copy-start.2
  58.3 4.6 %fusion.4 = f32[384,1024]{1,0:T(8,128)S(1)} fusion(bf16[384,2048]{1,0:T(8,128)(2,1)} %all-gather.2.cloned.1.call-done, bf16[1,2048,1024]{2,1,0:T(8,128)(2,1)} %param.9), kind=kOutput, calls=%fused_computation.5 | convolution fusion | flops 1610612736 | bytes 7340032 | tf_op jit(solution)/shard_map/dot_general | solution.py:24
  62.8 0.0 copy-done.2
  62.8 8.2 %fusion.9 = bf16[2048,384]{0,1:T(8,128)(2,1)} fusion(bf16[1,1024,2048]{2,1,0:T(8,128)(2,1)} %param.11, f32[384,1024]{1,0:T(8,128)S(1)} %fusion.4, bf16[384,2048]{1,0:T(8,128)(2,1)S(1)} %copy-done.2, bf16[1,2048,1024]{2,1,0:T(8,128)(2,1)} %param.10), kind=kOutput, calls=%fused_computation.8 | convolution fusion | flops 3224371200 | bytes 13107200 | tf_op jit(solution)/shard_map/fd,cf->dc/dot_general | solution.py:28
  71.1 0.0 copy-start.1
  71.1 0.0 reduce-scatter.2.cloned.1.call-update
  71.1 0.7 copy-done.1
  71.8 9.6 %reduce-scatter.2.cloned.1.call-done = bf16[1024,384]{0,1:T(8,128)(2,1)} async-done(((bf16[2048,384]{0,1:T(8,128)(2,1)}), bf16[1024,384]{0,1:T(8,128)(2,1)}) %reduce-scatter.2.cloned.1.call-update) | async-done | bytes 786448 | tf_op jit(solution)/shard_map/reduce_scatter | solution.py:27
  81.4 2.2 %multiply_convert_fusion = bf16[1024,384]{0,1:T(8,128)(2,1)} fusion(bf16[1024,384]{0,1:T(8,128)(2,1)} %reduce-scatter.2.cloned.1.call-done, f32[384]{0:T(512)S(1)} %reduce.4), kind=kLoop, calls=%fused_computation.9 | loop fusion | flops 1179648 | bytes 1574400 | tf_op jit(solution)/shard_map/convert_element_type | solution.py:35
  83.6 6.9 %all-to-all-start.2 = ((bf16[1024,16,24]{0,2,1:T(8,128)(2,1)}), bf16[1024,16,24]{0,2,1:T(8,128)(2,1)S(1)}, u32[]{:S(2)}, u32[]{:S(2)}) async-start(bf16[1024,16,24]{0,2,1:T(8,128)(2,1)} %bitcast.7), calls=%async_computation.3 | async-start | bytes 1572864 | tf_op jit(solution)/shard_map/all_to_all | solution.py:36
  90.5 0.1 sub.31
  90.6 19.9 %all-to-all-done.2 = bf16[1024,16,24]{0,2,1:T(8,128)(2,1)S(1)} async-done(((bf16[1024,16,24]{0,2,1:T(8,128)(2,1)}), bf16[1024,16,24]{0,2,1:T(8,128)(2,1)S(1)}, u32[]{:S(2)}, u32[]{:S(2)}) %all-to-all-start.2) | async-done | bytes 786464 | tf_op jit(solution)/shard_map/all_to_all | solution.py:36
  110.5 1.1 convolution_convert_fusion
  (4 shorter events, 0.1 us)
Async XLA Ops:
  6.5 18.4 %copy-start = (bf16[192,1024]{1,0:T(8,128)(2,1)S(1)}, bf16[192,1024]{1,0:T(8,128)(2,1)}, u32[]{:S(2)}) copy-start(bf16[192,1024]{1,0:T(8,128)(2,1)} %param.6) | copy-start | bytes 1179652
  8.0 15.6 %all-to-all-start = ((s32[16,1,24]{2,1,0:T(1,128)}), s32[16,1,24]{2,1,0:T(1,128)S(1)}, u32[]{:S(2)}, u32[]{:S(2)}) async-start(s32[16,1,24]{2,1,0:T(1,128)} %all_to_all.17), calls=%async_computation | async-start | bytes 16384 | tf_op jit(solution)/shard_map/all_to_all | solution.py:15
  16.3 41.9 %all-gather.2.cloned.1.call-start = ((), (), s32[]{:S(2)}) async-start(), calls=%async_computation.4 | async-start | bytes 2359296 | tf_op jit(solution)/shard_map/all_gather | solution.py:23
  50.6 30.8 %reduce-scatter.2.cloned.1.call-start = ((), (), s32[]{:S(2)}) async-start(), calls=%async_computation.5 | async-start | bytes 2359296 | tf_op jit(solution)/shard_map/reduce_scatter | solution.py:27
  58.3 4.6 %copy-start.2 = (bf16[384,2048]{1,0:T(8,128)(2,1)S(1)}, bf16[384,2048]{1,0:T(8,128)(2,1)}, u32[]{:S(2)}) copy-start(bf16[384,2048]{1,0:T(8,128)(2,1)} %all-gather.2.cloned.1.call-done) | copy-start | bytes 4718596
  71.1 0.7 copy-start.1
  83.6 26.9 %all-to-all-start.2 = ((bf16[1024,16,24]{0,2,1:T(8,128)(2,1)}), bf16[1024,16,24]{0,2,1:T(8,128)(2,1)S(1)}, u32[]{:S(2)}, u32[]{:S(2)}) async-start(bf16[1024,16,24]{0,2,1:T(8,128)(2,1)} %bitcast.7), calls=%async_computation.3 | async-start | bytes 1572864 | tf_op jit(solution)/shard_map/all_to_all | solution.py:36
Sparse Core Ops, SparseCore 0:
  50.7 7.5 all-gather.1
  71.2 10.1 reduce-scatter.1
where the time goes:
time: 119 us; the launch traced here: 118 us
  waiting for transfers between devices  44.4 us (37%)
  blocking collectives  23.4 us (20%)
  starting transfers between devices  15.3 us (13%)
  matrix products  13.9 us (12%)
  between operations  13.5 us (11%)
  local copies, waits for them, and re-layouts  4.12 us (3%)
  other arithmetic  3.82 us (3%)
    all_to_all x1, blocking collectives, on_device(): lax.all_to_all(outgoing, 'ep', split_axis=0, concat_axis=0, tiled=True)  23.4 us
    all_to_all x1, waiting for transfers between devices, on_device(): lax.all_to_all(weighted, 'ep', split_axis=1, concat_axis=1, tiled=True)  19.9 us
    reduce_scatter x1, waiting for transfers between devices, on_device(): lax.psum_scatter(jnp.einsum('fd,cf->dc', w_down, hidden, preferred_elemen...  9.61 us
    all_to_all x1, starting transfers between devices, on_device(): lax.all_to_all(chosen.reshape(ep_count, per_source), 'ep', split_axis=0,...  8.34 us
    dot_general x1, matrix products, on_device(): jnp.einsum('fd,cf->dc', w_down, hidden, preferred_element_type=jnp.float32)  8.25 us
    all_gather x1, waiting for transfers between devices, on_device(): shard_piece = lax.all_gather(arrived, 'tp', axis=1, tiled=True)  7.62 us
    all_to_all x1, waiting for transfers between devices, on_device(): lax.all_to_all(chosen.reshape(ep_count, per_source), 'ep', split_axis=0,...  7.17 us
    all_to_all x1, starting transfers between devices, on_device(): lax.all_to_all(weighted, 'ep', split_axis=1, concat_axis=1, tiled=True)  6.88 us
  transfers between devices with their start and end apart: 4, of which 4 were waited for; matrix products, arithmetic and copies ran while one was open for 0% of the time, Pallas kernels for 0%

commit v1 on v0

v1 whole, which is shorter than its diff:
```python
import jax
import jax.numpy as jnp
from jax import lax
from jax.sharding import PartitionSpec as P


def on_device(tokens, chosen, gate_score, gate_weight, up_weight, down_weight):
    ep_count = lax.axis_size("ep")
    tok_rows, width = tokens.shape
    per_source = chosen.shape[1] // ep_count
    offset = lax.axis_index("ep") * tok_rows
    core = lax.axis_index("tp")
    swap = [(0, 1), (1, 0)]
    w_gate = gate_weight[0]
    w_up = up_weight[0]
    w_down = down_weight[0]
    owned_ids = lax.all_to_all(
        chosen.reshape(ep_count, per_source), "ep", split_axis=0, concat_axis=0, tiled=True
    )
    local_rows = owned_ids.reshape(-1) - offset
    positions = lax.broadcasted_iota(jnp.int32, (1, tok_rows), 1)
    selector = (local_rows[:, None] == positions).astype(jnp.bfloat16)
    outgoing = jnp.dot(selector, tokens, preferred_element_type=jnp.float32).astype(jnp.bfloat16)
    arrived = lax.all_to_all(
        outgoing.reshape(ep_count, per_source, width), "ep", split_axis=0, concat_axis=0, tiled=True
    ).reshape(ep_count * per_source, width)
    other = lax.ppermute(arrived, "tp", swap)
    first = core == 0
    picked = jnp.concatenate(
        [jnp.where(first, arrived, other), jnp.where(first, other, arrived)], axis=1
    )
    gate_pre = jnp.dot(picked, w_gate, preferred_element_type=jnp.float32)
    up_pre = jnp.dot(picked, w_up, preferred_element_type=jnp.float32)
    hidden = (jax.nn.silu(gate_pre) * up_pre).astype(jnp.bfloat16)
    partial = jnp.dot(hidden, w_down, preferred_element_type=jnp.float32).astype(jnp.bfloat16)
    kept = lax.dynamic_slice_in_dim(partial, core * width, width, axis=1)
    sent = lax.dynamic_slice_in_dim(partial, (1 - core) * width, width, axis=1)
    got = lax.ppermute(sent, "tp", swap)
    summed = kept.astype(jnp.float32) + got.astype(jnp.float32)
    weighted = (summed * gate_score[0][:, None]).astype(jnp.bfloat16)
    returned = lax.all_to_all(
        weighted.reshape(ep_count, per_source, width), "ep", split_axis=0, concat_axis=0, tiled=True
    ).reshape(ep_count * per_source, width)
    rows = lax.broadcasted_iota(jnp.int32, (tok_rows, 1), 0)
    gather = (rows == local_rows[None, :]).astype(jnp.bfloat16)
    mixed_out = jnp.dot(gather, returned, preferred_element_type=jnp.float32)
    return mixed_out.astype(jnp.bfloat16)


def solution(mesh):
    in_specs = (
        P("ep", "tp"),
        P("ep", None),
        P("ep", None),
        P("ep", None, "tp"),
        P("ep", None, "tp"),
        P("ep", "tp", None),
    )
    out_specs = P("ep", "tp")
    return jax.shard_map(
        on_device, mesh=mesh, in_specs=in_specs, out_specs=out_specs, check_vma=False
    )
```

time: 119 us -> 84.3 us (0.71)
  waiting for transfers between devices: 44.4 us -> 11.2 us
  blocking collectives: 23.4 us -> 47.5 us
  between operations: 13.5 us -> 0.07 us
  starting transfers between devices: 15.3 us -> 8.55 us
  local copies, waits for them, and re-layouts: 4.12 us -> 1.25 us
  other arithmetic: 3.82 us -> 1.29 us
    all_to_all x1 -> x2, blocking collectives: 23.4 us -> 47.5 us  [the longest x1 24.7 us: on_device(): lax.all_to_all(weighted.reshape(ep_count, per_source, width), 'ep', split...]
    all_to_all x1 -> x0, waiting for transfers between devices: 19.9 us -> none  [on_device(): lax.all_to_all(weighted, 'ep', split_axis=1, concat_axis=1, tiled=True)]
    reduce_scatter x1 -> x0, waiting for transfers between devices: 9.61 us -> none  [on_device(): lax.psum_scatter(jnp.einsum('fd,cf->dc', w_down, hidden, preferred_elemen...]
    all_gather x1 -> x0, waiting for transfers between devices: 7.62 us -> none  [on_device(): shard_piece = lax.all_gather(arrived, 'tp', axis=1, tiled=True)]
    all_to_all x1 -> x0, starting transfers between devices: 6.88 us -> none  [on_device(): lax.all_to_all(weighted, 'ep', split_axis=1, concat_axis=1, tiled=True)]
    ppermute x0 -> x2, waiting for transfers between devices: none -> 4.02 us  [the longest x1 2.28 us: on_device(): other = lax.ppermute(arrived, 'tp', swap)]
    gather x1 -> x0, local copies, waits for them, and re-layouts: 2.07 us -> none  [on_device(): jnp.take(tokens, local_rows, axis=0).reshape(ep_count, per_source, -1)]
    convert_element_type x1, other arithmetic: 2.2 us -> 0.24 us  [on_device(): weighted = (summed * gate_score[0][:, None]).astype(jnp.bfloat16)]
  transfers between devices with their start and end apart: 4 -> 3, of which waited for: 4 -> 3; matrix products, arithmetic and copies ran while one was open for 0% -> 0% of each run, Pallas kernels for 0% -> 0%
where the time goes in v1:
time: 84.3 us; the launch traced here: 84 us
  blocking collectives  47.5 us (56%)
  matrix products  14.1 us (17%)
  waiting for transfers between devices  11.2 us (13%)
  starting transfers between devices  8.55 us (10%)
  other arithmetic  1.29 us (2%)
  local copies, waits for them, and re-layouts  1.25 us (1%)
    all_to_all x1, blocking collectives, on_device(): lax.all_to_all(weighted.reshape(ep_count, per_source, width), 'ep', split...  24.7 us
    all_to_all x1, blocking collectives, on_device(): lax.all_to_all(outgoing.reshape(ep_count, per_source, width), 'ep', split...  22.8 us
    all_to_all x1, starting transfers between devices, on_device(): lax.all_to_all(chosen.reshape(ep_count, per_source), 'ep', split_axis=0,...  8.34 us
    dot_general x1, matrix products, on_device(): jnp.dot(hidden, w_down, preferred_element_type=jnp.float32)  7.44 us
    all_to_all x1, waiting for transfers between devices, on_device(): lax.all_to_all(chosen.reshape(ep_count, per_source), 'ep', split_axis=0,...  7.22 us
    dot_general x1, matrix products, on_device(): gate_pre = jnp.dot(picked, w_gate, preferred_element_type=jnp.float32)  5.16 us
    ppermute x1, waiting for transfers between devices, on_device(): other = lax.ppermute(arrived, 'tp', swap)  2.28 us
    ppermute x1, waiting for transfers between devices, on_device(): got = lax.ppermute(sent, 'tp', swap)  1.74 us
  transfers between devices with their start and end apart: 3, of which 3 were waited for; matrix products, arithmetic and copies ran while one was open for 0% of the time, Pallas kernels for 0%

profile of v1, /device:TPU:0, one launch (start us, length us, event | category | flops | bytes accessed | tf_op | source)
XLA Modules:
  0.0 84.0 jit_solution(10658658547064016797)
XLA Ops:
  0.0 0.0 copy-start
  0.0 0.7 reduce
  0.8 0.7 all_to_all.12
  1.5 8.3 %all-to-all-start = ((s32[16,1,24]{2,1,0:T(1,128)}), s32[16,1,24]{2,1,0:T(1,128)S(1)}, u32[]{:S(2)}, u32[]{:S(2)}) async-start(s32[16,1,24]{2,1,0:T(1,128)} %all_to_all.12), calls=%async_computation | async-start | bytes 16384 | tf_op jit(solution)/shard_map/all_to_all | solution.py:17
  9.8 7.2 %all-to-all-done = s32[16,1,24]{2,1,0:T(1,128)S(1)} async-done(((s32[16,1,24]{2,1,0:T(1,128)}), s32[16,1,24]{2,1,0:T(1,128)S(1)}, u32[]{:S(2)}, u32[]{:S(2)}) %all-to-all-start) | async-done | bytes 1568 | tf_op jit(solution)/shard_map/all_to_all | solution.py:17
  17.1 0.1 sub.22
  17.1 0.0 copy-done
  17.2 0.4 convolution_convert_fusion
  17.6 22.8 %all_to_all.19 = bf16[16,24,1024]{2,1,0:T(8,128)(2,1)S(1)} all-to-all(bf16[16,24,1024]{2,1,0:T(8,128)(2,1)S(1)} %bitcast.24), channel_id=1, replica_groups=mesh['ep'=16,'tp'=2] {'ep'}, dimensions={0} | all-to-all | bytes 1572864 | tf_op jit(solution)/shard_map/all_to_all | solution.py:24
  40.3 0.0 collective-permute-start
  40.3 2.3 %collective-permute-done = bf16[384,1024]{1,0:T(8,128)(2,1)S(1)} collective-permute-done((bf16[384,1024]{1,0:T(8,128)(2,1)S(1)}, bf16[384,1024]{1,0:T(8,128)(2,1)S(1)}, u32[]{:S(2)}, u32[]{:S(2)}) %collective-permute-start) | collective-permute-done | bytes 786464 | tf_op jit(solution)/shard_map/ppermute | solution.py:27
  42.6 0.3 broadcast_select_fusion.1
  42.9 5.2 %fusion.4 = f32[384,1024]{1,0:T(8,128)} fusion(bf16[1,2048,1024]{2,1,0:T(8,128)(2,1)} %param.9, bf16[384,1024]{1,0:T(8,128)(2,1)S(1)} %get-tuple-element.6, bf16[384,1024]{1,0:T(8,128)(2,1)S(1)} %get-tuple-element.5), kind=kOutput, calls=%fused_computation.4 | convolution fusion | flops 1613758464 | bytes 7340032 | tf_op jit(solution)/shard_map/dot_general | solution.py:32
  48.0 7.4 %fusion.6 = bf16[384,2048]{1,0:T(8,128)(2,1)S(1)} fusion(bf16[1,1024,2048]{2,1,0:T(8,128)(2,1)} %param.11, f32[384,1024]{1,0:T(8,128)} %fusion.4, bf16[1,2048,1024]{2,1,0:T(8,128)(2,1)} %param.10, bf16[384,1024]{1,0:T(8,128)(2,1)S(1)} %get-tuple-element.6, bf16[384,1024]{1,0:T(8,128)(2,1)S(1)} %get-tuple-element.5), kind=kOutput, calls=%fused_computation.6 | convolution fusion | flops 3227516928 | bytes 13107200 | tf_op jit(solution)/shard_map/dot_general | solution.py:35
  55.5 0.0 copy-start.1
  55.5 0.1 constant_dynamic-slice_fusion
  55.6 0.2 collective-permute-start.1
  55.8 0.4 copy-done.1
  56.2 1.7 %collective-permute-done.1 = bf16[384,1024]{1,0:T(8,128)(2,1)S(1)} collective-permute-done((bf16[384,1024]{1,0:T(8,128)(2,1)S(1)}, bf16[384,1024]{1,0:T(8,128)(2,1)S(1)}, u32[]{:S(2)}, u32[]{:S(2)}) %collective-permute-start.1) | collective-permute-done | bytes 786464 | tf_op jit(solution)/shard_map/ppermute | solution.py:38
  57.9 0.2 multiply_convert_fusion
  58.2 24.7 %all_to_all.20 = bf16[16,24,1024]{2,1,0:T(8,128)(2,1)S(1)} all-to-all(bf16[16,24,1024]{2,1,0:T(8,128)(2,1)S(1)} %bitcast.25), channel_id=1, replica_groups=mesh['ep'=16,'tp'=2] {'ep'}, dimensions={0} | all-to-all | bytes 1572864 | tf_op jit(solution)/shard_map/all_to_all | solution.py:41
  82.9 1.1 %convolution_convert_fusion.1 = bf16[192,1024]{1,0:T(8,128)(2,1)} fusion(bf16[384,1024]{1,0:T(8,128)(2,1)S(1)} %bitcast.23, s32[384]{0:T(512)S(1)} %sub.22), kind=kOutput, calls=%fused_computation.11 | convolution fusion | flops 151265280 | bytes 1181184 | tf_op jit(solution)/shard_map/dot_general | solution.py:46
  (2 shorter events, 0.0 us)
Async XLA Ops:
  0.0 17.1 %copy-start = (bf16[192,1024]{1,0:T(8,128)(2,1)S(1)}, bf16[192,1024]{1,0:T(8,128)(2,1)}, u32[]{:S(2)}) copy-start(bf16[192,1024]{1,0:T(8,128)(2,1)} %param.6) | copy-start | bytes 1179652
  1.5 15.6 %all-to-all-start = ((s32[16,1,24]{2,1,0:T(1,128)}), s32[16,1,24]{2,1,0:T(1,128)S(1)}, u32[]{:S(2)}, u32[]{:S(2)}) async-start(s32[16,1,24]{2,1,0:T(1,128)} %all_to_all.12), calls=%async_computation | async-start | bytes 16384 | tf_op jit(solution)/shard_map/all_to_all | solution.py:17
  40.3 2.3 %collective-permute-start = (bf16[384,1024]{1,0:T(8,128)(2,1)S(1)}, bf16[384,1024]{1,0:T(8,128)(2,1)S(1)}, u32[]{:S(2)}, u32[]{:S(2)}) collective-permute-start(bf16[384,1024]{1,0:T(8,128)(2,1)S(1)} %bitcast.26), channel_id=1, source_target_pairs={{0,1},{1,0},{2,3},{3,2},{4,5},{5,4},{6,7},{7,6},{8,9},{9,8},{10,11... | collective-permute-start | bytes 2359304 | tf_op jit(solution)/shard_map/ppermute | solution.py:27
  55.5 0.7 copy-start.1
  55.6 2.4 %collective-permute-start.1 = (bf16[384,1024]{1,0:T(8,128)(2,1)S(1)}, bf16[384,1024]{1,0:T(8,128)(2,1)S(1)}, u32[]{:S(2)}, u32[]{:S(2)}) collective-permute-start(bf16[384,1024]{1,0:T(8,128)(2,1)S(1)} %constant_dynamic-slice_fusion), channel_id=1, source_target_pairs={{0,1},{1,0},{2,3},{3,2},{4,5},{5,4},{6,7},{7,6},{8,9},{9,8},{10,11... | collective-permute-start | bytes 2359304 | tf_op jit(solution)/shard_map/ppermute | solution.py:38

commit v2 on v1

v2 whole, which is shorter than its diff:
```python
import jax
import jax.numpy as jnp
from jax import lax
from jax.experimental import pallas as pl
from jax.experimental.pallas import tpu as pltpu
from jax.sharding import PartitionSpec as P


def tiles_of(count):
    tile = 256 if count % 256 == 0 else count
    return [pl.ds(start, tile) for start in range(0, count, tile)]


def half(ref, which, width):
    return pl.ds(pl.multiple_of(which * width, width), width)


def first_kernel(core_ref, own_ref, gate_hbm, up_hbm, gate_ref, up_ref, gate_buf, up_buf, sems):
    width = own_ref.shape[1]
    rows = half(gate_hbm, core_ref[0], width)
    cols = tiles_of(gate_ref.shape[1])
    pairs = ((gate_hbm, gate_buf), (up_hbm, up_buf))
    copies = [
        [pltpu.make_async_copy(src.at[0, rows, c], buf.at[:, c], sems.at[k, j]) for k, (src, buf) in enumerate(pairs)]
        for j, c in enumerate(cols)
    ]
    for step in copies:
        for copy in step:
            copy.start()
    for c, step in zip(cols, copies):
        for copy, out, buf in zip(step, (gate_ref, up_ref), (gate_buf, up_buf)):
            copy.wait()
            out[:, c] = jnp.dot(own_ref[...], buf[:, c], preferred_element_type=jnp.float32)


def second_kernel(
    core_ref, other_ref, gate_ref, up_ref, gate_hbm, up_hbm, down_hbm, hidden_ref, send_ref, gate_buf, up_buf, down_buf, sems
):
    width = other_ref.shape[1]
    theirs = half(gate_hbm, 1 - core_ref[0], width)
    cols = tiles_of(gate_ref.shape[1])
    outs = tiles_of(width)
    pairs = ((gate_hbm, gate_buf), (up_hbm, up_buf))
    copies = [
        [pltpu.make_async_copy(src.at[0, theirs, c], buf.at[:, c], sems.at[k, j]) for k, (src, buf) in enumerate(pairs)]
        for j, c in enumerate(cols)
    ]
    down_copy = pltpu.make_async_copy(down_hbm.at[0, :, theirs], down_buf, sems.at[2, 0])
    for step in copies:
        for copy in step:
            copy.start()
    down_copy.start()
    for c, (gate_copy, up_copy) in zip(cols, copies):
        gate_copy.wait()
        gate_pre = gate_ref[:, c] + jnp.dot(
            other_ref[...], gate_buf[:, c], preferred_element_type=jnp.float32
        )
        up_copy.wait()
        up_pre = up_ref[:, c] + jnp.dot(
            other_ref[...], up_buf[:, c], preferred_element_type=jnp.float32
        )
        hidden_ref[:, c] = (gate_pre / (1.0 + jnp.exp(-gate_pre)) * up_pre).astype(jnp.bfloat16)
    down_copy.wait()
    for c in outs:
        send_ref[:, c] = jnp.dot(
            hidden_ref[...], down_buf[:, c], preferred_element_type=jnp.float32
        ).astype(jnp.bfloat16)


def third_kernel(core_ref, hidden_ref, down_hbm, keep_ref, down_buf, sems):
    width = keep_ref.shape[1]
    cols = tiles_of(width)
    start = core_ref[0] * width
    copies = []
    for j, c in enumerate(cols):
        at = pl.ds(pl.multiple_of(start + c.start, c.size), c.size)
        copies.append(pltpu.make_async_copy(down_hbm.at[0, :, at], down_buf.at[:, c], sems.at[j]))
    for copy in copies:
        copy.start()
    for c, copy in zip(cols, copies):
        copy.wait()
        keep_ref[:, c] = jnp.dot(
            hidden_ref[...], down_buf[:, c], preferred_element_type=jnp.float32
        )


SMEM = pl.BlockSpec(memory_space=pltpu.SMEM)
VMEM = pl.BlockSpec(memory_space=pltpu.VMEM)
HBM = pl.BlockSpec(memory_space=pltpu.HBM)


def call(body, name, in_specs, outs, scratch, flops, nbytes):
    return pl.pallas_call(
        body,
        out_shape=outs,
        in_specs=in_specs,
        out_specs=tuple(VMEM for _ in outs),
        scratch_shapes=scratch,
        cost_estimate=pl.CostEstimate(flops=flops, bytes_accessed=nbytes, transcendentals=0),
        compiler_params=pltpu.CompilerParams(vmem_limit_bytes=48 << 20),
        name=name,
    )


def first_half(core, own, w_gate, w_up):
    rows, width = own.shape
    hidden = w_gate.shape[2]
    pre = jax.ShapeDtypeStruct((rows, hidden), jnp.float32)
    buf = pltpu.VMEM((width, hidden), jnp.bfloat16)
    sems = pltpu.SemaphoreType.DMA((2, len(tiles_of(hidden))))
    return call(
        first_kernel, "ffn_first", [SMEM, VMEM, HBM, HBM], (pre, pre), [buf, buf, sems],
        4 * rows * width * hidden, 4 * width * hidden,
    )(core, own, w_gate, w_up)


def second_half(core, other, gate_pre, up_pre, w_gate, w_up, w_down):
    rows, width = other.shape
    hidden = w_gate.shape[2]
    buf = pltpu.VMEM((width, hidden), jnp.bfloat16)
    sems = pltpu.SemaphoreType.DMA((3, len(tiles_of(hidden))))
    return call(
        second_kernel, "ffn_second", [SMEM, VMEM, VMEM, VMEM, HBM, HBM, HBM],
        (jax.ShapeDtypeStruct((rows, hidden), jnp.bfloat16), jax.ShapeDtypeStruct((rows, width), jnp.bfloat16)),
        [buf, buf, pltpu.VMEM((hidden, width), jnp.bfloat16), sems],
        6 * rows * width * hidden, 6 * width * hidden,
    )(core, other, gate_pre, up_pre, w_gate, w_up, w_down)


def third_part(core, hidden, w_down, width):
    rows, units = hidden.shape
    return call(
        third_kernel, "ffn_third", [SMEM, VMEM, HBM],
        (jax.ShapeDtypeStruct((rows, width), jnp.float32),),
        [pltpu.VMEM((units, width), jnp.bfloat16), pltpu.SemaphoreType.DMA((len(tiles_of(width)),))],
        2 * rows * width * units, 2 * width * units,
    )(core, hidden, w_down)[0]


def on_device(tokens, chosen, gate_score, gate_weight, up_weight, down_weight):
    ep_count = lax.axis_size("ep")
    tok_rows, width = tokens.shape
    per_source = chosen.shape[1] // ep_count
    offset = lax.axis_index("ep") * tok_rows
    core = lax.axis_index("tp").astype(jnp.int32).reshape(1)
    swap = [(0, 1), (1, 0)]
    owned_ids = lax.all_to_all(
        chosen.reshape(ep_count, per_source), "ep", split_axis=0, concat_axis=0, tiled=True
    )
    local_rows = owned_ids.reshape(-1) - offset
    positions = lax.broadcasted_iota(jnp.int32, (1, tok_rows), 1)
    selector = (local_rows[:, None] == positions).astype(jnp.bfloat16)
    outgoing = jnp.dot(selector, tokens, preferred_element_type=jnp.float32).astype(jnp.bfloat16)
    arrived = lax.all_to_all(
        outgoing.reshape(ep_count, per_source, width), "ep", split_axis=0, concat_axis=0, tiled=True
    ).reshape(ep_count * per_source, width)
    other = lax.ppermute(arrived, "tp", swap)
    gate_pre, up_pre = first_half(core, arrived, gate_weight, up_weight)
    hidden, sent = second_half(core, other, gate_pre, up_pre, gate_weight, up_weight, down_weight)
    got = lax.ppermute(sent, "tp", swap)
    kept = third_part(core, hidden, down_weight, width)
    summed = kept + got.astype(jnp.float32)
    weighted = (summed * gate_score[0][:, None]).astype(jnp.bfloat16)
    returned = lax.all_to_all(
        weighted.reshape(ep_count, per_source, width), "ep", split_axis=0, concat_axis=0, tiled=True
    ).reshape(ep_count * per_source, width)
    rows = lax.broadcasted_iota(jnp.int32, (tok_rows, 1), 0)
    gather = (rows == local_rows[None, :]).astype(jnp.bfloat16)
    mixed_out = jnp.dot(gather, returned, preferred_element_type=jnp.float32)
    return mixed_out.astype(jnp.bfloat16)


def solution(mesh):
    in_specs = (
        P("ep", "tp"),
        P("ep", None),
        P("ep", None),
        P("ep", None, "tp"),
        P("ep", None, "tp"),
        P("ep", "tp", None),
    )
    out_specs = P("ep", "tp")
    return jax.shard_map(
        on_device, mesh=mesh, in_specs=in_specs, out_specs=out_specs, check_vma=False
    )
```

time: 84.3 us -> 82.7 us (0.981)
  Pallas kernels: 0 us -> 15.5 us
  matrix products: 14.1 us -> 1.53 us
  waiting for transfers between devices: 11.2 us -> 7.23 us
    pallas_call x0 -> x3, Pallas kernels: none -> 15.5 us  [the longest x1 6.61 us: second_half(): call(second_kernel, 'ffn_second', [SMEM, VMEM, VMEM, VMEM, HBM, HBM, HBM]...]
    dot_general x2 -> x0, matrix products: 12.6 us -> none  [the longest x1 7.44 us: on_device(): jnp.dot(hidden, w_down, preferred_element_type=jnp.float32)]
    ppermute x1, waiting for transfers between devices: 2.28 us -> 0.01 us  [on_device(): other = lax.ppermute(arrived, 'tp', swap)]
    ppermute x1, waiting for transfers between devices: 1.74 us -> 0.01 us  [on_device(): got = lax.ppermute(sent, 'tp', swap)]
  transfers between devices with their start and end apart: 3 -> 3, of which waited for: 3 -> 1; matrix products, arithmetic and copies ran while one was open for 0% -> 0% of each run, Pallas kernels for 0% -> 11%
where the time goes in v2:
time: 82.7 us; the launch traced here: 82.4 us
  blocking collectives  47.4 us (57%)
  Pallas kernels  15.5 us (19%)
  starting transfers between devices  8.91 us (11%)
  waiting for transfers between devices  7.23 us (9%)
  matrix products  1.53 us (2%)
  other arithmetic  1.05 us (1%)
    all_to_all x1, blocking collectives, on_device(): lax.all_to_all(weighted.reshape(ep_count, per_source, width), 'ep', split...  24.6 us
    all_to_all x1, blocking collectives, on_device(): lax.all_to_all(outgoing.reshape(ep_count, per_source, width), 'ep', split...  22.8 us
    all_to_all x1, starting transfers between devices, on_device(): lax.all_to_all(chosen.reshape(ep_count, per_source), 'ep', split_axis=0,...  8.34 us
    all_to_all x1, waiting for transfers between devices, on_device(): lax.all_to_all(chosen.reshape(ep_count, per_source), 'ep', split_axis=0,...  7.22 us
    pallas_call x1, Pallas kernels, second_half(): call(second_kernel, 'ffn_second', [SMEM, VMEM, VMEM, VMEM, HBM, HBM, HBM]...  6.61 us
    pallas_call x1, Pallas kernels, first_half(): call(first_kernel, 'ffn_first', [SMEM, VMEM, HBM, HBM], (pre, pre), [buf,...  5.56 us
    pallas_call x1, Pallas kernels, third_part(): call(third_kernel, 'ffn_third', [SMEM, VMEM, HBM], (jax.ShapeDtypeStruct(...  3.3 us
  transfers between devices with their start and end apart: 3, of which 1 were waited for; matrix products, arithmetic and copies ran while one was open for 0% of the time, Pallas kernels for 11%

profile of v2, /device:TPU:0, one launch (start us, length us, event | category | flops | bytes accessed | tf_op | source)
XLA Modules:
  0.0 82.4 jit_solution(6070592575001093737)
XLA Ops:
  0.0 0.0 copy-start
  0.0 0.7 reduce
  0.8 0.7 all_to_all.12
  1.5 8.3 %all-to-all-start = ((s32[16,1,24]{2,1,0:T(1,128)}), s32[16,1,24]{2,1,0:T(1,128)S(1)}, u32[]{:S(2)}, u32[]{:S(2)}) async-start(s32[16,1,24]{2,1,0:T(1,128)} %all_to_all.12), calls=%async_computation | async-start | bytes 16384 | tf_op jit(solution)/shard_map/all_to_all | solution.py:147
  9.8 7.2 %all-to-all-done = s32[16,1,24]{2,1,0:T(1,128)S(1)} async-done(((s32[16,1,24]{2,1,0:T(1,128)}), s32[16,1,24]{2,1,0:T(1,128)S(1)}, u32[]{:S(2)}, u32[]{:S(2)}) %all-to-all-start) | async-done | bytes 1568 | tf_op jit(solution)/shard_map/all_to_all | solution.py:147
  17.1 0.1 sub.19
  17.1 0.0 copy-done
  17.2 0.4 convolution_convert_fusion
  17.6 22.8 %all_to_all.19 = bf16[16,24,1024]{2,1,0:T(8,128)(2,1)S(1)} all-to-all(bf16[16,24,1024]{2,1,0:T(8,128)(2,1)S(1)} %bitcast.10), channel_id=1, replica_groups=mesh['ep'=16,'tp'=2] {'ep'}, dimensions={0} | all-to-all | bytes 1572864 | tf_op jit(solution)/shard_map/all_to_all | solution.py:154
  40.3 0.0 collective-permute-start
  40.3 5.6 %ffn_first.1 = (f32[384,1024]{1,0:T(8,128)S(1)}, f32[384,1024]{1,0:T(8,128)S(1)}) custom-call(s32[1]{0:T(128)} %bitcast.core_ref, bf16[384,1024]{1,0:T(8,128)(2,1)S(1)} %bitcast.8, bf16[1,2048,1024]{2,1,0:T(8,128)(2,1)} %gate_hbm.3, bf16[1,2048,1024]{2,1,0:T(8,128)(2,1)} %up_hbm.3), custom_call_target="tpu_custom_call" | custom-call | flops 1610612736 | bytes 4194304 | tf_op jit(solution)/shard_map/ffn_first/pallas_call | solution.py:111
  45.9 0.0 collective-permute-done.other_ref
  45.9 0.0 copy-start.1
  45.9 6.6 %ffn_second.1 = (bf16[384,1024]{1,0:T(8,128)(2,1)S(1)}, bf16[384,1024]{1,0:T(8,128)(2,1)S(1)}) custom-call(s32[1]{0:T(128)} %bitcast.core_ref, bf16[384,1024]{1,0:T(8,128)(2,1)S(1)} %collective-permute-done.other_ref, f32[384,1024]{1,0:T(8,128)S(1)} %get-tuple-element.9.gate_ref, f32[384,1024]{1,0:T(8,128)S(1)} %get-tuple-element.10.up_ref, ...), custom_call_target="tpu_custom_call" | custom-call | flops 2415919104 | bytes 6291456 | tf_op jit(solution)/shard_map/ffn_second/pallas_call | solution.py:122
  52.5 0.6 collective-permute-start.1
  53.1 0.0 copy-done.1
  53.1 3.3 %ffn_third.1 = f32[384,1024]{1,0:T(8,128)S(1)} custom-call(s32[1]{0:T(128)} %bitcast.core_ref, bf16[384,1024]{1,0:T(8,128)(2,1)S(1)} %get-tuple-element.11.hidden_ref, bf16[1,1024,2048]{2,1,0:T(8,128)(2,1)} %down_hbm.3), custom_call_target="tpu_custom_call" | custom-call | flops 805306368 | bytes 2097152 | tf_op jit(solution)/shard_map/ffn_third/pallas_call | solution.py:132
  56.4 0.0 collective-permute-done.1
  56.5 0.3 multiply_convert_fusion
  56.7 24.6 %all_to_all.20 = bf16[16,24,1024]{2,1,0:T(8,128)(2,1)S(1)} all-to-all(bf16[16,24,1024]{2,1,0:T(8,128)(2,1)S(1)} %bitcast.11), channel_id=1, replica_groups=mesh['ep'=16,'tp'=2] {'ep'}, dimensions={0} | all-to-all | bytes 1572864 | tf_op jit(solution)/shard_map/all_to_all | solution.py:164
  81.3 1.1 %convolution_convert_fusion.1 = bf16[192,1024]{1,0:T(8,128)(2,1)} fusion(bf16[384,1024]{1,0:T(8,128)(2,1)S(1)} %bitcast.9, s32[384]{0:T(512)S(1)} %sub.19), kind=kOutput, calls=%fused_computation.2 | convolution fusion | flops 151265280 | bytes 1181184 | tf_op jit(solution)/shard_map/dot_general | solution.py:169
  (2 shorter events, 0.0 us)
Async XLA Ops:
  0.0 17.1 %copy-start = (bf16[192,1024]{1,0:T(8,128)(2,1)S(1)}, bf16[192,1024]{1,0:T(8,128)(2,1)}, u32[]{:S(2)}) copy-start(bf16[192,1024]{1,0:T(8,128)(2,1)} %param.6) | copy-start | bytes 1179652
  1.5 15.6 %all-to-all-start = ((s32[16,1,24]{2,1,0:T(1,128)}), s32[16,1,24]{2,1,0:T(1,128)S(1)}, u32[]{:S(2)}, u32[]{:S(2)}) async-start(s32[16,1,24]{2,1,0:T(1,128)} %all_to_all.12), calls=%async_computation | async-start | bytes 16384 | tf_op jit(solution)/shard_map/all_to_all | solution.py:147
  40.3 5.6 %collective-permute-start = (bf16[384,1024]{1,0:T(8,128)(2,1)S(1)}, bf16[384,1024]{1,0:T(8,128)(2,1)S(1)}, u32[]{:S(2)}, u32[]{:S(2)}) collective-permute-start(bf16[384,1024]{1,0:T(8,128)(2,1)S(1)} %bitcast.7), channel_id=1, source_target_pairs={{0,1},{1,0},{2,3},{3,2},{4,5},{5,4},{6,7},{7,6},{8,9},{9,8},{10,11... | collective-permute-start | bytes 2359304 | tf_op jit(solution)/shard_map/ppermute | solution.py:157
  45.9 7.2 %copy-start.1 = (f32[1,384]{1,0:T(1,128)S(1)}, f32[1,384]{1,0:T(1,128)}, u32[]{:S(2)}) copy-start(f32[1,384]{1,0:T(1,128)} %param.8) | copy-start | bytes 4612
  52.5 3.9 %collective-permute-start.1 = (bf16[384,1024]{1,0:T(8,128)(2,1)S(1)}, bf16[384,1024]{1,0:T(8,128)(2,1)S(1)}, u32[]{:S(2)}, u32[]{:S(2)}) collective-permute-start(bf16[384,1024]{1,0:T(8,128)(2,1)S(1)} %get-tuple-element.12), channel_id=1, source_target_pairs={{0,1},{1,0},{2,3},{3,2},{4,5},{5,4},{6,7},{7,6},{8,9},{9,8},{10,11... | collective-permute-start | bytes 2359304 | tf_op jit(solution)/shard_map/ppermute | solution.py:160

commit v3 on v1

v3 whole, which is shorter than its diff:
```python
import jax
import jax.numpy as jnp
from jax import lax
from jax.experimental import pallas as pl
from jax.experimental.pallas import tpu as pltpu
from jax.sharding import PartitionSpec as P

SMEM = pl.BlockSpec(memory_space=pltpu.SMEM)
VMEM = pl.BlockSpec(memory_space=pltpu.VMEM)
HBM = pl.BlockSpec(memory_space=pltpu.HBM)
MIB = 1 << 20


def nbytes(x):
    return x.size * x.dtype.itemsize


def call(body, name, in_specs, outs, flops, args, scratch=(), grant=0):
    held = sum(nbytes(x) for x in outs)
    held += sum(nbytes(x) for x, spec in zip(args, in_specs) if spec is VMEM)
    return pl.pallas_call(
        body,
        out_shape=outs,
        in_specs=in_specs,
        out_specs=tuple(VMEM for _ in outs),
        scratch_shapes=scratch,
        cost_estimate=pl.CostEstimate(flops=flops, bytes_accessed=held, transcendentals=0),
        compiler_params=pltpu.CompilerParams(
            vmem_limit_bytes=grant or min(held + 6 * MIB, 60 * MIB)
        ),
        name=name,
    )(*args)


def dot(a, b):
    return jnp.dot(a, b, preferred_element_type=jnp.float32)


def half(which, width):
    return pl.ds(pl.multiple_of(which * width, width), width)


def pick_kernel(per_source, place, ids_ref, within_ref, expert_ref, tokens_ref, out_ref, row_ref):
    me = place[0]
    count, slots = ids_ref.shape
    tok_rows = tokens_ref.shape[0]
    local = (ids_ref[...] - me * tok_rows).astype(jnp.float32)
    spread = lax.broadcasted_iota(jnp.int32, (slots, slots), 0) == me * per_source + within_ref[...]
    mine = jnp.dot(
        local, spread.astype(jnp.float32),
        precision=lax.Precision.HIGHEST, preferred_element_type=jnp.float32,
    )
    ours = lax.broadcasted_iota(jnp.int32, (count, slots), 0) == (expert_ref[...] ^ me)
    row = jnp.sum(jnp.where(ours, mine, 0.0), axis=0, keepdims=True).astype(jnp.int32)
    row_ref[...] = row
    selector = lax.broadcasted_iota(jnp.int32, (tok_rows, slots), 0) == row
    out_ref[...] = lax.dot_general(
        selector.astype(jnp.float32).astype(jnp.bfloat16), tokens_ref[...],
        (((0,), (0,)), ((), ())), preferred_element_type=jnp.float32,
    ).astype(jnp.bfloat16)


def first_kernel(place, own_ref, gate_w, up_w, gate_ref, up_ref):
    mine = half(place[1], own_ref.shape[1])
    gate_ref[...] = dot(own_ref[...], gate_w[0, mine, :])
    up_ref[...] = dot(own_ref[...], up_w[0, mine, :])


def scaled(score_ref, value):
    rows, width = value.shape
    column = jnp.transpose(jnp.broadcast_to(score_ref[...], (128, rows)))
    pieces = [value[:, c : c + 128] * column for c in range(0, width, 128)]
    return jnp.concatenate(pieces, axis=1)


def second_kernel(
    place, other_ref, gate_ref, up_ref, gate_w, up_w, down_w, score_ref, hidden_ref, send_ref
):
    theirs = half(1 - place[1], other_ref.shape[1])
    units = gate_ref.shape[1]
    tile = 256 if units % 256 == 0 else units
    for start in range(0, units, tile):
        c = pl.ds(start, tile)
        gate_pre = gate_ref[:, c] + dot(other_ref[...], gate_w[0, theirs, c])
        up_pre = up_ref[:, c] + dot(other_ref[...], up_w[0, theirs, c])
        hidden_ref[:, c] = (gate_pre / (1.0 + jnp.exp(-gate_pre)) * up_pre).astype(jnp.bfloat16)
    send_ref[...] = scaled(score_ref, dot(hidden_ref[...], down_w[0, :, theirs])).astype(jnp.bfloat16)


def third_kernel(place, hidden_ref, down_w, score_ref, keep_ref):
    mine = half(place[1], keep_ref.shape[1])
    keep_ref[...] = scaled(score_ref, dot(hidden_ref[...], down_w[0, :, mine]))


def mix_kernel(row_ref, returned_ref, out_ref):
    shape = (out_ref.shape[0], row_ref.shape[1])
    selector = lax.broadcasted_iota(jnp.int32, shape, 0) == row_ref[...]
    out_ref[...] = dot(
        selector.astype(jnp.float32).astype(jnp.bfloat16), returned_ref[...]
    ).astype(out_ref.dtype)


def gather_round(value, stride, radix, count):
    parts = [value]
    for k in range(1, radix):
        parts.append(lax.ppermute(value, "ep", [(e, e ^ (k * stride)) for e in range(count)]))
    return parts


def on_device(tokens, chosen, gate_score, gate_weight, up_weight, down_weight):
    ep_count = lax.axis_size("ep")
    tok_rows, width = tokens.shape
    slots = chosen.shape[1]
    per_source = slots // ep_count
    rows = ep_count * per_source
    units = gate_weight.shape[2]
    me = lax.axis_index("ep").astype(jnp.int32)
    place = jnp.stack([me, lax.axis_index("tp").astype(jnp.int32)])
    swap = [(0, 1), (1, 0)]

    ids, stride = chosen, 1
    while stride < ep_count:
        radix = 4 if ep_count % (4 * stride) == 0 else 2
        ids = jnp.concatenate(gather_round(ids, stride, radix, ep_count), axis=0)
        stride *= radix

    order = jnp.arange(slots, dtype=jnp.int32)[None, :]
    outgoing, row = call(
        lambda *refs: pick_kernel(per_source, *refs), "pick", [SMEM] + [VMEM] * 4,
        (
            jax.ShapeDtypeStruct((rows, width), tokens.dtype),
            jax.ShapeDtypeStruct((1, slots), jnp.int32),
        ),
        200 * rows * tok_rows * width,
        (place, ids, order % per_source, order // per_source, tokens),
        (), 0 if rows < 1024 else 48 * MIB,
    )
    arrived = lax.all_to_all(
        outgoing.reshape(ep_count, per_source, width), "ep", split_axis=0, concat_axis=0, tiled=True
    ).reshape(rows, width)
    other = lax.ppermute(arrived, "tp", swap)
    pre = jax.ShapeDtypeStruct((rows, units), jnp.float32)
    product = 2 * rows * width * units
    gate_pre, up_pre = call(
        first_kernel, "ffn_first", [SMEM] + [VMEM] * 3, (pre, pre), 2 * product,
        (place, arrived, gate_weight, up_weight),
    )
    hidden, sent = call(
        second_kernel, "ffn_second", [SMEM] + [VMEM] * 7,
        (
            jax.ShapeDtypeStruct((rows, units), jnp.bfloat16),
            jax.ShapeDtypeStruct((rows, width), jnp.bfloat16),
        ),
        3 * product,
        (place, other, gate_pre, up_pre, gate_weight, up_weight, down_weight, gate_score),
    )
    got = lax.ppermute(sent, "tp", swap)
    (kept,) = call(
        third_kernel, "ffn_third", [SMEM] + [VMEM] * 3,
        (jax.ShapeDtypeStruct((rows, width), jnp.float32),), product,
        (place, hidden, down_weight, gate_score),
    )
    weighted = (kept + got.astype(jnp.float32)).astype(jnp.bfloat16)
    returned = lax.all_to_all(
        weighted.reshape(ep_count, per_source, width), "ep", split_axis=0, concat_axis=0, tiled=True
    ).reshape(rows, width)
    (mixed_out,) = call(
        mix_kernel, "mix", [VMEM] * 2, (jax.ShapeDtypeStruct((tok_rows, width), jnp.bfloat16),),
        2 * rows * tok_rows * width, (row, returned),
    )
    return mixed_out


def solution(mesh):
    in_specs = (
        P("ep", "tp"),
        P("ep", None),
        P("ep", None),
        P("ep", None, "tp"),
        P("ep", None, "tp"),
        P("ep", "tp", None),
    )
    out_specs = P("ep", "tp")
    return jax.shard_map(
        on_device, mesh=mesh, in_specs=in_specs, out_specs=out_specs, check_vma=False
    )
```

time: 84.3 us -> 77.6 us (0.921)
  matrix products: 14.1 us -> 0 us
  Pallas kernels: 0 us -> 9.91 us
  waiting for transfers between devices: 11.2 us -> 7.76 us
  starting transfers between devices: 8.55 us -> 9.49 us
    dot_general x4 -> x0, matrix products: 14.1 us -> none  [the longest x1 7.44 us: on_device(): jnp.dot(hidden, w_down, preferred_element_type=jnp.float32)]
    pallas_call x0 -> x5, Pallas kernels: none -> 9.91 us  [call(): pl.pallas_call(body, out_shape=outs, in_specs=in_specs, out_specs=tuple((...]
    ppermute x0 -> x6, starting transfers between devices: none -> 8.94 us  [gather_round(): lax.ppermute(value, 'ep', [(e, e ^ k * stride) for e in range(count)])]
    all_to_all x1 -> x0, starting transfers between devices: 8.34 us -> none  [on_device(): lax.all_to_all(chosen.reshape(ep_count, per_source), 'ep', split_axis=0,...]
    ppermute x0 -> x6, waiting for transfers between devices: none -> 7.38 us  [gather_round(): lax.ppermute(value, 'ep', [(e, e ^ k * stride) for e in range(count)])]
    all_to_all x1 -> x0, waiting for transfers between devices: 7.22 us -> none  [on_device(): lax.all_to_all(chosen.reshape(ep_count, per_source), 'ep', split_axis=0,...]
    ppermute x1, waiting for transfers between devices: 2.28 us -> 0.01 us  [on_device(): other = lax.ppermute(arrived, 'tp', swap)]
    ppermute x1, waiting for transfers between devices: 1.74 us -> 0.38 us  [on_device(): got = lax.ppermute(sent, 'tp', swap)]
  transfers between devices with their start and end apart: 3 -> 8, of which waited for: 3 -> 6; matrix products, arithmetic and copies ran while one was open for 0% -> 0% of each run, Pallas kernels for 0% -> 5%
where the time goes in v3:
time: 77.6 us; the launch traced here: 77.3 us
  blocking collectives  47.3 us (61%)
  Pallas kernels  9.91 us (13%)
  starting transfers between devices  9.49 us (12%)
  waiting for transfers between devices  7.76 us (10%)
  local copies, waits for them, and re-layouts  1.73 us (2%)
  other arithmetic  1.04 us (1%)
    all_to_all x1, blocking collectives, on_device(): lax.all_to_all(weighted.reshape(ep_count, per_source, width), 'ep', split...  25 us
    all_to_all x1, blocking collectives, on_device(): lax.all_to_all(outgoing.reshape(ep_count, per_source, width), 'ep', split...  22.3 us
    pallas_call x5, Pallas kernels, call(): pl.pallas_call(body, out_shape=outs, in_specs=in_specs, out_specs=tuple((...  9.91 us
    ppermute x6, starting transfers between devices, gather_round(): lax.ppermute(value, 'ep', [(e, e ^ k * stride) for e in range(count)])  8.94 us
    ppermute x6, waiting for transfers between devices, gather_round(): lax.ppermute(value, 'ep', [(e, e ^ k * stride) for e in range(count)])  7.38 us
  transfers between devices with their start and end apart: 8, of which 6 were waited for; matrix products, arithmetic and copies ran while one was open for 0% of the time, Pallas kernels for 5%

profile of v3, /device:TPU:0, one launch (start us, length us, event | category | flops | bytes accessed | tf_op | source)
XLA Modules:
  0.0 77.3 jit_solution(3428760575767408536)
XLA Ops:
  0.0 3.9 %collective-permute-start.2 = (s32[1,384]{1,0:T(1,128)}, s32[1,384]{1,0:T(1,128)S(1)}, u32[]{:S(2)}, u32[]{:S(2)}) collective-permute-start(s32[1,384]{1,0:T(1,128)} %param.7), channel_id=1, source_target_pairs={{0,6},{2,4},{4,2},{6,0},{8,14},{10,12},{12,10},{14,8},{16,22},{18,... | collective-permute-start | bytes 4616 | tf_op jit(solution)/shard_map/ppermute | solution.py:106
  3.9 0.5 collective-permute-start.1
  4.4 0.1 collective-permute-start
  4.5 1.2 %collective-permute-done.2 = s32[1,384]{1,0:T(1,128)S(1)} collective-permute-done((s32[1,384]{1,0:T(1,128)}, s32[1,384]{1,0:T(1,128)S(1)}, u32[]{:S(2)}, u32[]{:S(2)}) %collective-permute-start.2) | collective-permute-done | bytes 1568 | tf_op jit(solution)/shard_map/ppermute | solution.py:106
  5.7 2.0 %collective-permute-done.1 = s32[1,384]{1,0:T(1,128)S(1)} collective-permute-done((s32[1,384]{1,0:T(1,128)}, s32[1,384]{1,0:T(1,128)S(1)}, u32[]{:S(2)}, u32[]{:S(2)}) %collective-permute-start.1) | collective-permute-done | bytes 1568 | tf_op jit(solution)/shard_map/ppermute | solution.py:106
  7.7 0.5 collective-permute-done
  8.2 0.7 pad_add_fusion
  8.9 3.7 %collective-permute-start.5 = (s32[4,384]{1,0:T(4,128)S(1)}, s32[4,384]{1,0:T(4,128)S(1)}, u32[]{:S(2)}, u32[]{:S(2)}) collective-permute-start(s32[4,384]{1,0:T(4,128)S(1)} %pad_add_fusion), channel_id=1, source_target_pairs={{0,24},{2,26},{4,28},{6,30},{8,16},{10,18},{12,20},{14,22},{16,8},... | collective-permute-start | bytes 18440 | tf_op jit(solution)/shard_map/ppermute | solution.py:106
  12.6 0.0 collective-permute-start.4
  12.6 0.8 %collective-permute-start.3 = (s32[4,384]{1,0:T(4,128)S(1)}, s32[4,384]{1,0:T(4,128)S(1)}, u32[]{:S(2)}, u32[]{:S(2)}) collective-permute-start(s32[4,384]{1,0:T(4,128)S(1)} %pad_add_fusion), channel_id=1, source_target_pairs={{0,8},{2,10},{4,12},{6,14},{8,0},{10,2},{12,4},{14,6},{16,24},{18,... | collective-permute-start | bytes 18440 | tf_op jit(solution)/shard_map/ppermute | solution.py:106
  13.4 0.1 pad_add_fusion.1.refs_0_.place
  13.4 1.0 %collective-permute-done.5 = s32[4,384]{1,0:T(4,128)S(1)} collective-permute-done((s32[4,384]{1,0:T(4,128)S(1)}, s32[4,384]{1,0:T(4,128)S(1)}, u32[]{:S(2)}, u32[]{:S(2)}) %collective-permute-start.5) | collective-permute-done | bytes 6176 | tf_op jit(solution)/shard_map/ppermute | solution.py:106
  14.4 2.7 %collective-permute-done.4 = s32[4,384]{1,0:T(4,128)S(1)} collective-permute-done((s32[4,384]{1,0:T(4,128)S(1)}, s32[4,384]{1,0:T(4,128)S(1)}, u32[]{:S(2)}, u32[]{:S(2)}) %collective-permute-start.4) | collective-permute-done | bytes 6176 | tf_op jit(solution)/shard_map/ppermute | solution.py:106
  17.1 0.0 collective-permute-done.3
  17.1 0.7 concatenate.8.refs_1_
  17.8 0.0 copy-start.4
  17.8 1.0 %copy-done.4 = bf16[192,1024]{1,0:T(8,128)(2,1)S(1)} copy-done((bf16[192,1024]{1,0:T(8,128)(2,1)S(1)}, bf16[192,1024]{1,0:T(8,128)(2,1)}, u32[]{:S(2)}) %copy-start.4) | copy-done | bytes 393240
  18.8 0.0 copy-start.1
  18.8 0.0 copy-start.2
  18.8 1.5 %pick.1 = (bf16[384,1024]{1,0:T(8,128)(2,1)S(1)}, s32[1,384]{1,0:T(1,128)S(1)}) custom-call(s32[2]{0:T(128)S(1)} %pad_add_fusion.1.refs_0_.place, s32[16,384]{1,0:T(8,128)S(1)} %concatenate.8.refs_1_, s32[1,384]{1,0:T(1,128)S(1)} %get-tuple-element.18.refs_2_, s32[1,384]{1,0:T(1,128)S(1)} %get-tuple-element.17.refs_3_, bf16[192,1024]{1,0:T(8,128)(2,1)S(1)} %copy-done.4), custom_call_target="tpu_custom_call" | custom-call | flops 15099494400 | bytes 1208832 | tf_op jit(solution)/shard_map/pick/pallas_call | solution.py:21
  20.3 22.3 %all_to_all.10 = bf16[16,24,1024]{2,1,0:T(8,128)(2,1)S(1)} all-to-all(bf16[16,24,1024]{2,1,0:T(8,128)(2,1)S(1)} %bitcast.9), channel_id=1, replica_groups=mesh['ep'=16,'tp'=2] {'ep'}, dimensions={0} | all-to-all | bytes 1572864 | tf_op jit(solution)/shard_map/all_to_all | solution.py:138
  42.6 0.0 copy-start.3
  42.6 0.0 collective-permute-start.6
  42.6 0.0 copy-done.1
  42.6 0.0 copy-done.2
  42.6 0.0 copy-start
  42.6 2.4 %ffn_first.1 = (f32[384,1024]{1,0:T(8,128)S(1)}, f32[384,1024]{1,0:T(8,128)S(1)}) custom-call(s32[2]{0:T(128)S(1)} %pad_add_fusion.1.refs_0_.place, bf16[384,1024]{1,0:T(8,128)(2,1)S(1)} %bitcast.7, bf16[1,2048,1024]{2,1,0:T(8,128)(2,1)S(1)} %copy-done.1, bf16[1,2048,1024]{2,1,0:T(8,128)(2,1)S(1)} %copy-done.2), custom_call_target="tpu_custom_call" | custom-call | flops 1610612736 | bytes 12320768 | tf_op jit(solution)/shard_map/ffn_first/pallas_call | solution.py:21
  45.0 0.0 collective-permute-done.6.other_ref
  45.0 0.0 copy-done.3
  45.0 0.0 copy-done
  45.0 3.5 %ffn_second.1 = (bf16[384,1024]{1,0:T(8,128)(2,1)S(1)}, bf16[384,1024]{1,0:T(8,128)(2,1)S(1)}) custom-call(s32[2]{0:T(128)S(1)} %pad_add_fusion.1.refs_0_.place, bf16[384,1024]{1,0:T(8,128)(2,1)S(1)} %collective-permute-done.6.other_ref, f32[384,1024]{1,0:T(8,128)S(1)} %get-tuple-element.13.gate_ref, f32[384,1024]{1,0:T(8,128)S(1)} %get-tuple-element.14.up_ref, ...), custom_call_target="tpu_custom_call" | custom-call | flops 2415919104 | bytes 18089472 | tf_op jit(solution)/shard_map/ffn_second/pallas_call | solution.py:21
  48.5 0.6 collective-permute-start.7
  49.0 1.5 %ffn_third.1 = f32[384,1024]{1,0:T(8,128)S(1)} custom-call(s32[2]{0:T(128)S(1)} %pad_add_fusion.1.refs_0_.place, bf16[384,1024]{1,0:T(8,128)(2,1)S(1)} %get-tuple-element.15.hidden_ref, bf16[1,1024,2048]{2,1,0:T(8,128)(2,1)S(1)} %copy-done, f32[1,384]{1,0:T(1,128)S(1)} %copy-done.3), custom_call_target="tpu_custom_call" | custom-call | flops 805306368 | bytes 6555136 | tf_op jit(solution)/shard_map/ffn_third/pallas_call | solution.py:21
  50.6 0.4 collective-permute-done.7
  50.9 0.3 add_convert_fusion
  51.2 25.0 %all_to_all.11 = bf16[16,24,1024]{2,1,0:T(8,128)(2,1)S(1)} all-to-all(bf16[16,24,1024]{2,1,0:T(8,128)(2,1)S(1)} %bitcast.10), channel_id=1, replica_groups=mesh['ep'=16,'tp'=2] {'ep'}, dimensions={0} | all-to-all | bytes 1572864 | tf_op jit(solution)/shard_map/all_to_all | solution.py:164
  76.2 1.1 %mix.1 = bf16[192,1024]{1,0:T(8,128)(2,1)} custom-call(s32[1,384]{1,0:T(1,128)S(1)} %get-tuple-element.11.row_ref, bf16[384,1024]{1,0:T(8,128)(2,1)S(1)} %bitcast.8), custom_call_target="tpu_custom_call" | custom-call | flops 150994944 | bytes 1181184 | tf_op jit(solution)/shard_map/mix/pallas_call | solution.py:21
  (1 shorter events, 0.0 us)
Async XLA Ops:
  0.0 5.7 %collective-permute-start.2 = (s32[1,384]{1,0:T(1,128)}, s32[1,384]{1,0:T(1,128)S(1)}, u32[]{:S(2)}, u32[]{:S(2)}) collective-permute-start(s32[1,384]{1,0:T(1,128)} %param.7), channel_id=1, source_target_pairs={{0,6},{2,4},{4,2},{6,0},{8,14},{10,12},{12,10},{14,8},{16,22},{18,... | collective-permute-start | bytes 4616 | tf_op jit(solution)/shard_map/ppermute | solution.py:106
  3.9 3.8 %collective-permute-start.1 = (s32[1,384]{1,0:T(1,128)}, s32[1,384]{1,0:T(1,128)S(1)}, u32[]{:S(2)}, u32[]{:S(2)}) collective-permute-start(s32[1,384]{1,0:T(1,128)} %param.7), channel_id=1, source_target_pairs={{0,4},{2,6},{4,0},{6,2},{8,12},{10,14},{12,8},{14,10},{16,20},{18,... | collective-permute-start | bytes 4616 | tf_op jit(solution)/shard_map/ppermute | solution.py:106
  4.4 3.8 %collective-permute-start = (s32[1,384]{1,0:T(1,128)}, s32[1,384]{1,0:T(1,128)S(1)}, u32[]{:S(2)}, u32[]{:S(2)}) collective-permute-start(s32[1,384]{1,0:T(1,128)} %param.7), channel_id=1, source_target_pairs={{0,2},{2,0},{4,6},{6,4},{8,10},{10,8},{12,14},{14,12},{16,18},{18,... | collective-permute-start | bytes 4616 | tf_op jit(solution)/shard_map/ppermute | solution.py:106
  8.9 5.5 %collective-permute-start.5 = (s32[4,384]{1,0:T(4,128)S(1)}, s32[4,384]{1,0:T(4,128)S(1)}, u32[]{:S(2)}, u32[]{:S(2)}) collective-permute-start(s32[4,384]{1,0:T(4,128)S(1)} %pad_add_fusion), channel_id=1, source_target_pairs={{0,24},{2,26},{4,28},{6,30},{8,16},{10,18},{12,20},{14,22},{16,8},... | collective-permute-start | bytes 18440 | tf_op jit(solution)/shard_map/ppermute | solution.py:106
  12.6 4.5 %collective-permute-start.4 = (s32[4,384]{1,0:T(4,128)S(1)}, s32[4,384]{1,0:T(4,128)S(1)}, u32[]{:S(2)}, u32[]{:S(2)}) collective-permute-start(s32[4,384]{1,0:T(4,128)S(1)} %pad_add_fusion), channel_id=1, source_target_pairs={{0,16},{2,18},{4,20},{6,22},{8,24},{10,26},{12,28},{14,30},{16,0},... | collective-permute-start | bytes 18440 | tf_op jit(solution)/shard_map/ppermute | solution.py:106
  12.6 4.5 %collective-permute-start.3 = (s32[4,384]{1,0:T(4,128)S(1)}, s32[4,384]{1,0:T(4,128)S(1)}, u32[]{:S(2)}, u32[]{:S(2)}) collective-permute-start(s32[4,384]{1,0:T(4,128)S(1)} %pad_add_fusion), channel_id=1, source_target_pairs={{0,8},{2,10},{4,12},{6,14},{8,0},{10,2},{12,4},{14,6},{16,24},{18,... | collective-permute-start | bytes 18440 | tf_op jit(solution)/shard_map/ppermute | solution.py:106
  17.8 1.0 %copy-start.4 = (bf16[192,1024]{1,0:T(8,128)(2,1)S(1)}, bf16[192,1024]{1,0:T(8,128)(2,1)}, u32[]{:S(2)}) copy-start(bf16[192,1024]{1,0:T(8,128)(2,1)} %refs_4_.1) | copy-start | bytes 1179652
  18.8 23.8 %copy-start.1 = (bf16[1,2048,1024]{2,1,0:T(8,128)(2,1)S(1)}, bf16[1,2048,1024]{2,1,0:T(8,128)(2,1)}, u32[]{:S(2)}) copy-start(bf16[1,2048,1024]{2,1,0:T(8,128)(2,1)} %gate_w.3) | copy-start | bytes 12582916
  18.8 23.8 %copy-start.2 = (bf16[1,2048,1024]{2,1,0:T(8,128)(2,1)S(1)}, bf16[1,2048,1024]{2,1,0:T(8,128)(2,1)}, u32[]{:S(2)}) copy-start(bf16[1,2048,1024]{2,1,0:T(8,128)(2,1)} %up_w.3) | copy-start | bytes 12582916
  42.6 2.4 %copy-start.3 = (f32[1,384]{1,0:T(1,128)S(1)}, f32[1,384]{1,0:T(1,128)}, u32[]{:S(2)}) copy-start(f32[1,384]{1,0:T(1,128)} %score_ref.3) | copy-start | bytes 4612
  42.6 2.4 %collective-permute-start.6 = (bf16[384,1024]{1,0:T(8,128)(2,1)S(1)}, bf16[384,1024]{1,0:T(8,128)(2,1)S(1)}, u32[]{:S(2)}, u32[]{:S(2)}) collective-permute-start(bf16[384,1024]{1,0:T(8,128)(2,1)S(1)} %bitcast.6), channel_id=1, source_target_pairs={{0,1},{1,0},{2,3},{3,2},{4,5},{5,4},{6,7},{7,6},{8,9},{9,8},{10,11... | collective-permute-start | bytes 2359304 | tf_op jit(solution)/shard_map/ppermute | solution.py:141
  42.6 2.4 %copy-start = (bf16[1,1024,2048]{2,1,0:T(8,128)(2,1)S(1)}, bf16[1,1024,2048]{2,1,0:T(8,128)(2,1)}, u32[]{:S(2)}) copy-start(bf16[1,1024,2048]{2,1,0:T(8,128)(2,1)} %down_w.3) | copy-start | bytes 12582916
  48.5 2.5 %collective-permute-start.7 = (bf16[384,1024]{1,0:T(8,128)(2,1)S(1)}, bf16[384,1024]{1,0:T(8,128)(2,1)S(1)}, u32[]{:S(2)}, u32[]{:S(2)}) collective-permute-start(bf16[384,1024]{1,0:T(8,128)(2,1)S(1)} %get-tuple-element.16), channel_id=1, source_target_pairs={{0,1},{1,0},{2,3},{3,2},{4,5},{5,4},{6,7},{7,6},{8,9},{9,8},{10,11... | collective-permute-start | bytes 2359304 | tf_op jit(solution)/shard_map/ppermute | solution.py:157

commit v4 on v3

--- a/solution.py
+++ b/solution.py
@@ -40,16 +40,26 @@
     return pl.ds(pl.multiple_of(which * width, width), width)
 
 
-def pick_kernel(per_source, place, ids_ref, within_ref, expert_ref, tokens_ref, out_ref, row_ref):
+def prep_kernel(per_source, place, within_ref, spread_ref):
+    slots = within_ref.shape[1]
+    column = lax.broadcasted_iota(jnp.int32, (slots, slots), 0)
+    hit = column == place[0] * per_source + within_ref[...]
+    spread_ref[...] = hit.astype(jnp.float32).astype(jnp.bfloat16)
+
+
+def pick_kernel(place, expert_ref, spread_ref, tokens_ref, *refs):
+    parts, (out_ref, row_ref, ids_ref) = refs[:-3], refs[-3:]
     me = place[0]
-    count, slots = ids_ref.shape
-    tok_rows = tokens_ref.shape[0]
-    local = (ids_ref[...] - me * tok_rows).astype(jnp.float32)
-    spread = lax.broadcasted_iota(jnp.int32, (slots, slots), 0) == me * per_source + within_ref[...]
-    mine = jnp.dot(
-        local, spread.astype(jnp.float32),
-        precision=lax.Precision.HIGHEST, preferred_element_type=jnp.float32,
-    )
+    tok_rows, slots = tokens_ref.shape[0], spread_ref.shape[0]
+    step = parts[0].shape[0]
+    count = step * len(parts)
+    for j, part in enumerate(parts):
+        ids_ref[pl.ds(j * step, step), :] = part[...]
+    local = ids_ref[...] - me * tok_rows
+    low, high = local & 127, local >> 7
+    both = jnp.concatenate([high, low], axis=0).astype(jnp.float32).astype(jnp.bfloat16)
+    mine = dot(both, spread_ref[...])
+    mine = mine[:count] * 128.0 + mine[count:]
     ours = lax.broadcasted_iota(jnp.int32, (count, slots), 0) == (expert_ref[...] ^ me)
     row = jnp.sum(jnp.where(ours, mine, 0.0), axis=0, keepdims=True).astype(jnp.int32)
     row_ref[...] = row
@@ -66,30 +76,25 @@
     up_ref[...] = dot(own_ref[...], up_w[0, mine, :])
 
 
-def scaled(score_ref, value):
-    rows, width = value.shape
-    column = jnp.transpose(jnp.broadcast_to(score_ref[...], (128, rows)))
-    pieces = [value[:, c : c + 128] * column for c in range(0, width, 128)]
-    return jnp.concatenate(pieces, axis=1)
-
-
 def second_kernel(
     place, other_ref, gate_ref, up_ref, gate_w, up_w, down_w, score_ref, hidden_ref, send_ref
 ):
     theirs = half(1 - place[1], other_ref.shape[1])
-    units = gate_ref.shape[1]
+    rows, units = gate_ref.shape
     tile = 256 if units % 256 == 0 else units
+    score = jnp.transpose(jnp.broadcast_to(score_ref[...], (128, rows)))
+    score = jnp.concatenate([score] * (tile // 128), axis=1)
     for start in range(0, units, tile):
         c = pl.ds(start, tile)
         gate_pre = gate_ref[:, c] + dot(other_ref[...], gate_w[0, theirs, c])
         up_pre = up_ref[:, c] + dot(other_ref[...], up_w[0, theirs, c])
-        hidden_ref[:, c] = (gate_pre / (1.0 + jnp.exp(-gate_pre)) * up_pre).astype(jnp.bfloat16)
-    send_ref[...] = scaled(score_ref, dot(hidden_ref[...], down_w[0, :, theirs])).astype(jnp.bfloat16)
+        hidden = gate_pre / (1.0 + jnp.exp(-gate_pre)) * (up_pre * score)
+        hidden_ref[:, c] = hidden.astype(jnp.bfloat16)
+    send_ref[...] = dot(hidden_ref[...], down_w[0, :, theirs]).astype(jnp.bfloat16)
 
 
-def third_kernel(place, hidden_ref, down_w, score_ref, keep_ref):
-    mine = half(place[1], keep_ref.shape[1])
-    keep_ref[...] = scaled(score_ref, dot(hidden_ref[...], down_w[0, :, mine]))
+def third_kernel(place, hidden_ref, down_w, keep_ref):
+    keep_ref[...] = dot(hidden_ref[...], down_w[0, :, half(place[1], keep_ref.shape[1])])
 
 
 def mix_kernel(row_ref, returned_ref, out_ref):
@@ -118,22 +123,29 @@
     place = jnp.stack([me, lax.axis_index("tp").astype(jnp.int32)])
     swap = [(0, 1), (1, 0)]
 
-    ids, stride = chosen, 1
+    order = jnp.arange(slots, dtype=jnp.int32)[None, :]
+    (spread,) = call(
+        lambda *refs: prep_kernel(per_source, *refs), "prep", [SMEM, VMEM],
+        (jax.ShapeDtypeStruct((slots, slots), jnp.bfloat16),), 10**10, (place, order % per_source),
+    )
+    parts, stride = [chosen], 1
     while stride < ep_count:
+        ids = jnp.concatenate(parts, axis=0)
         radix = 4 if ep_count % (4 * stride) == 0 else 2
-        ids = jnp.concatenate(gather_round(ids, stride, radix, ep_count), axis=0)
+        parts = gather_round(ids, stride, radix, ep_count)
+        if stride == 1:
+            parts, spread = lax.optimization_barrier((parts, spread))
         stride *= radix
 
-    order = jnp.arange(slots, dtype=jnp.int32)[None, :]
     outgoing, row = call(
-        lambda *refs: pick_kernel(per_source, *refs), "pick", [SMEM] + [VMEM] * 4,
+        pick_kernel, "pick", [SMEM] + [VMEM] * (3 + len(parts)),
         (
             jax.ShapeDtypeStruct((rows, width), tokens.dtype),
             jax.ShapeDtypeStruct((1, slots), jnp.int32),
         ),
         200 * rows * tok_rows * width,
-        (place, ids, order % per_source, order // per_source, tokens),
-        (), 0 if rows < 1024 else 48 * MIB,
+        (place, order // per_source, spread, tokens, *parts),
+        [pltpu.VMEM((ep_count, slots), jnp.int32)],
     )
     arrived = lax.all_to_all(
         outgoing.reshape(ep_count, per_source, width), "ep", split_axis=0, concat_axis=0, tiled=True
@@ -156,9 +168,9 @@
     )
     got = lax.ppermute(sent, "tp", swap)
     (kept,) = call(
-        third_kernel, "ffn_third", [SMEM] + [VMEM] * 3,
+        third_kernel, "ffn_third", [SMEM] + [VMEM] * 2,
         (jax.ShapeDtypeStruct((rows, width), jnp.float32),), product,
-        (place, hidden, down_weight, gate_score),
+        (place, hidden, down_weight),
     )
     weighted = (kept + got.astype(jnp.float32)).astype(jnp.bfloat16)
     returned = lax.all_to_all(

time: 77.6 us -> 75.1 us (0.968)
  local copies, waits for them, and re-layouts: 1.73 us -> 0.03 us
    unnamed x10 -> x12, local copies, waits for them, and re-layouts: 1.01 us -> 0.03 us
    pallas_call x5 -> x6, Pallas kernels: 9.91 us -> 10.2 us  [call(): pl.pallas_call(body, out_shape=outs, in_specs=in_specs, out_specs=tuple((...]
  transfers between devices with their start and end apart: 8 -> 8, of which waited for: 6 -> 5; matrix products, arithmetic and copies ran while one was open for 0% -> 0% of each run, Pallas kernels for 5% -> 6%
where the time goes in v4:
time: 75.1 us; the launch traced here: 74.9 us
  blocking collectives  46.6 us (62%)
  Pallas kernels  10.2 us (14%)
  starting transfers between devices  9.48 us (13%)
  waiting for transfers between devices  8.08 us (11%)
    all_to_all x1, blocking collectives, on_device(): lax.all_to_all(weighted.reshape(ep_count, per_source, width), 'ep', split...  25 us
    all_to_all x1, blocking collectives, on_device(): lax.all_to_all(outgoing.reshape(ep_count, per_source, width), 'ep', split...  21.6 us
    pallas_call x6, Pallas kernels, call(): pl.pallas_call(body, out_shape=outs, in_specs=in_specs, out_specs=tuple((...  10.2 us
    ppermute x6, starting transfers between devices, gather_round(): lax.ppermute(value, 'ep', [(e, e ^ k * stride) for e in range(count)])  8.94 us
    ppermute x6, waiting for transfers between devices, gather_round(): lax.ppermute(value, 'ep', [(e, e ^ k * stride) for e in range(count)])  7.7 us
  transfers between devices with their start and end apart: 8, of which 5 were waited for; matrix products, arithmetic and copies ran while one was open for 0% of the time, Pallas kernels for 6%

profile of v4, /device:TPU:0, one launch (start us, length us, event | category | flops | bytes accessed | tf_op | source)
XLA Modules:
  0.0 74.9 jit_solution(8020314934655213374)
XLA Ops:
  0.0 3.0 %collective-permute-start.1 = (s32[1,384]{1,0:T(1,128)}, s32[1,384]{1,0:T(1,128)S(1)}, u32[]{:S(2)}, u32[]{:S(2)}) collective-permute-start(s32[1,384]{1,0:T(1,128)} %param.7), channel_id=1, source_target_pairs={{0,4},{2,6},{4,0},{6,2},{8,12},{10,14},{12,8},{14,10},{16,20},{18,... | collective-permute-start | bytes 4616 | tf_op jit(solution)/shard_map/ppermute | solution.py:111
  3.0 1.5 %collective-permute-start = (s32[1,384]{1,0:T(1,128)}, s32[1,384]{1,0:T(1,128)S(1)}, u32[]{:S(2)}, u32[]{:S(2)}) collective-permute-start(s32[1,384]{1,0:T(1,128)} %param.7), channel_id=1, source_target_pairs={{0,2},{2,0},{4,6},{6,4},{8,10},{10,8},{12,14},{14,12},{16,18},{18,... | collective-permute-start | bytes 4616 | tf_op jit(solution)/shard_map/ppermute | solution.py:111
  4.5 0.0 collective-permute-start.2
  4.5 0.1 pad_add_fusion.1.refs_0_.place
  4.6 0.0 copy-start.5
  4.6 0.0 copy-start.4
  4.6 0.6 prep.1.spread_ref
  5.2 0.0 collective-permute-done.1
  5.2 1.6 %collective-permute-done = s32[1,384]{1,0:T(1,128)S(1)} collective-permute-done((s32[1,384]{1,0:T(1,128)}, s32[1,384]{1,0:T(1,128)S(1)}, u32[]{:S(2)}, u32[]{:S(2)}) %collective-permute-start) | collective-permute-done | bytes 1568 | tf_op jit(solution)/shard_map/ppermute | solution.py:111
  6.8 2.4 %collective-permute-done.2 = s32[1,384]{1,0:T(1,128)S(1)} collective-permute-done((s32[1,384]{1,0:T(1,128)}, s32[1,384]{1,0:T(1,128)S(1)}, u32[]{:S(2)}, u32[]{:S(2)}) %collective-permute-start.2) | collective-permute-done | bytes 1568 | tf_op jit(solution)/shard_map/ppermute | solution.py:111
  9.2 0.0 copy-done.5
  9.2 3.7 %collective-permute-start.5 = (s32[4,384]{1,0:T(4,128)S(1)}, s32[4,384]{1,0:T(4,128)S(1)}, u32[]{:S(2)}, u32[]{:S(2)}) collective-permute-start(s32[4,384]{1,0:T(4,128)S(1)} %pad_add_fusion.refs_0_), channel_id=1, source_target_pairs={{0,24},{2,26},{4,28},{6,30},{8,16},{10,18},{12,20},{14,22},{16,8},... | collective-permute-start | bytes 18440 | tf_op jit(solution)/shard_map/ppermute | solution.py:111
  12.9 0.0 collective-permute-start.4
  12.9 0.8 %collective-permute-start.3 = (s32[4,384]{1,0:T(4,128)S(1)}, s32[4,384]{1,0:T(4,128)S(1)}, u32[]{:S(2)}, u32[]{:S(2)}) collective-permute-start(s32[4,384]{1,0:T(4,128)S(1)} %pad_add_fusion.refs_0_), channel_id=1, source_target_pairs={{0,8},{2,10},{4,12},{6,14},{8,0},{10,2},{12,4},{14,6},{16,24},{18,... | collective-permute-start | bytes 18440 | tf_op jit(solution)/shard_map/ppermute | solution.py:111
  13.7 1.0 %collective-permute-done.5.refs_3_ = s32[4,384]{1,0:T(4,128)S(1)} collective-permute-done((s32[4,384]{1,0:T(4,128)S(1)}, s32[4,384]{1,0:T(4,128)S(1)}, u32[]{:S(2)}, u32[]{:S(2)}) %collective-permute-start.5) | collective-permute-done | bytes 6176 | tf_op jit(solution)/shard_map/ppermute | solution.py:111
  14.7 2.7 %collective-permute-done.4.refs_2_ = s32[4,384]{1,0:T(4,128)S(1)} collective-permute-done((s32[4,384]{1,0:T(4,128)S(1)}, s32[4,384]{1,0:T(4,128)S(1)}, u32[]{:S(2)}, u32[]{:S(2)}) %collective-permute-start.4) | collective-permute-done | bytes 6176 | tf_op jit(solution)/shard_map/ppermute | solution.py:111
  17.4 0.0 collective-permute-done.3.refs_1_
  17.4 0.0 copy-done.4
  17.4 0.0 copy-start
  17.4 0.0 copy-start.1
  17.4 1.1 %pick.1 = (bf16[384,1024]{1,0:T(8,128)(2,1)S(1)}, s32[1,384]{1,0:T(1,128)S(1)}) custom-call(s32[2]{0:T(128)S(1)} %pad_add_fusion.1.refs_0_.place, s32[1,384]{1,0:T(1,128)S(1)} %and_select_fusion.1.expert_ref, bf16[384,384]{1,0:T(8,128)(2,1)S(1)} %prep.1.spread_ref, bf16[192,1024]{1,0:T(8,128)(2,1)S(1)} %copy-done.4, s32[4,384]{1,0:T(4,128)S(1)} %pad_add_fusion.refs_0_, ...), custom_call_target="tpu_custom_call" | custom-call | flops 15099494400 | bytes 1502208 | tf_op jit(solution)/shard_map/pick/pallas_call | solution.py:21
  18.6 21.6 %all_to_all.10 = bf16[16,24,1024]{2,1,0:T(8,128)(2,1)S(1)} all-to-all(bf16[16,24,1024]{2,1,0:T(8,128)(2,1)S(1)} %bitcast.9), channel_id=1, replica_groups=mesh['ep'=16,'tp'=2] {'ep'}, dimensions={0} | all-to-all | bytes 1572864 | tf_op jit(solution)/shard_map/all_to_all | solution.py:150
  40.1 0.0 copy-start.3
  40.1 0.0 collective-permute-start.6
  40.1 0.0 copy-done
  40.1 0.0 copy-done.1
  40.1 0.0 copy-start.2
  40.1 2.4 %ffn_first.1 = (f32[384,1024]{1,0:T(8,128)S(1)}, f32[384,1024]{1,0:T(8,128)S(1)}) custom-call(s32[2]{0:T(128)S(1)} %pad_add_fusion.1.refs_0_.place, bf16[384,1024]{1,0:T(8,128)(2,1)S(1)} %bitcast.7, bf16[1,2048,1024]{2,1,0:T(8,128)(2,1)S(1)} %copy-done, bf16[1,2048,1024]{2,1,0:T(8,128)(2,1)S(1)} %copy-done.1), custom_call_target="tpu_custom_call" | custom-call | flops 1610612736 | bytes 12320768 | tf_op jit(solution)/shard_map/ffn_first/pallas_call | solution.py:21
  42.5 0.0 collective-permute-done.6.other_ref
  42.5 0.0 copy-done.3
  42.5 0.0 copy-done.2
  42.5 3.5 %ffn_second.1 = (bf16[384,1024]{1,0:T(8,128)(2,1)S(1)}, bf16[384,1024]{1,0:T(8,128)(2,1)S(1)}) custom-call(s32[2]{0:T(128)S(1)} %pad_add_fusion.1.refs_0_.place, bf16[384,1024]{1,0:T(8,128)(2,1)S(1)} %collective-permute-done.6.other_ref, f32[384,1024]{1,0:T(8,128)S(1)} %get-tuple-element.23.gate_ref, f32[384,1024]{1,0:T(8,128)S(1)} %get-tuple-element.24.up_ref, ...), custom_call_target="tpu_custom_call" | custom-call | flops 2415919104 | bytes 18089472 | tf_op jit(solution)/shard_map/ffn_second/pallas_call | solution.py:21
  46.1 0.5 collective-permute-start.7
  46.6 1.5 %ffn_third.1 = f32[384,1024]{1,0:T(8,128)S(1)} custom-call(s32[2]{0:T(128)S(1)} %pad_add_fusion.1.refs_0_.place, bf16[384,1024]{1,0:T(8,128)(2,1)S(1)} %get-tuple-element.25.hidden_ref, bf16[1,1024,2048]{2,1,0:T(8,128)(2,1)S(1)} %copy-done.2), custom_call_target="tpu_custom_call" | custom-call | flops 805306368 | bytes 6553600 | tf_op jit(solution)/shard_map/ffn_third/pallas_call | solution.py:21
  48.1 0.4 collective-permute-done.7
  48.5 0.3 add_convert_fusion
  48.8 25.0 %all_to_all.11 = bf16[16,24,1024]{2,1,0:T(8,128)(2,1)S(1)} all-to-all(bf16[16,24,1024]{2,1,0:T(8,128)(2,1)S(1)} %bitcast.10), channel_id=1, replica_groups=mesh['ep'=16,'tp'=2] {'ep'}, dimensions={0} | all-to-all | bytes 1572864 | tf_op jit(solution)/shard_map/all_to_all | solution.py:176
  73.8 1.1 %mix.1 = bf16[192,1024]{1,0:T(8,128)(2,1)} custom-call(s32[1,384]{1,0:T(1,128)S(1)} %get-tuple-element.21.row_ref, bf16[384,1024]{1,0:T(8,128)(2,1)S(1)} %bitcast.8), custom_call_target="tpu_custom_call" | custom-call | flops 150994944 | bytes 1181184 | tf_op jit(solution)/shard_map/mix/pallas_call | solution.py:21
  (3 shorter events, 0.0 us)
Async XLA Ops:
  0.0 5.2 %collective-permute-start.1 = (s32[1,384]{1,0:T(1,128)}, s32[1,384]{1,0:T(1,128)S(1)}, u32[]{:S(2)}, u32[]{:S(2)}) collective-permute-start(s32[1,384]{1,0:T(1,128)} %param.7), channel_id=1, source_target_pairs={{0,4},{2,6},{4,0},{6,2},{8,12},{10,14},{12,8},{14,10},{16,20},{18,... | collective-permute-start | bytes 4616 | tf_op jit(solution)/shard_map/ppermute | solution.py:111
  3.0 3.8 %collective-permute-start = (s32[1,384]{1,0:T(1,128)}, s32[1,384]{1,0:T(1,128)S(1)}, u32[]{:S(2)}, u32[]{:S(2)}) collective-permute-start(s32[1,384]{1,0:T(1,128)} %param.7), channel_id=1, source_target_pairs={{0,2},{2,0},{4,6},{6,4},{8,10},{10,8},{12,14},{14,12},{16,18},{18,... | collective-permute-start | bytes 4616 | tf_op jit(solution)/shard_map/ppermute | solution.py:111
  4.5 4.7 %collective-permute-start.2 = (s32[1,384]{1,0:T(1,128)}, s32[1,384]{1,0:T(1,128)S(1)}, u32[]{:S(2)}, u32[]{:S(2)}) collective-permute-start(s32[1,384]{1,0:T(1,128)} %param.7), channel_id=1, source_target_pairs={{0,6},{2,4},{4,2},{6,0},{8,14},{10,12},{12,10},{14,8},{16,22},{18,... | collective-permute-start | bytes 4616 | tf_op jit(solution)/shard_map/ppermute | solution.py:111
  4.6 4.6 %copy-start.5 = (s32[1,384]{1,0:T(1,128)S(1)}, s32[1,384]{1,0:T(1,128)}, u32[]{:S(2)}) copy-start(s32[1,384]{1,0:T(1,128)} %param.7) | copy-start | bytes 4612
  4.6 12.8 %copy-start.4 = (bf16[192,1024]{1,0:T(8,128)(2,1)S(1)}, bf16[192,1024]{1,0:T(8,128)(2,1)}, u32[]{:S(2)}) copy-start(bf16[192,1024]{1,0:T(8,128)(2,1)} %tokens_ref.1) | copy-start | bytes 1179652
  9.2 5.5 %collective-permute-start.5 = (s32[4,384]{1,0:T(4,128)S(1)}, s32[4,384]{1,0:T(4,128)S(1)}, u32[]{:S(2)}, u32[]{:S(2)}) collective-permute-start(s32[4,384]{1,0:T(4,128)S(1)} %pad_add_fusion.refs_0_), channel_id=1, source_target_pairs={{0,24},{2,26},{4,28},{6,30},{8,16},{10,18},{12,20},{14,22},{16,8},... | collective-permute-start | bytes 18440 | tf_op jit(solution)/shard_map/ppermute | solution.py:111
  12.9 4.5 %collective-permute-start.4 = (s32[4,384]{1,0:T(4,128)S(1)}, s32[4,384]{1,0:T(4,128)S(1)}, u32[]{:S(2)}, u32[]{:S(2)}) collective-permute-start(s32[4,384]{1,0:T(4,128)S(1)} %pad_add_fusion.refs_0_), channel_id=1, source_target_pairs={{0,16},{2,18},{4,20},{6,22},{8,24},{10,26},{12,28},{14,30},{16,0},... | collective-permute-start | bytes 18440 | tf_op jit(solution)/shard_map/ppermute | solution.py:111
  12.9 4.5 %collective-permute-start.3 = (s32[4,384]{1,0:T(4,128)S(1)}, s32[4,384]{1,0:T(4,128)S(1)}, u32[]{:S(2)}, u32[]{:S(2)}) collective-permute-start(s32[4,384]{1,0:T(4,128)S(1)} %pad_add_fusion.refs_0_), channel_id=1, source_target_pairs={{0,8},{2,10},{4,12},{6,14},{8,0},{10,2},{12,4},{14,6},{16,24},{18,... | collective-permute-start | bytes 18440 | tf_op jit(solution)/shard_map/ppermute | solution.py:111
  17.4 22.7 %copy-start = (bf16[1,2048,1024]{2,1,0:T(8,128)(2,1)S(1)}, bf16[1,2048,1024]{2,1,0:T(8,128)(2,1)}, u32[]{:S(2)}) copy-start(bf16[1,2048,1024]{2,1,0:T(8,128)(2,1)} %gate_w.3) | copy-start | bytes 12582916
  17.4 22.7 %copy-start.1 = (bf16[1,2048,1024]{2,1,0:T(8,128)(2,1)S(1)}, bf16[1,2048,1024]{2,1,0:T(8,128)(2,1)}, u32[]{:S(2)}) copy-start(bf16[1,2048,1024]{2,1,0:T(8,128)(2,1)} %up_w.3) | copy-start | bytes 12582916
  40.1 2.4 %copy-start.3 = (f32[1,384]{1,0:T(1,128)S(1)}, f32[1,384]{1,0:T(1,128)}, u32[]{:S(2)}) copy-start(f32[1,384]{1,0:T(1,128)} %score_ref.1) | copy-start | bytes 4612
  40.1 2.4 %collective-permute-start.6 = (bf16[384,1024]{1,0:T(8,128)(2,1)S(1)}, bf16[384,1024]{1,0:T(8,128)(2,1)S(1)}, u32[]{:S(2)}, u32[]{:S(2)}) collective-permute-start(bf16[384,1024]{1,0:T(8,128)(2,1)S(1)} %bitcast.6), channel_id=1, source_target_pairs={{0,1},{1,0},{2,3},{3,2},{4,5},{5,4},{6,7},{7,6},{8,9},{9,8},{10,11... | collective-permute-start | bytes 2359304 | tf_op jit(solution)/shard_map/ppermute | solution.py:153
  40.1 2.4 %copy-start.2 = (bf16[1,1024,2048]{2,1,0:T(8,128)(2,1)S(1)}, bf16[1,1024,2048]{2,1,0:T(8,128)(2,1)}, u32[]{:S(2)}) copy-start(bf16[1,1024,2048]{2,1,0:T(8,128)(2,1)} %down_w.3) | copy-start | bytes 12582916
  46.1 2.5 %collective-permute-start.7 = (bf16[384,1024]{1,0:T(8,128)(2,1)S(1)}, bf16[384,1024]{1,0:T(8,128)(2,1)S(1)}, u32[]{:S(2)}, u32[]{:S(2)}) collective-permute-start(bf16[384,1024]{1,0:T(8,128)(2,1)S(1)} %get-tuple-element.26), channel_id=1, source_target_pairs={{0,1},{1,0},{2,3},{3,2},{4,5},{5,4},{6,7},{7,6},{8,9},{9,8},{10,11... | collective-permute-start | bytes 2359304 | tf_op jit(solution)/shard_map/ppermute | solution.py:169

commit v5 on v4

--- a/solution.py
+++ b/solution.py
@@ -5,7 +5,6 @@
 from jax.experimental.pallas import tpu as pltpu
 from jax.sharding import PartitionSpec as P
 
-SMEM = pl.BlockSpec(memory_space=pltpu.SMEM)
 VMEM = pl.BlockSpec(memory_space=pltpu.VMEM)
 HBM = pl.BlockSpec(memory_space=pltpu.HBM)
 MIB = 1 << 20
@@ -40,16 +39,16 @@
     return pl.ds(pl.multiple_of(which * width, width), width)
 
 
-def prep_kernel(per_source, place, within_ref, spread_ref):
+def prep_kernel(per_source, within_ref, spread_ref):
     slots = within_ref.shape[1]
     column = lax.broadcasted_iota(jnp.int32, (slots, slots), 0)
-    hit = column == place[0] * per_source + within_ref[...]
+    hit = column == lax.axis_index("ep") * per_source + within_ref[...]
     spread_ref[...] = hit.astype(jnp.float32).astype(jnp.bfloat16)
 
 
-def pick_kernel(place, expert_ref, spread_ref, tokens_ref, *refs):
+def pick_kernel(expert_ref, code_ref, spread_ref, tokens_ref, *refs):
     parts, (out_ref, row_ref, ids_ref) = refs[:-3], refs[-3:]
-    me = place[0]
+    me = lax.axis_index("ep")
     tok_rows, slots = tokens_ref.shape[0], spread_ref.shape[0]
     step = parts[0].shape[0]
     count = step * len(parts)
@@ -60,7 +59,7 @@
     both = jnp.concatenate([high, low], axis=0).astype(jnp.float32).astype(jnp.bfloat16)
     mine = dot(both, spread_ref[...])
     mine = mine[:count] * 128.0 + mine[count:]
-    ours = lax.broadcasted_iota(jnp.int32, (count, slots), 0) == (expert_ref[...] ^ me)
+    ours = code_ref[...] == (expert_ref[...] ^ me)
     row = jnp.sum(jnp.where(ours, mine, 0.0), axis=0, keepdims=True).astype(jnp.int32)
     row_ref[...] = row
     selector = lax.broadcasted_iota(jnp.int32, (tok_rows, slots), 0) == row
@@ -70,18 +69,19 @@
     ).astype(jnp.bfloat16)
 
 
-def first_kernel(place, own_ref, gate_w, up_w, gate_ref, up_ref):
-    mine = half(place[1], own_ref.shape[1])
+def first_kernel(own_ref, gate_w, up_w, down_w, gate_ref, up_ref):
+    del down_w
+    mine = half(lax.axis_index("tp"), own_ref.shape[1])
     gate_ref[...] = dot(own_ref[...], gate_w[0, mine, :])
     up_ref[...] = dot(own_ref[...], up_w[0, mine, :])
 
 
 def second_kernel(
-    place, other_ref, gate_ref, up_ref, gate_w, up_w, down_w, score_ref, hidden_ref, send_ref
+    other_ref, gate_ref, up_ref, gate_w, up_w, down_w, score_ref, hidden_ref, send_ref
 ):
-    theirs = half(1 - place[1], other_ref.shape[1])
+    theirs = half(1 - lax.axis_index("tp"), other_ref.shape[1])
     rows, units = gate_ref.shape
-    tile = 256 if units % 256 == 0 else units
+    tile = 512 if units % 512 == 0 else units
     score = jnp.transpose(jnp.broadcast_to(score_ref[...], (128, rows)))
     score = jnp.concatenate([score] * (tile // 128), axis=1)
     for start in range(0, units, tile):
@@ -93,8 +93,8 @@
     send_ref[...] = dot(hidden_ref[...], down_w[0, :, theirs]).astype(jnp.bfloat16)
 
 
-def third_kernel(place, hidden_ref, down_w, keep_ref):
-    keep_ref[...] = dot(hidden_ref[...], down_w[0, :, half(place[1], keep_ref.shape[1])])
+def third_kernel(hidden_ref, down_w, keep_ref):
+    keep_ref[...] = dot(hidden_ref[...], down_w[0, :, half(lax.axis_index("tp"), keep_ref.shape[1])])
 
 
 def mix_kernel(row_ref, returned_ref, out_ref):
@@ -119,32 +119,31 @@
     per_source = slots // ep_count
     rows = ep_count * per_source
     units = gate_weight.shape[2]
-    me = lax.axis_index("ep").astype(jnp.int32)
-    place = jnp.stack([me, lax.axis_index("tp").astype(jnp.int32)])
     swap = [(0, 1), (1, 0)]
 
     order = jnp.arange(slots, dtype=jnp.int32)[None, :]
     (spread,) = call(
-        lambda *refs: prep_kernel(per_source, *refs), "prep", [SMEM, VMEM],
-        (jax.ShapeDtypeStruct((slots, slots), jnp.bfloat16),), 10**10, (place, order % per_source),
+        lambda *refs: prep_kernel(per_source, *refs), "prep", [VMEM],
+        (jax.ShapeDtypeStruct((slots, slots), jnp.bfloat16),), 10**10, (order % per_source,),
     )
-    parts, stride = [chosen], 1
-    while stride < ep_count:
+    parts, codes, stride = [chosen], [0], ep_count
+    while stride > 1:
         ids = jnp.concatenate(parts, axis=0)
-        radix = 4 if ep_count % (4 * stride) == 0 else 2
+        radix = 4 if stride % 4 == 0 else 2
+        stride //= radix
+        codes = [k * stride + c for k in range(radix) for c in codes]
         parts = gather_round(ids, stride, radix, ep_count)
-        if stride == 1:
+        if stride * radix == ep_count:
             parts, spread = lax.optimization_barrier((parts, spread))
-        stride *= radix
 
     outgoing, row = call(
-        pick_kernel, "pick", [SMEM] + [VMEM] * (3 + len(parts)),
+        pick_kernel, "pick", [VMEM] * (4 + len(parts)),
         (
             jax.ShapeDtypeStruct((rows, width), tokens.dtype),
             jax.ShapeDtypeStruct((1, slots), jnp.int32),
         ),
         200 * rows * tok_rows * width,
-        (place, order // per_source, spread, tokens, *parts),
+        (order // per_source, jnp.array(codes, jnp.int32)[:, None], spread, tokens, *parts),
         [pltpu.VMEM((ep_count, slots), jnp.int32)],
     )
     arrived = lax.all_to_all(
@@ -154,23 +153,23 @@
     pre = jax.ShapeDtypeStruct((rows, units), jnp.float32)
     product = 2 * rows * width * units
     gate_pre, up_pre = call(
-        first_kernel, "ffn_first", [SMEM] + [VMEM] * 3, (pre, pre), 2 * product,
-        (place, arrived, gate_weight, up_weight),
+        first_kernel, "ffn_first", [VMEM] * 4, (pre, pre), 2 * product,
+        (arrived, gate_weight, up_weight, down_weight),
     )
     hidden, sent = call(
-        second_kernel, "ffn_second", [SMEM] + [VMEM] * 7,
+        second_kernel, "ffn_second", [VMEM] * 7,
         (
             jax.ShapeDtypeStruct((rows, units), jnp.bfloat16),
             jax.ShapeDtypeStruct((rows, width), jnp.bfloat16),
         ),
         3 * product,
-        (place, other, gate_pre, up_pre, gate_weight, up_weight, down_weight, gate_score),
+        (other, gate_pre, up_pre, gate_weight, up_weight, down_weight, gate_score),
     )
     got = lax.ppermute(sent, "tp", swap)
     (kept,) = call(
-        third_kernel, "ffn_third", [SMEM] + [VMEM] * 2,
+        third_kernel, "ffn_third", [VMEM] * 2,
         (jax.ShapeDtypeStruct((rows, width), jnp.float32),), product,
-        (place, hidden, down_weight),
+        (hidden, down_weight),
     )
     weighted = (kept + got.astype(jnp.float32)).astype(jnp.bfloat16)
     returned = lax.all_to_all(

time: 75.1 us -> 73.7 us (0.981)
  Pallas kernels: 10.2 us -> 7.44 us
  waiting for transfers between devices: 8.08 us -> 10.1 us
    pallas_call x6, Pallas kernels: 10.2 us -> 7.44 us  [call(): pl.pallas_call(body, out_shape=outs, in_specs=in_specs, out_specs=tuple((...]
    ppermute x6, waiting for transfers between devices: 7.7 us -> 8.54 us  [gather_round(): lax.ppermute(value, 'ep', [(e, e ^ k * stride) for e in range(count)])]
    ppermute x1, waiting for transfers between devices: 0.38 us -> 1.17 us  [on_device(): got = lax.ppermute(sent, 'tp', swap)]
  transfers between devices with their start and end apart: 8 -> 8, of which waited for: 5 -> 8; matrix products, arithmetic and copies ran while one was open for 0% -> 0% of each run, Pallas kernels for 6% -> 4%
where the time goes in v5:
time: 73.7 us; the launch traced here: 73.5 us
  blocking collectives  46 us (62%)
  waiting for transfers between devices  10.1 us (14%)
  starting transfers between devices  9.4 us (13%)
  Pallas kernels  7.44 us (10%)
    all_to_all x1, blocking collectives, on_device(): lax.all_to_all(weighted.reshape(ep_count, per_source, width), 'ep', split...  24.8 us
    all_to_all x1, blocking collectives, on_device(): lax.all_to_all(outgoing.reshape(ep_count, per_source, width), 'ep', split...  21.3 us
    ppermute x6, starting transfers between devices, gather_round(): lax.ppermute(value, 'ep', [(e, e ^ k * stride) for e in range(count)])  9.2 us
    ppermute x6, waiting for transfers between devices, gather_round(): lax.ppermute(value, 'ep', [(e, e ^ k * stride) for e in range(count)])  8.54 us
    pallas_call x6, Pallas kernels, call(): pl.pallas_call(body, out_shape=outs, in_specs=in_specs, out_specs=tuple((...  7.44 us
  transfers between devices with their start and end apart: 8, of which 8 were waited for; matrix products, arithmetic and copies ran while one was open for 0% of the time, Pallas kernels for 4%

profile of v5, /device:TPU:0, one launch (start us, length us, event | category | flops | bytes accessed | tf_op | source)
XLA Modules:
  0.0 73.5 jit_solution(12556809214526343915)
XLA Ops:
  0.0 4.1 %collective-permute-start.1 = (s32[1,384]{1,0:T(1,128)}, s32[1,384]{1,0:T(1,128)S(1)}, u32[]{:S(2)}, u32[]{:S(2)}) collective-permute-start(s32[1,384]{1,0:T(1,128)} %param.8), channel_id=1, source_target_pairs={{0,16},{2,18},{4,20},{6,22},{8,24},{10,26},{12,28},{14,30},{16,0},... | collective-permute-start | bytes 4616 | tf_op jit(solution)/shard_map/ppermute | solution.py:111
  4.1 1.6 %collective-permute-start = (s32[1,384]{1,0:T(1,128)}, s32[1,384]{1,0:T(1,128)S(1)}, u32[]{:S(2)}, u32[]{:S(2)}) collective-permute-start(s32[1,384]{1,0:T(1,128)} %param.8), channel_id=1, source_target_pairs={{0,8},{2,10},{4,12},{6,14},{8,0},{10,2},{12,4},{14,6},{16,24},{18,... | collective-permute-start | bytes 4616 | tf_op jit(solution)/shard_map/ppermute | solution.py:111
  5.6 0.0 collective-permute-start.2
  5.7 0.0 copy-start.6
  5.7 0.0 copy-start.4
  5.7 0.0 copy-start.5
  5.7 0.1 prep.1.spread_ref
  5.8 0.1 collective-permute-done.1
  5.8 2.0 %collective-permute-done = s32[1,384]{1,0:T(1,128)S(1)} collective-permute-done((s32[1,384]{1,0:T(1,128)}, s32[1,384]{1,0:T(1,128)S(1)}, u32[]{:S(2)}, u32[]{:S(2)}) %collective-permute-start) | collective-permute-done | bytes 1568 | tf_op jit(solution)/shard_map/ppermute | solution.py:111
  7.9 3.4 %collective-permute-done.2 = s32[1,384]{1,0:T(1,128)S(1)} collective-permute-done((s32[1,384]{1,0:T(1,128)}, s32[1,384]{1,0:T(1,128)S(1)}, u32[]{:S(2)}, u32[]{:S(2)}) %collective-permute-start.2) | collective-permute-done | bytes 1568 | tf_op jit(solution)/shard_map/ppermute | solution.py:111
  11.2 0.0 copy-done.6
  11.2 2.5 %collective-permute-start.5 = (s32[4,384]{1,0:T(4,128)S(1)}, s32[4,384]{1,0:T(4,128)S(1)}, u32[]{:S(2)}, u32[]{:S(2)}) collective-permute-start(s32[4,384]{1,0:T(4,128)S(1)} %pad_add_fusion.refs_0_), channel_id=1, source_target_pairs={{0,6},{2,4},{4,2},{6,0},{8,14},{10,12},{12,10},{14,8},{16,22},{18,... | collective-permute-start | bytes 18440 | tf_op jit(solution)/shard_map/ppermute | solution.py:111
  13.8 0.5 collective-permute-start.4
  14.3 0.5 collective-permute-start.3
  14.8 1.0 %collective-permute-done.5.refs_3_ = s32[4,384]{1,0:T(4,128)S(1)} collective-permute-done((s32[4,384]{1,0:T(4,128)S(1)}, s32[4,384]{1,0:T(4,128)S(1)}, u32[]{:S(2)}, u32[]{:S(2)}) %collective-permute-start.5) | collective-permute-done | bytes 6176 | tf_op jit(solution)/shard_map/ppermute | solution.py:111
  15.8 1.5 %collective-permute-done.4.refs_2_ = s32[4,384]{1,0:T(4,128)S(1)} collective-permute-done((s32[4,384]{1,0:T(4,128)S(1)}, s32[4,384]{1,0:T(4,128)S(1)}, u32[]{:S(2)}, u32[]{:S(2)}) %collective-permute-start.4) | collective-permute-done | bytes 6176 | tf_op jit(solution)/shard_map/ppermute | solution.py:111
  17.4 0.5 collective-permute-done.3.refs_1_
  17.9 0.0 copy-done.4
  17.9 0.0 copy-done.5
  17.9 0.0 copy-start
  17.9 0.0 copy-start.1
  17.9 0.0 copy-start.2
  17.9 0.6 pick.1
  18.5 21.3 %all_to_all.10 = bf16[16,24,1024]{2,1,0:T(8,128)(2,1)S(1)} all-to-all(bf16[16,24,1024]{2,1,0:T(8,128)(2,1)S(1)} %bitcast.7), channel_id=1, replica_groups=mesh['ep'=16,'tp'=2] {'ep'}, dimensions={0} | all-to-all | bytes 1572864 | tf_op jit(solution)/shard_map/all_to_all | solution.py:149
  39.8 0.0 copy-start.3
  39.8 0.0 collective-permute-start.6
  39.8 0.0 copy-done
  39.8 0.0 copy-done.1
  39.8 0.0 copy-done.2
  39.8 1.8 %ffn_first.1 = (f32[384,1024]{1,0:T(8,128)S(1)}, f32[384,1024]{1,0:T(8,128)S(1)}) custom-call(bf16[384,1024]{1,0:T(8,128)(2,1)S(1)} %bitcast.5, bf16[1,2048,1024]{2,1,0:T(8,128)(2,1)S(1)} %copy-done.1, bf16[1,2048,1024]{2,1,0:T(8,128)(2,1)S(1)} %copy-done.2, bf16[1,1024,2048]{2,1,0:T(8,128)(2,1)S(1)} %copy-done), custom_call_target="tpu_custom_call" | custom-call | flops 1610612736 | bytes 16515072 | tf_op jit(solution)/shard_map/ffn_first/pallas_call | solution.py:20
  41.6 0.4 collective-permute-done.6.other_ref
  42.1 0.0 copy-done.3
  42.1 2.9 %ffn_second.1 = (bf16[384,1024]{1,0:T(8,128)(2,1)S(1)}, bf16[384,1024]{1,0:T(8,128)(2,1)S(1)}) custom-call(bf16[384,1024]{1,0:T(8,128)(2,1)S(1)} %collective-permute-done.6.other_ref, f32[384,1024]{1,0:T(8,128)S(1)} %get-tuple-element.23.gate_ref, f32[384,1024]{1,0:T(8,128)S(1)} %get-tuple-element.24.up_ref, bf16[1,2048,1024]{2,1,0:T(8,128)(2,1)S(1)} %copy-done.1, ...), custom_call_target="tpu_custom_call" | custom-call | flops 2415919104 | bytes 18089472 | tf_op jit(solution)/shard_map/ffn_second/pallas_call | solution.py:20
  45.0 0.2 collective-permute-start.7
  45.2 1.0 %ffn_third.1 = f32[384,1024]{1,0:T(8,128)S(1)} custom-call(bf16[384,1024]{1,0:T(8,128)(2,1)S(1)} %get-tuple-element.25.hidden_ref, bf16[1,1024,2048]{2,1,0:T(8,128)(2,1)S(1)} %copy-done), custom_call_target="tpu_custom_call" | custom-call | flops 805306368 | bytes 6553600 | tf_op jit(solution)/shard_map/ffn_third/pallas_call | solution.py:20
  46.1 1.2 %collective-permute-done.7 = bf16[384,1024]{1,0:T(8,128)(2,1)S(1)} collective-permute-done((bf16[384,1024]{1,0:T(8,128)(2,1)S(1)}, bf16[384,1024]{1,0:T(8,128)(2,1)S(1)}, u32[]{:S(2)}, u32[]{:S(2)}) %collective-permute-start.7) | collective-permute-done | bytes 786464 | tf_op jit(solution)/shard_map/ppermute | solution.py:168
  47.3 0.3 add_convert_fusion
  47.6 24.8 %all_to_all.11 = bf16[16,24,1024]{2,1,0:T(8,128)(2,1)S(1)} all-to-all(bf16[16,24,1024]{2,1,0:T(8,128)(2,1)S(1)} %bitcast.8), channel_id=1, replica_groups=mesh['ep'=16,'tp'=2] {'ep'}, dimensions={0} | all-to-all | bytes 1572864 | tf_op jit(solution)/shard_map/all_to_all | solution.py:175
  72.3 1.1 %mix.1 = bf16[192,1024]{1,0:T(8,128)(2,1)} custom-call(s32[1,384]{1,0:T(1,128)S(1)} %get-tuple-element.21.row_ref, bf16[384,1024]{1,0:T(8,128)(2,1)S(1)} %bitcast.6), custom_call_target="tpu_custom_call" | custom-call | flops 150994944 | bytes 1181184 | tf_op jit(solution)/shard_map/mix/pallas_call | solution.py:20
  (3 shorter events, 0.0 us)
Async XLA Ops:
  0.0 5.8 %collective-permute-start.1 = (s32[1,384]{1,0:T(1,128)}, s32[1,384]{1,0:T(1,128)S(1)}, u32[]{:S(2)}, u32[]{:S(2)}) collective-permute-start(s32[1,384]{1,0:T(1,128)} %param.8), channel_id=1, source_target_pairs={{0,16},{2,18},{4,20},{6,22},{8,24},{10,26},{12,28},{14,30},{16,0},... | collective-permute-start | bytes 4616 | tf_op jit(solution)/shard_map/ppermute | solution.py:111
  4.1 3.8 %collective-permute-start = (s32[1,384]{1,0:T(1,128)}, s32[1,384]{1,0:T(1,128)S(1)}, u32[]{:S(2)}, u32[]{:S(2)}) collective-permute-start(s32[1,384]{1,0:T(1,128)} %param.8), channel_id=1, source_target_pairs={{0,8},{2,10},{4,12},{6,14},{8,0},{10,2},{12,4},{14,6},{16,24},{18,... | collective-permute-start | bytes 4616 | tf_op jit(solution)/shard_map/ppermute | solution.py:111
  5.6 5.6 %collective-permute-start.2 = (s32[1,384]{1,0:T(1,128)}, s32[1,384]{1,0:T(1,128)S(1)}, u32[]{:S(2)}, u32[]{:S(2)}) collective-permute-start(s32[1,384]{1,0:T(1,128)} %param.8), channel_id=1, source_target_pairs={{0,24},{2,26},{4,28},{6,30},{8,16},{10,18},{12,20},{14,22},{16,8},... | collective-permute-start | bytes 4616 | tf_op jit(solution)/shard_map/ppermute | solution.py:111
  5.7 5.6 %copy-start.6 = (s32[1,384]{1,0:T(1,128)S(1)}, s32[1,384]{1,0:T(1,128)}, u32[]{:S(2)}) copy-start(s32[1,384]{1,0:T(1,128)} %param.8) | copy-start | bytes 4612
  5.7 12.2 %copy-start.4 = (bf16[192,1024]{1,0:T(8,128)(2,1)S(1)}, bf16[192,1024]{1,0:T(8,128)(2,1)}, u32[]{:S(2)}) copy-start(bf16[192,1024]{1,0:T(8,128)(2,1)} %tokens_ref.1) | copy-start | bytes 1179652
  5.7 12.2 %copy-start.5 = (s32[16,1]{1,0:T(8,128)S(1)}, s32[16,1]{1,0:T(8,128)}, u32[]{:S(2)}) copy-start(s32[16,1]{1,0:T(8,128)} %constant.28.code_ref) | copy-start | bytes 196
  11.2 4.6 %collective-permute-start.5 = (s32[4,384]{1,0:T(4,128)S(1)}, s32[4,384]{1,0:T(4,128)S(1)}, u32[]{:S(2)}, u32[]{:S(2)}) collective-permute-start(s32[4,384]{1,0:T(4,128)S(1)} %pad_add_fusion.refs_0_), channel_id=1, source_target_pairs={{0,6},{2,4},{4,2},{6,0},{8,14},{10,12},{12,10},{14,8},{16,22},{18,... | collective-permute-start | bytes 18440 | tf_op jit(solution)/shard_map/ppermute | solution.py:111
  13.8 3.6 %collective-permute-start.4 = (s32[4,384]{1,0:T(4,128)S(1)}, s32[4,384]{1,0:T(4,128)S(1)}, u32[]{:S(2)}, u32[]{:S(2)}) collective-permute-start(s32[4,384]{1,0:T(4,128)S(1)} %pad_add_fusion.refs_0_), channel_id=1, source_target_pairs={{0,4},{2,6},{4,0},{6,2},{8,12},{10,14},{12,8},{14,10},{16,20},{18,... | collective-permute-start | bytes 18440 | tf_op jit(solution)/shard_map/ppermute | solution.py:111
  14.3 3.6 %collective-permute-start.3 = (s32[4,384]{1,0:T(4,128)S(1)}, s32[4,384]{1,0:T(4,128)S(1)}, u32[]{:S(2)}, u32[]{:S(2)}) collective-permute-start(s32[4,384]{1,0:T(4,128)S(1)} %pad_add_fusion.refs_0_), channel_id=1, source_target_pairs={{0,2},{2,0},{4,6},{6,4},{8,10},{10,8},{12,14},{14,12},{16,18},{18,... | collective-permute-start | bytes 18440 | tf_op jit(solution)/shard_map/ppermute | solution.py:111
  17.9 21.9 %copy-start = (bf16[1,1024,2048]{2,1,0:T(8,128)(2,1)S(1)}, bf16[1,1024,2048]{2,1,0:T(8,128)(2,1)}, u32[]{:S(2)}) copy-start(bf16[1,1024,2048]{2,1,0:T(8,128)(2,1)} %down_w.5) | copy-start | bytes 12582916
  17.9 21.9 %copy-start.1 = (bf16[1,2048,1024]{2,1,0:T(8,128)(2,1)S(1)}, bf16[1,2048,1024]{2,1,0:T(8,128)(2,1)}, u32[]{:S(2)}) copy-start(bf16[1,2048,1024]{2,1,0:T(8,128)(2,1)} %gate_w.3) | copy-start | bytes 12582916
  17.9 21.9 %copy-start.2 = (bf16[1,2048,1024]{2,1,0:T(8,128)(2,1)S(1)}, bf16[1,2048,1024]{2,1,0:T(8,128)(2,1)}, u32[]{:S(2)}) copy-start(bf16[1,2048,1024]{2,1,0:T(8,128)(2,1)} %up_w.3) | copy-start | bytes 12582916
  39.8 2.3 %copy-start.3 = (f32[1,384]{1,0:T(1,128)S(1)}, f32[1,384]{1,0:T(1,128)}, u32[]{:S(2)}) copy-start(f32[1,384]{1,0:T(1,128)} %score_ref.1) | copy-start | bytes 4612
  39.8 2.3 %collective-permute-start.6 = (bf16[384,1024]{1,0:T(8,128)(2,1)S(1)}, bf16[384,1024]{1,0:T(8,128)(2,1)S(1)}, u32[]{:S(2)}, u32[]{:S(2)}) collective-permute-start(bf16[384,1024]{1,0:T(8,128)(2,1)S(1)} %bitcast.4), channel_id=1, source_target_pairs={{0,1},{1,0},{2,3},{3,2},{4,5},{5,4},{6,7},{7,6},{8,9},{9,8},{10,11... | collective-permute-start | bytes 2359304 | tf_op jit(solution)/shard_map/ppermute | solution.py:152
  45.0 2.4 %collective-permute-start.7 = (bf16[384,1024]{1,0:T(8,128)(2,1)S(1)}, bf16[384,1024]{1,0:T(8,128)(2,1)S(1)}, u32[]{:S(2)}, u32[]{:S(2)}) collective-permute-start(bf16[384,1024]{1,0:T(8,128)(2,1)S(1)} %get-tuple-element.26), channel_id=1, source_target_pairs={{0,1},{1,0},{2,3},{3,2},{4,5},{5,4},{6,7},{7,6},{8,9},{9,8},{10,11... | collective-permute-start | bytes 2359304 | tf_op jit(solution)/shard_map/ppermute | solution.py:168

commit v6 on v5

--- a/solution.py
+++ b/solution.py
@@ -4,6 +4,7 @@
 from jax.experimental import pallas as pl
 from jax.experimental.pallas import tpu as pltpu
 from jax.sharding import PartitionSpec as P
+
 
 VMEM = pl.BlockSpec(memory_space=pltpu.VMEM)
 HBM = pl.BlockSpec(memory_space=pltpu.HBM)
@@ -14,7 +15,7 @@
     return x.size * x.dtype.itemsize
 
 
-def call(body, name, in_specs, outs, flops, args, scratch=(), grant=0):
+def call(body, in_specs, outs, flops, args, scratch=(), grant=0):
     held = sum(nbytes(x) for x in outs)
     held += sum(nbytes(x) for x, spec in zip(args, in_specs) if spec is VMEM)
     return pl.pallas_call(
@@ -27,7 +28,6 @@
         compiler_params=pltpu.CompilerParams(
             vmem_limit_bytes=grant or min(held + 6 * MIB, 60 * MIB)
         ),
-        name=name,
     )(*args)
 
 
@@ -112,7 +112,7 @@
     return parts
 
 
-def on_device(tokens, chosen, gate_score, gate_weight, up_weight, down_weight):
+def layer(tokens, chosen, gate_score, gate_weight, up_weight, down_weight):
     ep_count = lax.axis_size("ep")
     tok_rows, width = tokens.shape
     slots = chosen.shape[1]
@@ -123,7 +123,7 @@
 
     order = jnp.arange(slots, dtype=jnp.int32)[None, :]
     (spread,) = call(
-        lambda *refs: prep_kernel(per_source, *refs), "prep", [VMEM],
+        lambda *refs: prep_kernel(per_source, *refs), [VMEM],
         (jax.ShapeDtypeStruct((slots, slots), jnp.bfloat16),), 10**10, (order % per_source,),
     )
     parts, codes, stride = [chosen], [0], ep_count
@@ -132,12 +132,13 @@
         radix = 4 if stride % 4 == 0 else 2
         stride //= radix
         codes = [k * stride + c for k in range(radix) for c in codes]
+        first = stride * radix == ep_count
         parts = gather_round(ids, stride, radix, ep_count)
-        if stride * radix == ep_count:
+        if first:
             parts, spread = lax.optimization_barrier((parts, spread))
 
     outgoing, row = call(
-        pick_kernel, "pick", [VMEM] * (4 + len(parts)),
+        pick_kernel, [VMEM] * (4 + len(parts)),
         (
             jax.ShapeDtypeStruct((rows, width), tokens.dtype),
             jax.ShapeDtypeStruct((1, slots), jnp.int32),
@@ -153,11 +154,11 @@
     pre = jax.ShapeDtypeStruct((rows, units), jnp.float32)
     product = 2 * rows * width * units
     gate_pre, up_pre = call(
-        first_kernel, "ffn_first", [VMEM] * 4, (pre, pre), 2 * product,
+        first_kernel, [VMEM] * 4, (pre, pre), 2 * product,
         (arrived, gate_weight, up_weight, down_weight),
     )
     hidden, sent = call(
-        second_kernel, "ffn_second", [VMEM] * 7,
+        second_kernel, [VMEM] * 7,
         (
             jax.ShapeDtypeStruct((rows, units), jnp.bfloat16),
             jax.ShapeDtypeStruct((rows, width), jnp.bfloat16),
@@ -167,7 +168,7 @@
     )
     got = lax.ppermute(sent, "tp", swap)
     (kept,) = call(
-        third_kernel, "ffn_third", [VMEM] * 2,
+        third_kernel, [VMEM] * 2,
         (jax.ShapeDtypeStruct((rows, width), jnp.float32),), product,
         (hidden, down_weight),
     )
@@ -176,7 +177,7 @@
         weighted.reshape(ep_count, per_source, width), "ep", split_axis=0, concat_axis=0, tiled=True
     ).reshape(rows, width)
     (mixed_out,) = call(
-        mix_kernel, "mix", [VMEM] * 2, (jax.ShapeDtypeStruct((tok_rows, width), jnp.bfloat16),),
+        mix_kernel, [VMEM] * 2, (jax.ShapeDtypeStruct((tok_rows, width), jnp.bfloat16),),
         2 * rows * tok_rows * width, (row, returned),
     )
     return mixed_out
@@ -192,6 +193,4 @@
         P("ep", "tp", None),
     )
     out_specs = P("ep", "tp")
-    return jax.shard_map(
-        on_device, mesh=mesh, in_specs=in_specs, out_specs=out_specs, check_vma=False
-    )
+    return jax.shard_map(layer, mesh=mesh, in_specs=in_specs, out_specs=out_specs, check_vma=False)

time: 73.7 us -> 73.7 us (level)
  no operation moved by 1% of the time
where the time goes in v6:
time: 73.7 us; the launch traced here: 73.5 us
  blocking collectives  46 us (62%)
  waiting for transfers between devices  10.1 us (14%)
  starting transfers between devices  9.4 us (13%)
  Pallas kernels  7.44 us (10%)
    all_to_all x1, blocking collectives, layer(): lax.all_to_all(weighted.reshape(ep_count, per_source, width), 'ep', split...  24.8 us
    all_to_all x1, blocking collectives, layer(): lax.all_to_all(outgoing.reshape(ep_count, per_source, width), 'ep', split...  21.3 us
    ppermute x6, starting transfers between devices, gather_round(): lax.ppermute(value, 'ep', [(e, e ^ k * stride) for e in range(count)])  9.2 us
    ppermute x6, waiting for transfers between devices, gather_round(): lax.ppermute(value, 'ep', [(e, e ^ k * stride) for e in range(count)])  8.54 us
    pallas_call x6, Pallas kernels, call(): pl.pallas_call(body, out_shape=outs, in_specs=in_specs, out_specs=tuple((...  7.44 us
  transfers between devices with their start and end apart: 8, of which 8 were waited for; matrix products, arithmetic and copies ran while one was open for 0% of the time, Pallas kernels for 4%

profile of v6, /device:TPU:0, one launch (start us, length us, event | category | flops | bytes accessed | tf_op | source)
XLA Modules:
  0.0 73.5 jit_solution(12556809214526343915)
XLA Ops:
  0.0 4.1 %collective-permute-start.1 = (s32[1,384]{1,0:T(1,128)}, s32[1,384]{1,0:T(1,128)S(1)}, u32[]{:S(2)}, u32[]{:S(2)}) collective-permute-start(s32[1,384]{1,0:T(1,128)} %param.8), channel_id=1, source_target_pairs={{0,16},{2,18},{4,20},{6,22},{8,24},{10,26},{12,28},{14,30},{16,0},... | collective-permute-start | bytes 4616 | tf_op jit(solution)/shard_map/ppermute | solution.py:111
  4.1 1.6 %collective-permute-start = (s32[1,384]{1,0:T(1,128)}, s32[1,384]{1,0:T(1,128)S(1)}, u32[]{:S(2)}, u32[]{:S(2)}) collective-permute-start(s32[1,384]{1,0:T(1,128)} %param.8), channel_id=1, source_target_pairs={{0,8},{2,10},{4,12},{6,14},{8,0},{10,2},{12,4},{14,6},{16,24},{18,... | collective-permute-start | bytes 4616 | tf_op jit(solution)/shard_map/ppermute | solution.py:111
  5.6 0.0 collective-permute-start.2
  5.7 0.0 copy-start.6
  5.7 0.0 copy-start.4
  5.7 0.0 copy-start.5
  5.7 0.1 shard_map.73.spread_ref
  5.8 0.1 collective-permute-done.1
  5.8 2.0 %collective-permute-done = s32[1,384]{1,0:T(1,128)S(1)} collective-permute-done((s32[1,384]{1,0:T(1,128)}, s32[1,384]{1,0:T(1,128)S(1)}, u32[]{:S(2)}, u32[]{:S(2)}) %collective-permute-start) | collective-permute-done | bytes 1568 | tf_op jit(solution)/shard_map/ppermute | solution.py:111
  7.9 3.4 %collective-permute-done.2 = s32[1,384]{1,0:T(1,128)S(1)} collective-permute-done((s32[1,384]{1,0:T(1,128)}, s32[1,384]{1,0:T(1,128)S(1)}, u32[]{:S(2)}, u32[]{:S(2)}) %collective-permute-start.2) | collective-permute-done | bytes 1568 | tf_op jit(solution)/shard_map/ppermute | solution.py:111
  11.2 0.0 copy-done.6
  11.2 2.5 %collective-permute-start.5 = (s32[4,384]{1,0:T(4,128)S(1)}, s32[4,384]{1,0:T(4,128)S(1)}, u32[]{:S(2)}, u32[]{:S(2)}) collective-permute-start(s32[4,384]{1,0:T(4,128)S(1)} %pad_add_fusion.refs_0_), channel_id=1, source_target_pairs={{0,6},{2,4},{4,2},{6,0},{8,14},{10,12},{12,10},{14,8},{16,22},{18,... | collective-permute-start | bytes 18440 | tf_op jit(solution)/shard_map/ppermute | solution.py:111
  13.8 0.5 collective-permute-start.4
  14.3 0.5 collective-permute-start.3
  14.8 1.0 %collective-permute-done.5.refs_3_ = s32[4,384]{1,0:T(4,128)S(1)} collective-permute-done((s32[4,384]{1,0:T(4,128)S(1)}, s32[4,384]{1,0:T(4,128)S(1)}, u32[]{:S(2)}, u32[]{:S(2)}) %collective-permute-start.5) | collective-permute-done | bytes 6176 | tf_op jit(solution)/shard_map/ppermute | solution.py:111
  15.8 1.5 %collective-permute-done.4.refs_2_ = s32[4,384]{1,0:T(4,128)S(1)} collective-permute-done((s32[4,384]{1,0:T(4,128)S(1)}, s32[4,384]{1,0:T(4,128)S(1)}, u32[]{:S(2)}, u32[]{:S(2)}) %collective-permute-start.4) | collective-permute-done | bytes 6176 | tf_op jit(solution)/shard_map/ppermute | solution.py:111
  17.4 0.5 collective-permute-done.3.refs_1_
  17.9 0.0 copy-done.4
  17.9 0.0 copy-done.5
  17.9 0.0 copy-start
  17.9 0.0 copy-start.1
  17.9 0.0 copy-start.2
  17.9 0.6 shard_map.74
  18.5 21.3 %all_to_all.10 = bf16[16,24,1024]{2,1,0:T(8,128)(2,1)S(1)} all-to-all(bf16[16,24,1024]{2,1,0:T(8,128)(2,1)S(1)} %bitcast.7), channel_id=1, replica_groups=mesh['ep'=16,'tp'=2] {'ep'}, dimensions={0} | all-to-all | bytes 1572864 | tf_op jit(solution)/shard_map/all_to_all | solution.py:150
  39.8 0.0 copy-start.3
  39.8 0.0 collective-permute-start.6
  39.8 0.0 copy-done
  39.8 0.0 copy-done.1
  39.8 0.0 copy-done.2
  39.8 1.8 %shard_map.75 = (f32[384,1024]{1,0:T(8,128)S(1)}, f32[384,1024]{1,0:T(8,128)S(1)}) custom-call(bf16[384,1024]{1,0:T(8,128)(2,1)S(1)} %bitcast.5, bf16[1,2048,1024]{2,1,0:T(8,128)(2,1)S(1)} %copy-done.1, bf16[1,2048,1024]{2,1,0:T(8,128)(2,1)S(1)} %copy-done.2, bf16[1,1024,2048]{2,1,0:T(8,128)(2,1)S(1)} %copy-done), custom_call_target="tpu_custom_call" | custom-call | flops 1610612736 | bytes 16515072 | tf_op jit(solution)/shard_map/pallas_call | solution.py:21
  41.6 0.4 collective-permute-done.6.other_ref
  42.1 0.0 copy-done.3
  42.1 2.9 %shard_map.76 = (bf16[384,1024]{1,0:T(8,128)(2,1)S(1)}, bf16[384,1024]{1,0:T(8,128)(2,1)S(1)}) custom-call(bf16[384,1024]{1,0:T(8,128)(2,1)S(1)} %collective-permute-done.6.other_ref, f32[384,1024]{1,0:T(8,128)S(1)} %get-tuple-element.23.gate_ref, f32[384,1024]{1,0:T(8,128)S(1)} %get-tuple-element.24.up_ref, bf16[1,2048,1024]{2,1,0:T(8,128)(2,1)S(1)} %copy-done.1, ...), custom_call_target="tpu_custom_call" | custom-call | flops 2415919104 | bytes 18089472 | tf_op jit(solution)/shard_map/pallas_call | solution.py:21
  45.0 0.2 collective-permute-start.7
  45.2 1.0 %shard_map.77 = f32[384,1024]{1,0:T(8,128)S(1)} custom-call(bf16[384,1024]{1,0:T(8,128)(2,1)S(1)} %get-tuple-element.25.hidden_ref, bf16[1,1024,2048]{2,1,0:T(8,128)(2,1)S(1)} %copy-done), custom_call_target="tpu_custom_call" | custom-call | flops 805306368 | bytes 6553600 | tf_op jit(solution)/shard_map/pallas_call | solution.py:21
  46.1 1.2 %collective-permute-done.7 = bf16[384,1024]{1,0:T(8,128)(2,1)S(1)} collective-permute-done((bf16[384,1024]{1,0:T(8,128)(2,1)S(1)}, bf16[384,1024]{1,0:T(8,128)(2,1)S(1)}, u32[]{:S(2)}, u32[]{:S(2)}) %collective-permute-start.7) | collective-permute-done | bytes 786464 | tf_op jit(solution)/shard_map/ppermute | solution.py:169
  47.3 0.3 add_convert_fusion
  47.6 24.8 %all_to_all.11 = bf16[16,24,1024]{2,1,0:T(8,128)(2,1)S(1)} all-to-all(bf16[16,24,1024]{2,1,0:T(8,128)(2,1)S(1)} %bitcast.8), channel_id=1, replica_groups=mesh['ep'=16,'tp'=2] {'ep'}, dimensions={0} | all-to-all | bytes 1572864 | tf_op jit(solution)/shard_map/all_to_all | solution.py:176
  72.3 1.1 %shard_map.78 = bf16[192,1024]{1,0:T(8,128)(2,1)} custom-call(s32[1,384]{1,0:T(1,128)S(1)} %get-tuple-element.21.row_ref, bf16[384,1024]{1,0:T(8,128)(2,1)S(1)} %bitcast.6), custom_call_target="tpu_custom_call" | custom-call | flops 150994944 | bytes 1181184 | tf_op jit(solution)/shard_map/pallas_call | solution.py:21
  (3 shorter events, 0.0 us)
Async XLA Ops:
  0.0 5.8 %collective-permute-start.1 = (s32[1,384]{1,0:T(1,128)}, s32[1,384]{1,0:T(1,128)S(1)}, u32[]{:S(2)}, u32[]{:S(2)}) collective-permute-start(s32[1,384]{1,0:T(1,128)} %param.8), channel_id=1, source_target_pairs={{0,16},{2,18},{4,20},{6,22},{8,24},{10,26},{12,28},{14,30},{16,0},... | collective-permute-start | bytes 4616 | tf_op jit(solution)/shard_map/ppermute | solution.py:111
  4.1 3.8 %collective-permute-start = (s32[1,384]{1,0:T(1,128)}, s32[1,384]{1,0:T(1,128)S(1)}, u32[]{:S(2)}, u32[]{:S(2)}) collective-permute-start(s32[1,384]{1,0:T(1,128)} %param.8), channel_id=1, source_target_pairs={{0,8},{2,10},{4,12},{6,14},{8,0},{10,2},{12,4},{14,6},{16,24},{18,... | collective-permute-start | bytes 4616 | tf_op jit(solution)/shard_map/ppermute | solution.py:111
  5.6 5.6 %collective-permute-start.2 = (s32[1,384]{1,0:T(1,128)}, s32[1,384]{1,0:T(1,128)S(1)}, u32[]{:S(2)}, u32[]{:S(2)}) collective-permute-start(s32[1,384]{1,0:T(1,128)} %param.8), channel_id=1, source_target_pairs={{0,24},{2,26},{4,28},{6,30},{8,16},{10,18},{12,20},{14,22},{16,8},... | collective-permute-start | bytes 4616 | tf_op jit(solution)/shard_map/ppermute | solution.py:111
  5.7 5.6 %copy-start.6 = (s32[1,384]{1,0:T(1,128)S(1)}, s32[1,384]{1,0:T(1,128)}, u32[]{:S(2)}) copy-start(s32[1,384]{1,0:T(1,128)} %param.8) | copy-start | bytes 4612
  5.7 12.2 %copy-start.4 = (bf16[192,1024]{1,0:T(8,128)(2,1)S(1)}, bf16[192,1024]{1,0:T(8,128)(2,1)}, u32[]{:S(2)}) copy-start(bf16[192,1024]{1,0:T(8,128)(2,1)} %tokens_ref.1) | copy-start | bytes 1179652
  5.7 12.2 %copy-start.5 = (s32[16,1]{1,0:T(8,128)S(1)}, s32[16,1]{1,0:T(8,128)}, u32[]{:S(2)}) copy-start(s32[16,1]{1,0:T(8,128)} %constant.28.code_ref) | copy-start | bytes 196
  11.2 4.6 %collective-permute-start.5 = (s32[4,384]{1,0:T(4,128)S(1)}, s32[4,384]{1,0:T(4,128)S(1)}, u32[]{:S(2)}, u32[]{:S(2)}) collective-permute-start(s32[4,384]{1,0:T(4,128)S(1)} %pad_add_fusion.refs_0_), channel_id=1, source_target_pairs={{0,6},{2,4},{4,2},{6,0},{8,14},{10,12},{12,10},{14,8},{16,22},{18,... | collective-permute-start | bytes 18440 | tf_op jit(solution)/shard_map/ppermute | solution.py:111
  13.8 3.6 %collective-permute-start.4 = (s32[4,384]{1,0:T(4,128)S(1)}, s32[4,384]{1,0:T(4,128)S(1)}, u32[]{:S(2)}, u32[]{:S(2)}) collective-permute-start(s32[4,384]{1,0:T(4,128)S(1)} %pad_add_fusion.refs_0_), channel_id=1, source_target_pairs={{0,4},{2,6},{4,0},{6,2},{8,12},{10,14},{12,8},{14,10},{16,20},{18,... | collective-permute-start | bytes 18440 | tf_op jit(solution)/shard_map/ppermute | solution.py:111
  14.3 3.6 %collective-permute-start.3 = (s32[4,384]{1,0:T(4,128)S(1)}, s32[4,384]{1,0:T(4,128)S(1)}, u32[]{:S(2)}, u32[]{:S(2)}) collective-permute-start(s32[4,384]{1,0:T(4,128)S(1)} %pad_add_fusion.refs_0_), channel_id=1, source_target_pairs={{0,2},{2,0},{4,6},{6,4},{8,10},{10,8},{12,14},{14,12},{16,18},{18,... | collective-permute-start | bytes 18440 | tf_op jit(solution)/shard_map/ppermute | solution.py:111
  17.9 21.9 %copy-start = (bf16[1,1024,2048]{2,1,0:T(8,128)(2,1)S(1)}, bf16[1,1024,2048]{2,1,0:T(8,128)(2,1)}, u32[]{:S(2)}) copy-start(bf16[1,1024,2048]{2,1,0:T(8,128)(2,1)} %down_w.5) | copy-start | bytes 12582916
  17.9 21.9 %copy-start.1 = (bf16[1,2048,1024]{2,1,0:T(8,128)(2,1)S(1)}, bf16[1,2048,1024]{2,1,0:T(8,128)(2,1)}, u32[]{:S(2)}) copy-start(bf16[1,2048,1024]{2,1,0:T(8,128)(2,1)} %gate_w.3) | copy-start | bytes 12582916
  17.9 21.9 %copy-start.2 = (bf16[1,2048,1024]{2,1,0:T(8,128)(2,1)S(1)}, bf16[1,2048,1024]{2,1,0:T(8,128)(2,1)}, u32[]{:S(2)}) copy-start(bf16[1,2048,1024]{2,1,0:T(8,128)(2,1)} %up_w.3) | copy-start | bytes 12582916
  39.8 2.3 %copy-start.3 = (f32[1,384]{1,0:T(1,128)S(1)}, f32[1,384]{1,0:T(1,128)}, u32[]{:S(2)}) copy-start(f32[1,384]{1,0:T(1,128)} %score_ref.1) | copy-start | bytes 4612
  39.8 2.3 %collective-permute-start.6 = (bf16[384,1024]{1,0:T(8,128)(2,1)S(1)}, bf16[384,1024]{1,0:T(8,128)(2,1)S(1)}, u32[]{:S(2)}, u32[]{:S(2)}) collective-permute-start(bf16[384,1024]{1,0:T(8,128)(2,1)S(1)} %bitcast.4), channel_id=1, source_target_pairs={{0,1},{1,0},{2,3},{3,2},{4,5},{5,4},{6,7},{7,6},{8,9},{9,8},{10,11... | collective-permute-start | bytes 2359304 | tf_op jit(solution)/shard_map/ppermute | solution.py:153
  45.0 2.4 %collective-permute-start.7 = (bf16[384,1024]{1,0:T(8,128)(2,1)S(1)}, bf16[384,1024]{1,0:T(8,128)(2,1)S(1)}, u32[]{:S(2)}, u32[]{:S(2)}) collective-permute-start(bf16[384,1024]{1,0:T(8,128)(2,1)S(1)} %get-tuple-element.26), channel_id=1, source_target_pairs={{0,1},{1,0},{2,3},{3,2},{4,5},{5,4},{6,7},{7,6},{8,9},{9,8},{10,11... | collective-permute-start | bytes 2359304 | tf_op jit(solution)/shard_map/ppermute | solution.py:169

commit v7 on v6

--- a/solution.py
+++ b/solution.py
@@ -15,18 +15,18 @@
     return x.size * x.dtype.itemsize
 
 
-def call(body, in_specs, outs, flops, args, scratch=(), grant=0):
+def call(body, in_specs, outs, flops, args, scratch=(), out_spec=VMEM):
     held = sum(nbytes(x) for x in outs)
     held += sum(nbytes(x) for x, spec in zip(args, in_specs) if spec is VMEM)
     return pl.pallas_call(
         body,
         out_shape=outs,
         in_specs=in_specs,
-        out_specs=tuple(VMEM for _ in outs),
+        out_specs=tuple(out_spec for _ in outs),
         scratch_shapes=scratch,
         cost_estimate=pl.CostEstimate(flops=flops, bytes_accessed=held, transcendentals=0),
         compiler_params=pltpu.CompilerParams(
-            vmem_limit_bytes=grant or min(held + 6 * MIB, 60 * MIB)
+            vmem_limit_bytes=min(held + 6 * MIB, 60 * MIB)
         ),
     )(*args)
 
@@ -97,12 +97,23 @@
     keep_ref[...] = dot(hidden_ref[...], down_w[0, :, half(lax.axis_index("tp"), keep_ref.shape[1])])
 
 
-def mix_kernel(row_ref, returned_ref, out_ref):
-    shape = (out_ref.shape[0], row_ref.shape[1])
+def join_kernel(keep_ref, got_ref, out_ref):
+    out_ref[...] = (keep_ref[...] + got_ref[...].astype(jnp.float32)).astype(jnp.bfloat16)
+
+
+def mix_kernel(row_ref, returned_ref, out_hbm, mixed_ref, sems):
+    tok_rows, width = out_hbm.shape
+    shape = (tok_rows, row_ref.shape[1])
     selector = lax.broadcasted_iota(jnp.int32, shape, 0) == row_ref[...]
-    out_ref[...] = dot(
-        selector.astype(jnp.float32).astype(jnp.bfloat16), returned_ref[...]
-    ).astype(out_ref.dtype)
+    selector = selector.astype(jnp.float32).astype(jnp.bfloat16)
+    copies = []
+    for j in range(2):
+        at = pl.ds(j * width // 2, width // 2)
+        mixed_ref[:, at] = dot(selector, returned_ref[:, at]).astype(mixed_ref.dtype)
+        copies.append(pltpu.make_async_copy(mixed_ref.at[:, at], out_hbm.at[:, at], sems.at[j]))
+        copies[-1].start()
+    for copy in copies:
+        copy.wait()
 
 
 def gather_round(value, stride, radix, count):
@@ -172,13 +183,17 @@
         (jax.ShapeDtypeStruct((rows, width), jnp.float32),), product,
         (hidden, down_weight),
     )
-    weighted = (kept + got.astype(jnp.float32)).astype(jnp.bfloat16)
+    (weighted,) = call(
+        join_kernel, [VMEM] * 2, (jax.ShapeDtypeStruct((rows, width), jnp.bfloat16),),
+        rows * width, (kept, got),
+    )
     returned = lax.all_to_all(
         weighted.reshape(ep_count, per_source, width), "ep", split_axis=0, concat_axis=0, tiled=True
     ).reshape(rows, width)
     (mixed_out,) = call(
         mix_kernel, [VMEM] * 2, (jax.ShapeDtypeStruct((tok_rows, width), jnp.bfloat16),),
         2 * rows * tok_rows * width, (row, returned),
+        [pltpu.VMEM((tok_rows, width), jnp.bfloat16), pltpu.SemaphoreType.DMA((2,))], HBM,
     )
     return mixed_out
 

time: 73.7 us -> 73.5 us (level)
    pallas_call x6 -> x7, Pallas kernels: 7.44 us -> 7.54 us  [call(): pl.pallas_call(body, out_shape=outs, in_specs=in_specs, out_specs=tuple((...]
where the time goes in v7:
time: 73.5 us; the launch traced here: 73.3 us
  blocking collectives  46 us (63%)
  waiting for transfers between devices  10.1 us (14%)
  starting transfers between devices  9.4 us (13%)
  Pallas kernels  7.54 us (10%)
    all_to_all x1, blocking collectives, layer(): lax.all_to_all(weighted.reshape(ep_count, per_source, width), 'ep', split...  24.8 us
    all_to_all x1, blocking collectives, layer(): lax.all_to_all(outgoing.reshape(ep_count, per_source, width), 'ep', split...  21.3 us
    ppermute x6, starting transfers between devices, gather_round(): lax.ppermute(value, 'ep', [(e, e ^ k * stride) for e in range(count)])  9.2 us
    ppermute x6, waiting for transfers between devices, gather_round(): lax.ppermute(value, 'ep', [(e, e ^ k * stride) for e in range(count)])  8.54 us
    pallas_call x7, Pallas kernels, call(): pl.pallas_call(body, out_shape=outs, in_specs=in_specs, out_specs=tuple((...  7.54 us
  transfers between devices with their start and end apart: 8, of which 8 were waited for; matrix products, arithmetic and copies ran while one was open for 0% of the time, Pallas kernels for 4%

profile of v7, /device:TPU:0, one launch (start us, length us, event | category | flops | bytes accessed | tf_op | source)
XLA Modules:
  0.0 73.3 jit_solution(18315955966989033524)
XLA Ops:
  0.0 4.1 %collective-permute-start.1 = (s32[1,384]{1,0:T(1,128)}, s32[1,384]{1,0:T(1,128)S(1)}, u32[]{:S(2)}, u32[]{:S(2)}) collective-permute-start(s32[1,384]{1,0:T(1,128)} %param.8), channel_id=1, source_target_pairs={{0,16},{2,18},{4,20},{6,22},{8,24},{10,26},{12,28},{14,30},{16,0},... | collective-permute-start | bytes 4616 | tf_op jit(solution)/shard_map/ppermute | solution.py:122
  4.1 1.6 %collective-permute-start = (s32[1,384]{1,0:T(1,128)}, s32[1,384]{1,0:T(1,128)S(1)}, u32[]{:S(2)}, u32[]{:S(2)}) collective-permute-start(s32[1,384]{1,0:T(1,128)} %param.8), channel_id=1, source_target_pairs={{0,8},{2,10},{4,12},{6,14},{8,0},{10,2},{12,4},{14,6},{16,24},{18,... | collective-permute-start | bytes 4616 | tf_op jit(solution)/shard_map/ppermute | solution.py:122
  5.6 0.0 collective-permute-start.2
  5.7 0.0 copy-start.6
  5.7 0.0 copy-start.4
  5.7 0.0 copy-start.5
  5.7 0.1 shard_map.73.spread_ref
  5.8 0.1 collective-permute-done.1
  5.8 2.0 %collective-permute-done = s32[1,384]{1,0:T(1,128)S(1)} collective-permute-done((s32[1,384]{1,0:T(1,128)}, s32[1,384]{1,0:T(1,128)S(1)}, u32[]{:S(2)}, u32[]{:S(2)}) %collective-permute-start) | collective-permute-done | bytes 1568 | tf_op jit(solution)/shard_map/ppermute | solution.py:122
  7.9 3.4 %collective-permute-done.2 = s32[1,384]{1,0:T(1,128)S(1)} collective-permute-done((s32[1,384]{1,0:T(1,128)}, s32[1,384]{1,0:T(1,128)S(1)}, u32[]{:S(2)}, u32[]{:S(2)}) %collective-permute-start.2) | collective-permute-done | bytes 1568 | tf_op jit(solution)/shard_map/ppermute | solution.py:122
  11.2 0.0 copy-done.6
  11.2 2.5 %collective-permute-start.5 = (s32[4,384]{1,0:T(4,128)S(1)}, s32[4,384]{1,0:T(4,128)S(1)}, u32[]{:S(2)}, u32[]{:S(2)}) collective-permute-start(s32[4,384]{1,0:T(4,128)S(1)} %pad_add_fusion.refs_0_), channel_id=1, source_target_pairs={{0,6},{2,4},{4,2},{6,0},{8,14},{10,12},{12,10},{14,8},{16,22},{18,... | collective-permute-start | bytes 18440 | tf_op jit(solution)/shard_map/ppermute | solution.py:122
  13.8 0.5 collective-permute-start.4
  14.3 0.5 collective-permute-start.3
  14.8 1.0 %collective-permute-done.5.refs_3_ = s32[4,384]{1,0:T(4,128)S(1)} collective-permute-done((s32[4,384]{1,0:T(4,128)S(1)}, s32[4,384]{1,0:T(4,128)S(1)}, u32[]{:S(2)}, u32[]{:S(2)}) %collective-permute-start.5) | collective-permute-done | bytes 6176 | tf_op jit(solution)/shard_map/ppermute | solution.py:122
  15.8 1.5 %collective-permute-done.4.refs_2_ = s32[4,384]{1,0:T(4,128)S(1)} collective-permute-done((s32[4,384]{1,0:T(4,128)S(1)}, s32[4,384]{1,0:T(4,128)S(1)}, u32[]{:S(2)}, u32[]{:S(2)}) %collective-permute-start.4) | collective-permute-done | bytes 6176 | tf_op jit(solution)/shard_map/ppermute | solution.py:122
  17.4 0.5 collective-permute-done.3.refs_1_
  17.9 0.0 copy-done.4
  17.9 0.0 copy-done.5
  17.9 0.0 copy-start
  17.9 0.0 copy-start.1
  17.9 0.0 copy-start.2
  17.9 0.6 shard_map.74
  18.5 21.3 %all_to_all.10 = bf16[16,24,1024]{2,1,0:T(8,128)(2,1)S(1)} all-to-all(bf16[16,24,1024]{2,1,0:T(8,128)(2,1)S(1)} %bitcast.8), channel_id=1, replica_groups=mesh['ep'=16,'tp'=2] {'ep'}, dimensions={0} | all-to-all | bytes 1572864 | tf_op jit(solution)/shard_map/all_to_all | solution.py:161
  39.8 0.0 copy-start.3
  39.8 0.0 collective-permute-start.6
  39.8 0.0 copy-done
  39.8 0.0 copy-done.1
  39.8 0.0 copy-done.2
  39.8 1.8 %shard_map.75 = (f32[384,1024]{1,0:T(8,128)S(1)}, f32[384,1024]{1,0:T(8,128)S(1)}) custom-call(bf16[384,1024]{1,0:T(8,128)(2,1)S(1)} %bitcast.5, bf16[1,2048,1024]{2,1,0:T(8,128)(2,1)S(1)} %copy-done.1, bf16[1,2048,1024]{2,1,0:T(8,128)(2,1)S(1)} %copy-done.2, bf16[1,1024,2048]{2,1,0:T(8,128)(2,1)S(1)} %copy-done), custom_call_target="tpu_custom_call" | custom-call | flops 1610612736 | bytes 16515072 | tf_op jit(solution)/shard_map/pallas_call | solution.py:21
  41.6 0.4 collective-permute-done.6.other_ref
  42.1 0.0 copy-done.3
  42.1 2.9 %shard_map.76 = (bf16[384,1024]{1,0:T(8,128)(2,1)S(1)}, bf16[384,1024]{1,0:T(8,128)(2,1)S(1)}) custom-call(bf16[384,1024]{1,0:T(8,128)(2,1)S(1)} %collective-permute-done.6.other_ref, f32[384,1024]{1,0:T(8,128)S(1)} %get-tuple-element.23.gate_ref, f32[384,1024]{1,0:T(8,128)S(1)} %get-tuple-element.24.up_ref, bf16[1,2048,1024]{2,1,0:T(8,128)(2,1)S(1)} %copy-done.1, ...), custom_call_target="tpu_custom_call" | custom-call | flops 2415919104 | bytes 18089472 | tf_op jit(solution)/shard_map/pallas_call | solution.py:21
  45.0 0.2 collective-permute-start.7
  45.2 1.0 %shard_map.77.keep_ref = f32[384,1024]{1,0:T(8,128)S(1)} custom-call(bf16[384,1024]{1,0:T(8,128)(2,1)S(1)} %get-tuple-element.25.hidden_ref, bf16[1,1024,2048]{2,1,0:T(8,128)(2,1)S(1)} %copy-done), custom_call_target="tpu_custom_call" | custom-call | flops 805306368 | bytes 6553600 | tf_op jit(solution)/shard_map/pallas_call | solution.py:21
  46.1 1.2 %collective-permute-done.7.got_ref = bf16[384,1024]{1,0:T(8,128)(2,1)S(1)} collective-permute-done((bf16[384,1024]{1,0:T(8,128)(2,1)S(1)}, bf16[384,1024]{1,0:T(8,128)(2,1)S(1)}, u32[]{:S(2)}, u32[]{:S(2)}) %collective-permute-start.7) | collective-permute-done | bytes 786464 | tf_op jit(solution)/shard_map/ppermute | solution.py:180
  47.3 0.2 shard_map.78
  47.5 24.8 %all_to_all.11 = bf16[16,24,1024]{2,1,0:T(8,128)(2,1)S(1)} all-to-all(bf16[16,24,1024]{2,1,0:T(8,128)(2,1)S(1)} %bitcast.7), channel_id=1, replica_groups=mesh['ep'=16,'tp'=2] {'ep'}, dimensions={0} | all-to-all | bytes 1572864 | tf_op jit(solution)/shard_map/all_to_all | solution.py:190
  72.2 1.1 %shard_map.79 = bf16[192,1024]{1,0:T(8,128)(2,1)} custom-call(s32[1,384]{1,0:T(1,128)S(1)} %get-tuple-element.21.row_ref, bf16[384,1024]{1,0:T(8,128)(2,1)S(1)} %bitcast.6), custom_call_target="tpu_custom_call" | custom-call | flops 150994944 | bytes 1181184 | tf_op jit(solution)/shard_map/pallas_call | solution.py:21
  (3 shorter events, 0.0 us)
Async XLA Ops:
  0.0 5.8 %collective-permute-start.1 = (s32[1,384]{1,0:T(1,128)}, s32[1,384]{1,0:T(1,128)S(1)}, u32[]{:S(2)}, u32[]{:S(2)}) collective-permute-start(s32[1,384]{1,0:T(1,128)} %param.8), channel_id=1, source_target_pairs={{0,16},{2,18},{4,20},{6,22},{8,24},{10,26},{12,28},{14,30},{16,0},... | collective-permute-start | bytes 4616 | tf_op jit(solution)/shard_map/ppermute | solution.py:122
  4.1 3.8 %collective-permute-start = (s32[1,384]{1,0:T(1,128)}, s32[1,384]{1,0:T(1,128)S(1)}, u32[]{:S(2)}, u32[]{:S(2)}) collective-permute-start(s32[1,384]{1,0:T(1,128)} %param.8), channel_id=1, source_target_pairs={{0,8},{2,10},{4,12},{6,14},{8,0},{10,2},{12,4},{14,6},{16,24},{18,... | collective-permute-start | bytes 4616 | tf_op jit(solution)/shard_map/ppermute | solution.py:122
  5.6 5.6 %collective-permute-start.2 = (s32[1,384]{1,0:T(1,128)}, s32[1,384]{1,0:T(1,128)S(1)}, u32[]{:S(2)}, u32[]{:S(2)}) collective-permute-start(s32[1,384]{1,0:T(1,128)} %param.8), channel_id=1, source_target_pairs={{0,24},{2,26},{4,28},{6,30},{8,16},{10,18},{12,20},{14,22},{16,8},... | collective-permute-start | bytes 4616 | tf_op jit(solution)/shard_map/ppermute | solution.py:122
  5.7 5.6 %copy-start.6 = (s32[1,384]{1,0:T(1,128)S(1)}, s32[1,384]{1,0:T(1,128)}, u32[]{:S(2)}) copy-start(s32[1,384]{1,0:T(1,128)} %param.8) | copy-start | bytes 4612
  5.7 12.2 %copy-start.4 = (bf16[192,1024]{1,0:T(8,128)(2,1)S(1)}, bf16[192,1024]{1,0:T(8,128)(2,1)}, u32[]{:S(2)}) copy-start(bf16[192,1024]{1,0:T(8,128)(2,1)} %tokens_ref.1) | copy-start | bytes 1179652
  5.7 12.2 %copy-start.5 = (s32[16,1]{1,0:T(8,128)S(1)}, s32[16,1]{1,0:T(8,128)}, u32[]{:S(2)}) copy-start(s32[16,1]{1,0:T(8,128)} %constant.28.code_ref) | copy-start | bytes 196
  11.2 4.6 %collective-permute-start.5 = (s32[4,384]{1,0:T(4,128)S(1)}, s32[4,384]{1,0:T(4,128)S(1)}, u32[]{:S(2)}, u32[]{:S(2)}) collective-permute-start(s32[4,384]{1,0:T(4,128)S(1)} %pad_add_fusion.refs_0_), channel_id=1, source_target_pairs={{0,6},{2,4},{4,2},{6,0},{8,14},{10,12},{12,10},{14,8},{16,22},{18,... | collective-permute-start | bytes 18440 | tf_op jit(solution)/shard_map/ppermute | solution.py:122
  13.8 3.6 %collective-permute-start.4 = (s32[4,384]{1,0:T(4,128)S(1)}, s32[4,384]{1,0:T(4,128)S(1)}, u32[]{:S(2)}, u32[]{:S(2)}) collective-permute-start(s32[4,384]{1,0:T(4,128)S(1)} %pad_add_fusion.refs_0_), channel_id=1, source_target_pairs={{0,4},{2,6},{4,0},{6,2},{8,12},{10,14},{12,8},{14,10},{16,20},{18,... | collective-permute-start | bytes 18440 | tf_op jit(solution)/shard_map/ppermute | solution.py:122
  14.3 3.6 %collective-permute-start.3 = (s32[4,384]{1,0:T(4,128)S(1)}, s32[4,384]{1,0:T(4,128)S(1)}, u32[]{:S(2)}, u32[]{:S(2)}) collective-permute-start(s32[4,384]{1,0:T(4,128)S(1)} %pad_add_fusion.refs_0_), channel_id=1, source_target_pairs={{0,2},{2,0},{4,6},{6,4},{8,10},{10,8},{12,14},{14,12},{16,18},{18,... | collective-permute-start | bytes 18440 | tf_op jit(solution)/shard_map/ppermute | solution.py:122
  17.9 21.9 %copy-start = (bf16[1,1024,2048]{2,1,0:T(8,128)(2,1)S(1)}, bf16[1,1024,2048]{2,1,0:T(8,128)(2,1)}, u32[]{:S(2)}) copy-start(bf16[1,1024,2048]{2,1,0:T(8,128)(2,1)} %down_w.5) | copy-start | bytes 12582916
  17.9 21.9 %copy-start.1 = (bf16[1,2048,1024]{2,1,0:T(8,128)(2,1)S(1)}, bf16[1,2048,1024]{2,1,0:T(8,128)(2,1)}, u32[]{:S(2)}) copy-start(bf16[1,2048,1024]{2,1,0:T(8,128)(2,1)} %gate_w.3) | copy-start | bytes 12582916
  17.9 21.9 %copy-start.2 = (bf16[1,2048,1024]{2,1,0:T(8,128)(2,1)S(1)}, bf16[1,2048,1024]{2,1,0:T(8,128)(2,1)}, u32[]{:S(2)}) copy-start(bf16[1,2048,1024]{2,1,0:T(8,128)(2,1)} %up_w.3) | copy-start | bytes 12582916
  39.8 2.3 %copy-start.3 = (f32[1,384]{1,0:T(1,128)S(1)}, f32[1,384]{1,0:T(1,128)}, u32[]{:S(2)}) copy-start(f32[1,384]{1,0:T(1,128)} %score_ref.1) | copy-start | bytes 4612
  39.8 2.3 %collective-permute-start.6 = (bf16[384,1024]{1,0:T(8,128)(2,1)S(1)}, bf16[384,1024]{1,0:T(8,128)(2,1)S(1)}, u32[]{:S(2)}, u32[]{:S(2)}) collective-permute-start(bf16[384,1024]{1,0:T(8,128)(2,1)S(1)} %bitcast.4), channel_id=1, source_target_pairs={{0,1},{1,0},{2,3},{3,2},{4,5},{5,4},{6,7},{7,6},{8,9},{9,8},{10,11... | collective-permute-start | bytes 2359304 | tf_op jit(solution)/shard_map/ppermute | solution.py:164
  45.0 2.4 %collective-permute-start.7 = (bf16[384,1024]{1,0:T(8,128)(2,1)S(1)}, bf16[384,1024]{1,0:T(8,128)(2,1)S(1)}, u32[]{:S(2)}, u32[]{:S(2)}) collective-permute-start(bf16[384,1024]{1,0:T(8,128)(2,1)S(1)} %get-tuple-element.26), channel_id=1, source_target_pairs={{0,1},{1,0},{2,3},{3,2},{4,5},{5,4},{6,7},{7,6},{8,9},{9,8},{10,11... | collective-permute-start | bytes 2359304 | tf_op jit(solution)/shard_map/ppermute | solution.py:180

commit v8 on v7

--- a/solution.py
+++ b/solution.py
@@ -107,8 +107,8 @@
     selector = lax.broadcasted_iota(jnp.int32, shape, 0) == row_ref[...]
     selector = selector.astype(jnp.float32).astype(jnp.bfloat16)
     copies = []
-    for j in range(2):
-        at = pl.ds(j * width // 2, width // 2)
+    for j in range(4):
+        at = pl.ds(j * width // 4, width // 4)
         mixed_ref[:, at] = dot(selector, returned_ref[:, at]).astype(mixed_ref.dtype)
         copies.append(pltpu.make_async_copy(mixed_ref.at[:, at], out_hbm.at[:, at], sems.at[j]))
         copies[-1].start()
@@ -193,7 +193,7 @@
     (mixed_out,) = call(
         mix_kernel, [VMEM] * 2, (jax.ShapeDtypeStruct((tok_rows, width), jnp.bfloat16),),
         2 * rows * tok_rows * width, (row, returned),
-        [pltpu.VMEM((tok_rows, width), jnp.bfloat16), pltpu.SemaphoreType.DMA((2,))], HBM,
+        [pltpu.VMEM((tok_rows, width), jnp.bfloat16), pltpu.SemaphoreType.DMA((4,))], HBM,
     )
     return mixed_out
 

time: 73.5 us -> 73.5 us (level)
  no operation moved by 1% of the time
where the time goes in v8:
time: 73.5 us; the launch traced here: 73.3 us
  blocking collectives  46 us (63%)
  waiting for transfers between devices  10.1 us (14%)
  starting transfers between devices  9.4 us (13%)
  Pallas kernels  7.55 us (10%)
    all_to_all x1, blocking collectives, layer(): lax.all_to_all(weighted.reshape(ep_count, per_source, width), 'ep', split...  24.8 us
    all_to_all x1, blocking collectives, layer(): lax.all_to_all(outgoing.reshape(ep_count, per_source, width), 'ep', split...  21.3 us
    ppermute x6, starting transfers between devices, gather_round(): lax.ppermute(value, 'ep', [(e, e ^ k * stride) for e in range(count)])  9.2 us
    ppermute x6, waiting for transfers between devices, gather_round(): lax.ppermute(value, 'ep', [(e, e ^ k * stride) for e in range(count)])  8.54 us
    pallas_call x7, Pallas kernels, call(): pl.pallas_call(body, out_shape=outs, in_specs=in_specs, out_specs=tuple((...  7.55 us
  transfers between devices with their start and end apart: 8, of which 8 were waited for; matrix products, arithmetic and copies ran while one was open for 0% of the time, Pallas kernels for 4%

profile of v8, /device:TPU:0, one launch (start us, length us, event | category | flops | bytes accessed | tf_op | source)
XLA Modules:
  0.0 73.3 jit_solution(6793003289278530829)
XLA Ops:
  0.0 4.1 %collective-permute-start.1 = (s32[1,384]{1,0:T(1,128)}, s32[1,384]{1,0:T(1,128)S(1)}, u32[]{:S(2)}, u32[]{:S(2)}) collective-permute-start(s32[1,384]{1,0:T(1,128)} %param.8), channel_id=1, source_target_pairs={{0,16},{2,18},{4,20},{6,22},{8,24},{10,26},{12,28},{14,30},{16,0},... | collective-permute-start | bytes 4616 | tf_op jit(solution)/shard_map/ppermute | solution.py:122
  4.1 1.6 %collective-permute-start = (s32[1,384]{1,0:T(1,128)}, s32[1,384]{1,0:T(1,128)S(1)}, u32[]{:S(2)}, u32[]{:S(2)}) collective-permute-start(s32[1,384]{1,0:T(1,128)} %param.8), channel_id=1, source_target_pairs={{0,8},{2,10},{4,12},{6,14},{8,0},{10,2},{12,4},{14,6},{16,24},{18,... | collective-permute-start | bytes 4616 | tf_op jit(solution)/shard_map/ppermute | solution.py:122
  5.6 0.0 collective-permute-start.2
  5.7 0.0 copy-start.6
  5.7 0.0 copy-start.4
  5.7 0.0 copy-start.5
  5.7 0.1 shard_map.73.spread_ref
  5.8 0.1 collective-permute-done.1
  5.8 2.0 %collective-permute-done = s32[1,384]{1,0:T(1,128)S(1)} collective-permute-done((s32[1,384]{1,0:T(1,128)}, s32[1,384]{1,0:T(1,128)S(1)}, u32[]{:S(2)}, u32[]{:S(2)}) %collective-permute-start) | collective-permute-done | bytes 1568 | tf_op jit(solution)/shard_map/ppermute | solution.py:122
  7.9 3.4 %collective-permute-done.2 = s32[1,384]{1,0:T(1,128)S(1)} collective-permute-done((s32[1,384]{1,0:T(1,128)}, s32[1,384]{1,0:T(1,128)S(1)}, u32[]{:S(2)}, u32[]{:S(2)}) %collective-permute-start.2) | collective-permute-done | bytes 1568 | tf_op jit(solution)/shard_map/ppermute | solution.py:122
  11.2 0.0 copy-done.6
  11.2 2.5 %collective-permute-start.5 = (s32[4,384]{1,0:T(4,128)S(1)}, s32[4,384]{1,0:T(4,128)S(1)}, u32[]{:S(2)}, u32[]{:S(2)}) collective-permute-start(s32[4,384]{1,0:T(4,128)S(1)} %pad_add_fusion.refs_0_), channel_id=1, source_target_pairs={{0,6},{2,4},{4,2},{6,0},{8,14},{10,12},{12,10},{14,8},{16,22},{18,... | collective-permute-start | bytes 18440 | tf_op jit(solution)/shard_map/ppermute | solution.py:122
  13.8 0.5 collective-permute-start.4
  14.3 0.5 collective-permute-start.3
  14.8 1.0 %collective-permute-done.5.refs_3_ = s32[4,384]{1,0:T(4,128)S(1)} collective-permute-done((s32[4,384]{1,0:T(4,128)S(1)}, s32[4,384]{1,0:T(4,128)S(1)}, u32[]{:S(2)}, u32[]{:S(2)}) %collective-permute-start.5) | collective-permute-done | bytes 6176 | tf_op jit(solution)/shard_map/ppermute | solution.py:122
  15.8 1.5 %collective-permute-done.4.refs_2_ = s32[4,384]{1,0:T(4,128)S(1)} collective-permute-done((s32[4,384]{1,0:T(4,128)S(1)}, s32[4,384]{1,0:T(4,128)S(1)}, u32[]{:S(2)}, u32[]{:S(2)}) %collective-permute-start.4) | collective-permute-done | bytes 6176 | tf_op jit(solution)/shard_map/ppermute | solution.py:122
  17.4 0.5 collective-permute-done.3.refs_1_
  17.9 0.0 copy-done.4
  17.9 0.0 copy-done.5
  17.9 0.0 copy-start
  17.9 0.0 copy-start.1
  17.9 0.0 copy-start.2
  17.9 0.6 shard_map.74
  18.5 21.3 %all_to_all.10 = bf16[16,24,1024]{2,1,0:T(8,128)(2,1)S(1)} all-to-all(bf16[16,24,1024]{2,1,0:T(8,128)(2,1)S(1)} %bitcast.8), channel_id=1, replica_groups=mesh['ep'=16,'tp'=2] {'ep'}, dimensions={0} | all-to-all | bytes 1572864 | tf_op jit(solution)/shard_map/all_to_all | solution.py:161
  39.8 0.0 copy-start.3
  39.8 0.0 collective-permute-start.6
  39.8 0.0 copy-done
  39.8 0.0 copy-done.1
  39.8 0.0 copy-done.2
  39.8 1.8 %shard_map.75 = (f32[384,1024]{1,0:T(8,128)S(1)}, f32[384,1024]{1,0:T(8,128)S(1)}) custom-call(bf16[384,1024]{1,0:T(8,128)(2,1)S(1)} %bitcast.5, bf16[1,2048,1024]{2,1,0:T(8,128)(2,1)S(1)} %copy-done.1, bf16[1,2048,1024]{2,1,0:T(8,128)(2,1)S(1)} %copy-done.2, bf16[1,1024,2048]{2,1,0:T(8,128)(2,1)S(1)} %copy-done), custom_call_target="tpu_custom_call" | custom-call | flops 1610612736 | bytes 16515072 | tf_op jit(solution)/shard_map/pallas_call | solution.py:21
  41.6 0.4 collective-permute-done.6.other_ref
  42.1 0.0 copy-done.3
  42.1 2.9 %shard_map.76 = (bf16[384,1024]{1,0:T(8,128)(2,1)S(1)}, bf16[384,1024]{1,0:T(8,128)(2,1)S(1)}) custom-call(bf16[384,1024]{1,0:T(8,128)(2,1)S(1)} %collective-permute-done.6.other_ref, f32[384,1024]{1,0:T(8,128)S(1)} %get-tuple-element.23.gate_ref, f32[384,1024]{1,0:T(8,128)S(1)} %get-tuple-element.24.up_ref, bf16[1,2048,1024]{2,1,0:T(8,128)(2,1)S(1)} %copy-done.1, ...), custom_call_target="tpu_custom_call" | custom-call | flops 2415919104 | bytes 18089472 | tf_op jit(solution)/shard_map/pallas_call | solution.py:21
  45.0 0.2 collective-permute-start.7
  45.2 1.0 %shard_map.77.keep_ref = f32[384,1024]{1,0:T(8,128)S(1)} custom-call(bf16[384,1024]{1,0:T(8,128)(2,1)S(1)} %get-tuple-element.25.hidden_ref, bf16[1,1024,2048]{2,1,0:T(8,128)(2,1)S(1)} %copy-done), custom_call_target="tpu_custom_call" | custom-call | flops 805306368 | bytes 6553600 | tf_op jit(solution)/shard_map/pallas_call | solution.py:21
  46.1 1.2 %collective-permute-done.7.got_ref = bf16[384,1024]{1,0:T(8,128)(2,1)S(1)} collective-permute-done((bf16[384,1024]{1,0:T(8,128)(2,1)S(1)}, bf16[384,1024]{1,0:T(8,128)(2,1)S(1)}, u32[]{:S(2)}, u32[]{:S(2)}) %collective-permute-start.7) | collective-permute-done | bytes 786464 | tf_op jit(solution)/shard_map/ppermute | solution.py:180
  47.3 0.2 shard_map.78
  47.5 24.8 %all_to_all.11 = bf16[16,24,1024]{2,1,0:T(8,128)(2,1)S(1)} all-to-all(bf16[16,24,1024]{2,1,0:T(8,128)(2,1)S(1)} %bitcast.7), channel_id=1, replica_groups=mesh['ep'=16,'tp'=2] {'ep'}, dimensions={0} | all-to-all | bytes 1572864 | tf_op jit(solution)/shard_map/all_to_all | solution.py:190
  72.2 1.1 %shard_map.79 = bf16[192,1024]{1,0:T(8,128)(2,1)} custom-call(s32[1,384]{1,0:T(1,128)S(1)} %get-tuple-element.21.row_ref, bf16[384,1024]{1,0:T(8,128)(2,1)S(1)} %bitcast.6), custom_call_target="tpu_custom_call" | custom-call | flops 150994944 | bytes 1181184 | tf_op jit(solution)/shard_map/pallas_call | solution.py:21
  (3 shorter events, 0.0 us)
Async XLA Ops:
  0.0 5.8 %collective-permute-start.1 = (s32[1,384]{1,0:T(1,128)}, s32[1,384]{1,0:T(1,128)S(1)}, u32[]{:S(2)}, u32[]{:S(2)}) collective-permute-start(s32[1,384]{1,0:T(1,128)} %param.8), channel_id=1, source_target_pairs={{0,16},{2,18},{4,20},{6,22},{8,24},{10,26},{12,28},{14,30},{16,0},... | collective-permute-start | bytes 4616 | tf_op jit(solution)/shard_map/ppermute | solution.py:122
  4.1 3.8 %collective-permute-start = (s32[1,384]{1,0:T(1,128)}, s32[1,384]{1,0:T(1,128)S(1)}, u32[]{:S(2)}, u32[]{:S(2)}) collective-permute-start(s32[1,384]{1,0:T(1,128)} %param.8), channel_id=1, source_target_pairs={{0,8},{2,10},{4,12},{6,14},{8,0},{10,2},{12,4},{14,6},{16,24},{18,... | collective-permute-start | bytes 4616 | tf_op jit(solution)/shard_map/ppermute | solution.py:122
  5.6 5.6 %collective-permute-start.2 = (s32[1,384]{1,0:T(1,128)}, s32[1,384]{1,0:T(1,128)S(1)}, u32[]{:S(2)}, u32[]{:S(2)}) collective-permute-start(s32[1,384]{1,0:T(1,128)} %param.8), channel_id=1, source_target_pairs={{0,24},{2,26},{4,28},{6,30},{8,16},{10,18},{12,20},{14,22},{16,8},... | collective-permute-start | bytes 4616 | tf_op jit(solution)/shard_map/ppermute | solution.py:122
  5.7 5.6 %copy-start.6 = (s32[1,384]{1,0:T(1,128)S(1)}, s32[1,384]{1,0:T(1,128)}, u32[]{:S(2)}) copy-start(s32[1,384]{1,0:T(1,128)} %param.8) | copy-start | bytes 4612
  5.7 12.2 %copy-start.4 = (bf16[192,1024]{1,0:T(8,128)(2,1)S(1)}, bf16[192,1024]{1,0:T(8,128)(2,1)}, u32[]{:S(2)}) copy-start(bf16[192,1024]{1,0:T(8,128)(2,1)} %tokens_ref.1) | copy-start | bytes 1179652
  5.7 12.2 %copy-start.5 = (s32[16,1]{1,0:T(8,128)S(1)}, s32[16,1]{1,0:T(8,128)}, u32[]{:S(2)}) copy-start(s32[16,1]{1,0:T(8,128)} %constant.28.code_ref) | copy-start | bytes 196
  11.2 4.6 %collective-permute-start.5 = (s32[4,384]{1,0:T(4,128)S(1)}, s32[4,384]{1,0:T(4,128)S(1)}, u32[]{:S(2)}, u32[]{:S(2)}) collective-permute-start(s32[4,384]{1,0:T(4,128)S(1)} %pad_add_fusion.refs_0_), channel_id=1, source_target_pairs={{0,6},{2,4},{4,2},{6,0},{8,14},{10,12},{12,10},{14,8},{16,22},{18,... | collective-permute-start | bytes 18440 | tf_op jit(solution)/shard_map/ppermute | solution.py:122
  13.8 3.6 %collective-permute-start.4 = (s32[4,384]{1,0:T(4,128)S(1)}, s32[4,384]{1,0:T(4,128)S(1)}, u32[]{:S(2)}, u32[]{:S(2)}) collective-permute-start(s32[4,384]{1,0:T(4,128)S(1)} %pad_add_fusion.refs_0_), channel_id=1, source_target_pairs={{0,4},{2,6},{4,0},{6,2},{8,12},{10,14},{12,8},{14,10},{16,20},{18,... | collective-permute-start | bytes 18440 | tf_op jit(solution)/shard_map/ppermute | solution.py:122
  14.3 3.6 %collective-permute-start.3 = (s32[4,384]{1,0:T(4,128)S(1)}, s32[4,384]{1,0:T(4,128)S(1)}, u32[]{:S(2)}, u32[]{:S(2)}) collective-permute-start(s32[4,384]{1,0:T(4,128)S(1)} %pad_add_fusion.refs_0_), channel_id=1, source_target_pairs={{0,2},{2,0},{4,6},{6,4},{8,10},{10,8},{12,14},{14,12},{16,18},{18,... | collective-permute-start | bytes 18440 | tf_op jit(solution)/shard_map/ppermute | solution.py:122
  17.9 21.9 %copy-start = (bf16[1,1024,2048]{2,1,0:T(8,128)(2,1)S(1)}, bf16[1,1024,2048]{2,1,0:T(8,128)(2,1)}, u32[]{:S(2)}) copy-start(bf16[1,1024,2048]{2,1,0:T(8,128)(2,1)} %down_w.5) | copy-start | bytes 12582916
  17.9 21.9 %copy-start.1 = (bf16[1,2048,1024]{2,1,0:T(8,128)(2,1)S(1)}, bf16[1,2048,1024]{2,1,0:T(8,128)(2,1)}, u32[]{:S(2)}) copy-start(bf16[1,2048,1024]{2,1,0:T(8,128)(2,1)} %gate_w.3) | copy-start | bytes 12582916
  17.9 21.9 %copy-start.2 = (bf16[1,2048,1024]{2,1,0:T(8,128)(2,1)S(1)}, bf16[1,2048,1024]{2,1,0:T(8,128)(2,1)}, u32[]{:S(2)}) copy-start(bf16[1,2048,1024]{2,1,0:T(8,128)(2,1)} %up_w.3) | copy-start | bytes 12582916
  39.8 2.3 %copy-start.3 = (f32[1,384]{1,0:T(1,128)S(1)}, f32[1,384]{1,0:T(1,128)}, u32[]{:S(2)}) copy-start(f32[1,384]{1,0:T(1,128)} %score_ref.1) | copy-start | bytes 4612
  39.8 2.3 %collective-permute-start.6 = (bf16[384,1024]{1,0:T(8,128)(2,1)S(1)}, bf16[384,1024]{1,0:T(8,128)(2,1)S(1)}, u32[]{:S(2)}, u32[]{:S(2)}) collective-permute-start(bf16[384,1024]{1,0:T(8,128)(2,1)S(1)} %bitcast.4), channel_id=1, source_target_pairs={{0,1},{1,0},{2,3},{3,2},{4,5},{5,4},{6,7},{7,6},{8,9},{9,8},{10,11... | collective-permute-start | bytes 2359304 | tf_op jit(solution)/shard_map/ppermute | solution.py:164
  45.0 2.4 %collective-permute-start.7 = (bf16[384,1024]{1,0:T(8,128)(2,1)S(1)}, bf16[384,1024]{1,0:T(8,128)(2,1)S(1)}, u32[]{:S(2)}, u32[]{:S(2)}) collective-permute-start(bf16[384,1024]{1,0:T(8,128)(2,1)S(1)} %get-tuple-element.26), channel_id=1, source_target_pairs={{0,1},{1,0},{2,3},{3,2},{4,5},{5,4},{6,7},{7,6},{8,9},{9,8},{10,11... | collective-permute-start | bytes 2359304 | tf_op jit(solution)/shard_map/ppermute | solution.py:180

commit v9 on v7

--- a/solution.py
+++ b/solution.py
@@ -47,7 +47,7 @@
 
 
 def pick_kernel(expert_ref, code_ref, spread_ref, tokens_ref, *refs):
-    parts, (out_ref, row_ref, ids_ref) = refs[:-3], refs[-3:]
+    parts, (out_ref, selector_ref, ids_ref) = refs[:-3], refs[-3:]
     me = lax.axis_index("ep")
     tok_rows, slots = tokens_ref.shape[0], spread_ref.shape[0]
     step = parts[0].shape[0]
@@ -55,17 +55,20 @@
     for j, part in enumerate(parts):
         ids_ref[pl.ds(j * step, step), :] = part[...]
     local = ids_ref[...] - me * tok_rows
-    low, high = local & 127, local >> 7
-    both = jnp.concatenate([high, low], axis=0).astype(jnp.float32).astype(jnp.bfloat16)
-    mine = dot(both, spread_ref[...])
-    mine = mine[:count] * 128.0 + mine[count:]
+    if tok_rows <= 256:
+        mine = dot(local.astype(jnp.float32).astype(jnp.bfloat16), spread_ref[...])
+    else:
+        low, high = local & 127, local >> 7
+        both = jnp.concatenate([high, low], axis=0).astype(jnp.float32).astype(jnp.bfloat16)
+        mine = dot(both, spread_ref[...])
+        mine = mine[:count] * 128.0 + mine[count:]
     ours = code_ref[...] == (expert_ref[...] ^ me)
     row = jnp.sum(jnp.where(ours, mine, 0.0), axis=0, keepdims=True).astype(jnp.int32)
-    row_ref[...] = row
     selector = lax.broadcasted_iota(jnp.int32, (tok_rows, slots), 0) == row
+    selector = selector.astype(jnp.float32).astype(jnp.bfloat16)
+    selector_ref[...] = selector
     out_ref[...] = lax.dot_general(
-        selector.astype(jnp.float32).astype(jnp.bfloat16), tokens_ref[...],
-        (((0,), (0,)), ((), ())), preferred_element_type=jnp.float32,
+        selector, tokens_ref[...], (((0,), (0,)), ((), ())), preferred_element_type=jnp.float32
     ).astype(jnp.bfloat16)
 
 
@@ -101,15 +104,12 @@
     out_ref[...] = (keep_ref[...] + got_ref[...].astype(jnp.float32)).astype(jnp.bfloat16)
 
 
-def mix_kernel(row_ref, returned_ref, out_hbm, mixed_ref, sems):
-    tok_rows, width = out_hbm.shape
-    shape = (tok_rows, row_ref.shape[1])
-    selector = lax.broadcasted_iota(jnp.int32, shape, 0) == row_ref[...]
-    selector = selector.astype(jnp.float32).astype(jnp.bfloat16)
+def mix_kernel(selector_ref, returned_ref, out_hbm, mixed_ref, sems):
+    width = out_hbm.shape[1]
     copies = []
     for j in range(2):
         at = pl.ds(j * width // 2, width // 2)
-        mixed_ref[:, at] = dot(selector, returned_ref[:, at]).astype(mixed_ref.dtype)
+        mixed_ref[:, at] = dot(selector_ref[...], returned_ref[:, at]).astype(mixed_ref.dtype)
         copies.append(pltpu.make_async_copy(mixed_ref.at[:, at], out_hbm.at[:, at], sems.at[j]))
         copies[-1].start()
     for copy in copies:
@@ -148,11 +148,11 @@
         if first:
             parts, spread = lax.optimization_barrier((parts, spread))
 
-    outgoing, row = call(
+    outgoing, selector = call(
         pick_kernel, [VMEM] * (4 + len(parts)),
         (
             jax.ShapeDtypeStruct((rows, width), tokens.dtype),
-            jax.ShapeDtypeStruct((1, slots), jnp.int32),
+            jax.ShapeDtypeStruct((tok_rows, slots), jnp.bfloat16),
         ),
         200 * rows * tok_rows * width,
         (order // per_source, jnp.array(codes, jnp.int32)[:, None], spread, tokens, *parts),
@@ -192,7 +192,7 @@
     ).reshape(rows, width)
     (mixed_out,) = call(
         mix_kernel, [VMEM] * 2, (jax.ShapeDtypeStruct((tok_rows, width), jnp.bfloat16),),
-        2 * rows * tok_rows * width, (row, returned),
+        2 * rows * tok_rows * width, (selector, returned),
         [pltpu.VMEM((tok_rows, width), jnp.bfloat16), pltpu.SemaphoreType.DMA((2,))], HBM,
     )
     return mixed_out

time: 73.5 us -> 73.5 us (level)
  no operation moved by 1% of the time
where the time goes in v9:
time: 73.5 us; the launch traced here: 73.3 us
  blocking collectives  46 us (63%)
  waiting for transfers between devices  10.1 us (14%)
  starting transfers between devices  9.4 us (13%)
  Pallas kernels  7.54 us (10%)
    all_to_all x1, blocking collectives, layer(): lax.all_to_all(weighted.reshape(ep_count, per_source, width), 'ep', split...  24.8 us
    all_to_all x1, blocking collectives, layer(): lax.all_to_all(outgoing.reshape(ep_count, per_source, width), 'ep', split...  21.3 us
    ppermute x6, starting transfers between devices, gather_round(): lax.ppermute(value, 'ep', [(e, e ^ k * stride) for e in range(count)])  9.2 us
    ppermute x6, waiting for transfers between devices, gather_round(): lax.ppermute(value, 'ep', [(e, e ^ k * stride) for e in range(count)])  8.54 us
    pallas_call x7, Pallas kernels, call(): pl.pallas_call(body, out_shape=outs, in_specs=in_specs, out_specs=tuple((...  7.54 us
  transfers between devices with their start and end apart: 8, of which 8 were waited for; matrix products, arithmetic and copies ran while one was open for 0% of the time, Pallas kernels for 4%

profile of v9, /device:TPU:0, one launch (start us, length us, event | category | flops | bytes accessed | tf_op | source)
XLA Modules:
  0.0 73.3 jit_solution(12008601326484410077)
XLA Ops:
  0.0 4.1 %collective-permute-start.1 = (s32[1,384]{1,0:T(1,128)}, s32[1,384]{1,0:T(1,128)S(1)}, u32[]{:S(2)}, u32[]{:S(2)}) collective-permute-start(s32[1,384]{1,0:T(1,128)} %param.8), channel_id=1, source_target_pairs={{0,16},{2,18},{4,20},{6,22},{8,24},{10,26},{12,28},{14,30},{16,0},... | collective-permute-start | bytes 4616 | tf_op jit(solution)/shard_map/ppermute | solution.py:122
  4.1 1.6 %collective-permute-start = (s32[1,384]{1,0:T(1,128)}, s32[1,384]{1,0:T(1,128)S(1)}, u32[]{:S(2)}, u32[]{:S(2)}) collective-permute-start(s32[1,384]{1,0:T(1,128)} %param.8), channel_id=1, source_target_pairs={{0,8},{2,10},{4,12},{6,14},{8,0},{10,2},{12,4},{14,6},{16,24},{18,... | collective-permute-start | bytes 4616 | tf_op jit(solution)/shard_map/ppermute | solution.py:122
  5.6 0.0 collective-permute-start.2
  5.7 0.0 copy-start.6
  5.7 0.0 copy-start.4
  5.7 0.0 copy-start.5
  5.7 0.1 shard_map.73.spread_ref
  5.8 0.1 collective-permute-done.1
  5.8 2.0 %collective-permute-done = s32[1,384]{1,0:T(1,128)S(1)} collective-permute-done((s32[1,384]{1,0:T(1,128)}, s32[1,384]{1,0:T(1,128)S(1)}, u32[]{:S(2)}, u32[]{:S(2)}) %collective-permute-start) | collective-permute-done | bytes 1568 | tf_op jit(solution)/shard_map/ppermute | solution.py:122
  7.9 3.4 %collective-permute-done.2 = s32[1,384]{1,0:T(1,128)S(1)} collective-permute-done((s32[1,384]{1,0:T(1,128)}, s32[1,384]{1,0:T(1,128)S(1)}, u32[]{:S(2)}, u32[]{:S(2)}) %collective-permute-start.2) | collective-permute-done | bytes 1568 | tf_op jit(solution)/shard_map/ppermute | solution.py:122
  11.2 0.0 copy-done.6
  11.2 2.5 %collective-permute-start.5 = (s32[4,384]{1,0:T(4,128)S(1)}, s32[4,384]{1,0:T(4,128)S(1)}, u32[]{:S(2)}, u32[]{:S(2)}) collective-permute-start(s32[4,384]{1,0:T(4,128)S(1)} %pad_add_fusion.refs_0_), channel_id=1, source_target_pairs={{0,6},{2,4},{4,2},{6,0},{8,14},{10,12},{12,10},{14,8},{16,22},{18,... | collective-permute-start | bytes 18440 | tf_op jit(solution)/shard_map/ppermute | solution.py:122
  13.8 0.5 collective-permute-start.4
  14.3 0.5 collective-permute-start.3
  14.8 1.0 %collective-permute-done.5.refs_3_ = s32[4,384]{1,0:T(4,128)S(1)} collective-permute-done((s32[4,384]{1,0:T(4,128)S(1)}, s32[4,384]{1,0:T(4,128)S(1)}, u32[]{:S(2)}, u32[]{:S(2)}) %collective-permute-start.5) | collective-permute-done | bytes 6176 | tf_op jit(solution)/shard_map/ppermute | solution.py:122
  15.8 1.5 %collective-permute-done.4.refs_2_ = s32[4,384]{1,0:T(4,128)S(1)} collective-permute-done((s32[4,384]{1,0:T(4,128)S(1)}, s32[4,384]{1,0:T(4,128)S(1)}, u32[]{:S(2)}, u32[]{:S(2)}) %collective-permute-start.4) | collective-permute-done | bytes 6176 | tf_op jit(solution)/shard_map/ppermute | solution.py:122
  17.4 0.5 collective-permute-done.3.refs_1_
  17.9 0.0 copy-done.4
  17.9 0.0 copy-done.5
  17.9 0.0 copy-start
  17.9 0.0 copy-start.1
  17.9 0.0 copy-start.2
  17.9 0.6 shard_map.74
  18.5 21.3 %all_to_all.10 = bf16[16,24,1024]{2,1,0:T(8,128)(2,1)S(1)} all-to-all(bf16[16,24,1024]{2,1,0:T(8,128)(2,1)S(1)} %bitcast.8), channel_id=1, replica_groups=mesh['ep'=16,'tp'=2] {'ep'}, dimensions={0} | all-to-all | bytes 1572864 | tf_op jit(solution)/shard_map/all_to_all | solution.py:161
  39.8 0.0 copy-start.3
  39.8 0.0 collective-permute-start.6
  39.8 0.0 copy-done
  39.8 0.0 copy-done.1
  39.8 0.0 copy-done.2
  39.8 1.8 %shard_map.75 = (f32[384,1024]{1,0:T(8,128)S(1)}, f32[384,1024]{1,0:T(8,128)S(1)}) custom-call(bf16[384,1024]{1,0:T(8,128)(2,1)S(1)} %bitcast.5, bf16[1,2048,1024]{2,1,0:T(8,128)(2,1)S(1)} %copy-done.1, bf16[1,2048,1024]{2,1,0:T(8,128)(2,1)S(1)} %copy-done.2, bf16[1,1024,2048]{2,1,0:T(8,128)(2,1)S(1)} %copy-done), custom_call_target="tpu_custom_call" | custom-call | flops 1610612736 | bytes 16515072 | tf_op jit(solution)/shard_map/pallas_call | solution.py:21
  41.6 0.4 collective-permute-done.6.other_ref
  42.1 0.0 copy-done.3
  42.1 2.9 %shard_map.76 = (bf16[384,1024]{1,0:T(8,128)(2,1)S(1)}, bf16[384,1024]{1,0:T(8,128)(2,1)S(1)}) custom-call(bf16[384,1024]{1,0:T(8,128)(2,1)S(1)} %collective-permute-done.6.other_ref, f32[384,1024]{1,0:T(8,128)S(1)} %get-tuple-element.23.gate_ref, f32[384,1024]{1,0:T(8,128)S(1)} %get-tuple-element.24.up_ref, bf16[1,2048,1024]{2,1,0:T(8,128)(2,1)S(1)} %copy-done.1, ...), custom_call_target="tpu_custom_call" | custom-call | flops 2415919104 | bytes 18089472 | tf_op jit(solution)/shard_map/pallas_call | solution.py:21
  44.9 0.2 collective-permute-start.7
  45.1 1.0 %shard_map.77.keep_ref = f32[384,1024]{1,0:T(8,128)S(1)} custom-call(bf16[384,1024]{1,0:T(8,128)(2,1)S(1)} %get-tuple-element.25.hidden_ref, bf16[1,1024,2048]{2,1,0:T(8,128)(2,1)S(1)} %copy-done), custom_call_target="tpu_custom_call" | custom-call | flops 805306368 | bytes 6553600 | tf_op jit(solution)/shard_map/pallas_call | solution.py:21
  46.1 1.2 %collective-permute-done.7.got_ref = bf16[384,1024]{1,0:T(8,128)(2,1)S(1)} collective-permute-done((bf16[384,1024]{1,0:T(8,128)(2,1)S(1)}, bf16[384,1024]{1,0:T(8,128)(2,1)S(1)}, u32[]{:S(2)}, u32[]{:S(2)}) %collective-permute-start.7) | collective-permute-done | bytes 786464 | tf_op jit(solution)/shard_map/ppermute | solution.py:180
  47.3 0.2 shard_map.78
  47.5 24.8 %all_to_all.11 = bf16[16,24,1024]{2,1,0:T(8,128)(2,1)S(1)} all-to-all(bf16[16,24,1024]{2,1,0:T(8,128)(2,1)S(1)} %bitcast.7), channel_id=1, replica_groups=mesh['ep'=16,'tp'=2] {'ep'}, dimensions={0} | all-to-all | bytes 1572864 | tf_op jit(solution)/shard_map/all_to_all | solution.py:190
  72.2 1.1 %shard_map.79 = bf16[192,1024]{1,0:T(8,128)(2,1)} custom-call(bf16[192,384]{1,0:T(8,128)(2,1)S(1)} %get-tuple-element.21.selector_ref, bf16[384,1024]{1,0:T(8,128)(2,1)S(1)} %bitcast.6), custom_call_target="tpu_custom_call" | custom-call | flops 150994944 | bytes 1327104 | tf_op jit(solution)/shard_map/pallas_call | solution.py:21
  (3 shorter events, 0.0 us)
Async XLA Ops:
  0.0 5.8 %collective-permute-start.1 = (s32[1,384]{1,0:T(1,128)}, s32[1,384]{1,0:T(1,128)S(1)}, u32[]{:S(2)}, u32[]{:S(2)}) collective-permute-start(s32[1,384]{1,0:T(1,128)} %param.8), channel_id=1, source_target_pairs={{0,16},{2,18},{4,20},{6,22},{8,24},{10,26},{12,28},{14,30},{16,0},... | collective-permute-start | bytes 4616 | tf_op jit(solution)/shard_map/ppermute | solution.py:122
  4.1 3.8 %collective-permute-start = (s32[1,384]{1,0:T(1,128)}, s32[1,384]{1,0:T(1,128)S(1)}, u32[]{:S(2)}, u32[]{:S(2)}) collective-permute-start(s32[1,384]{1,0:T(1,128)} %param.8), channel_id=1, source_target_pairs={{0,8},{2,10},{4,12},{6,14},{8,0},{10,2},{12,4},{14,6},{16,24},{18,... | collective-permute-start | bytes 4616 | tf_op jit(solution)/shard_map/ppermute | solution.py:122
  5.6 5.6 %collective-permute-start.2 = (s32[1,384]{1,0:T(1,128)}, s32[1,384]{1,0:T(1,128)S(1)}, u32[]{:S(2)}, u32[]{:S(2)}) collective-permute-start(s32[1,384]{1,0:T(1,128)} %param.8), channel_id=1, source_target_pairs={{0,24},{2,26},{4,28},{6,30},{8,16},{10,18},{12,20},{14,22},{16,8},... | collective-permute-start | bytes 4616 | tf_op jit(solution)/shard_map/ppermute | solution.py:122
  5.7 5.6 %copy-start.6 = (s32[1,384]{1,0:T(1,128)S(1)}, s32[1,384]{1,0:T(1,128)}, u32[]{:S(2)}) copy-start(s32[1,384]{1,0:T(1,128)} %param.8) | copy-start | bytes 4612
  5.7 12.2 %copy-start.4 = (bf16[192,1024]{1,0:T(8,128)(2,1)S(1)}, bf16[192,1024]{1,0:T(8,128)(2,1)}, u32[]{:S(2)}) copy-start(bf16[192,1024]{1,0:T(8,128)(2,1)} %tokens_ref.1) | copy-start | bytes 1179652
  5.7 12.2 %copy-start.5 = (s32[16,1]{1,0:T(8,128)S(1)}, s32[16,1]{1,0:T(8,128)}, u32[]{:S(2)}) copy-start(s32[16,1]{1,0:T(8,128)} %constant.28.code_ref) | copy-start | bytes 196
  11.2 4.6 %collective-permute-start.5 = (s32[4,384]{1,0:T(4,128)S(1)}, s32[4,384]{1,0:T(4,128)S(1)}, u32[]{:S(2)}, u32[]{:S(2)}) collective-permute-start(s32[4,384]{1,0:T(4,128)S(1)} %pad_add_fusion.refs_0_), channel_id=1, source_target_pairs={{0,6},{2,4},{4,2},{6,0},{8,14},{10,12},{12,10},{14,8},{16,22},{18,... | collective-permute-start | bytes 18440 | tf_op jit(solution)/shard_map/ppermute | solution.py:122
  13.8 3.6 %collective-permute-start.4 = (s32[4,384]{1,0:T(4,128)S(1)}, s32[4,384]{1,0:T(4,128)S(1)}, u32[]{:S(2)}, u32[]{:S(2)}) collective-permute-start(s32[4,384]{1,0:T(4,128)S(1)} %pad_add_fusion.refs_0_), channel_id=1, source_target_pairs={{0,4},{2,6},{4,0},{6,2},{8,12},{10,14},{12,8},{14,10},{16,20},{18,... | collective-permute-start | bytes 18440 | tf_op jit(solution)/shard_map/ppermute | solution.py:122
  14.3 3.6 %collective-permute-start.3 = (s32[4,384]{1,0:T(4,128)S(1)}, s32[4,384]{1,0:T(4,128)S(1)}, u32[]{:S(2)}, u32[]{:S(2)}) collective-permute-start(s32[4,384]{1,0:T(4,128)S(1)} %pad_add_fusion.refs_0_), channel_id=1, source_target_pairs={{0,2},{2,0},{4,6},{6,4},{8,10},{10,8},{12,14},{14,12},{16,18},{18,... | collective-permute-start | bytes 18440 | tf_op jit(solution)/shard_map/ppermute | solution.py:122
  17.9 21.9 %copy-start = (bf16[1,1024,2048]{2,1,0:T(8,128)(2,1)S(1)}, bf16[1,1024,2048]{2,1,0:T(8,128)(2,1)}, u32[]{:S(2)}) copy-start(bf16[1,1024,2048]{2,1,0:T(8,128)(2,1)} %down_w.5) | copy-start | bytes 12582916
  17.9 21.9 %copy-start.1 = (bf16[1,2048,1024]{2,1,0:T(8,128)(2,1)S(1)}, bf16[1,2048,1024]{2,1,0:T(8,128)(2,1)}, u32[]{:S(2)}) copy-start(bf16[1,2048,1024]{2,1,0:T(8,128)(2,1)} %gate_w.3) | copy-start | bytes 12582916
  17.9 21.9 %copy-start.2 = (bf16[1,2048,1024]{2,1,0:T(8,128)(2,1)S(1)}, bf16[1,2048,1024]{2,1,0:T(8,128)(2,1)}, u32[]{:S(2)}) copy-start(bf16[1,2048,1024]{2,1,0:T(8,128)(2,1)} %up_w.3) | copy-start | bytes 12582916
  39.8 2.3 %copy-start.3 = (f32[1,384]{1,0:T(1,128)S(1)}, f32[1,384]{1,0:T(1,128)}, u32[]{:S(2)}) copy-start(f32[1,384]{1,0:T(1,128)} %score_ref.1) | copy-start | bytes 4612
  39.8 2.3 %collective-permute-start.6 = (bf16[384,1024]{1,0:T(8,128)(2,1)S(1)}, bf16[384,1024]{1,0:T(8,128)(2,1)S(1)}, u32[]{:S(2)}, u32[]{:S(2)}) collective-permute-start(bf16[384,1024]{1,0:T(8,128)(2,1)S(1)} %bitcast.4), channel_id=1, source_target_pairs={{0,1},{1,0},{2,3},{3,2},{4,5},{5,4},{6,7},{7,6},{8,9},{9,8},{10,11... | collective-permute-start | bytes 2359304 | tf_op jit(solution)/shard_map/ppermute | solution.py:164
  44.9 2.4 %collective-permute-start.7 = (bf16[384,1024]{1,0:T(8,128)(2,1)S(1)}, bf16[384,1024]{1,0:T(8,128)(2,1)S(1)}, u32[]{:S(2)}, u32[]{:S(2)}) collective-permute-start(bf16[384,1024]{1,0:T(8,128)(2,1)S(1)} %get-tuple-element.26), channel_id=1, source_target_pairs={{0,1},{1,0},{2,3},{3,2},{4,5},{5,4},{6,7},{7,6},{8,9},{9,8},{10,11... | collective-permute-start | bytes 2359304 | tf_op jit(solution)/shard_map/ppermute | solution.py:180
